TPU v7x, 256 devices: a whole 4x4x8 slice. The times are simulated.
256 devices in a mesh: ep: 16 (over y, x), tp: 16 (over z, core).
Axes of the slice: x: 4, y: 4, z: 8, core: 2. Of those that a mesh axis runs over, the one named last changes fastest.
Arguments:
- tokens: bfloat16 [512, 4096], P('ep'), may hold values from -6 to 6
- state_matrix: float32 [512, 16, 128, 128], P('ep', 'tp'), may hold values from -1.5 to 1.5
- state_norm: float32 [512, 16, 128], P('ep', 'tp'), may hold values from -4 to 4
- state_max: float32 [512, 16], P('ep', 'tp'), may hold values from -5 to 5
- mixer_gain: float32 [4096], replicated, may hold values from 0.1 to 1.9
- w_query: bfloat16 [4096, 2048], P('ep', 'tp'), may hold values from -0.09375 to 0.09375
- w_key: bfloat16 [4096, 2048], P('ep', 'tp'), may hold values from -0.09375 to 0.09375
- w_value: bfloat16 [4096, 2048], P('ep', 'tp'), may hold values from -0.09375 to 0.09375
- w_outgate: bfloat16 [4096, 2048], P('ep', 'tp'), may hold values from -0.09375 to 0.09375
- w_ingate: bfloat16 [4096, 16], replicated, may hold values from -0.09375 to 0.09375
- w_forget: bfloat16 [4096, 16], replicated, may hold values from -0.09375 to 0.09375
- forget_bias: float32 [16], replicated, may hold values from -2 to 4
- w_proj: bfloat16 [2048, 4096], P('tp', 'ep'), may hold values from -0.125 to 0.125
- ffn_gain: float32 [4096], replicated, may hold values from 0.1 to 1.9
- w_branch: bfloat16 [4096], replicated, may hold values from -0.09375 to 0.09375
- routes: int32 [512, 2], P('ep'), may hold values from 0 to 15, all different within a row; in each aligned block of 32 rows (0 to 31, 32 to 63, ...) at most 6 rows name the same one
- route_weight: float32 [512, 2], P('ep'), may hold values from 0.2 to 1
- expert_gate: bfloat16 [16, 4096, 4096], P('ep', None, 'tp'), may hold values from -0.09375 to 0.09375
- expert_up: bfloat16 [16, 4096, 4096], P('ep', None, 'tp'), may hold values from -0.09375 to 0.09375
- expert_down: bfloat16 [16, 4096, 4096], P('ep', 'tp'), may hold values from -0.09375 to 0.09375
- dense_gate: bfloat16 [4096, 8192], P('ep', 'tp'), may hold values from -0.09375 to 0.09375
- dense_up: bfloat16 [4096, 8192], P('ep', 'tp'), may hold values from -0.09375 to 0.09375
- dense_down: bfloat16 [8192, 4096], P('tp', 'ep'), may hold values from -0.0625 to 0.0625
Outputs:
- layer_out: bfloat16 [512, 4096], P('ep')
- new_matrix: float32 [512, 16, 128, 128], P('ep', 'tp')
- new_norm: float32 [512, 16, 128], P('ep', 'tp')
- new_max: float32 [512, 16], P('ep', 'tp')
Inputs may be any that keep to these rules, and one draw needn't show every extreme that they name: `routes`: each row names 2 different experts. Among the rows of one index of ep (32 sequences) no expert is named more than 6 times, and in some such group one expert is named exactly 6 times.
All inputs are finite; a program needn't handle non-finite values.
Results may differ from a plain program's by a relative error of at most 0.012.
Values may be sent and summed in bfloat16 or wider, within the bound.
A program may use at most 64 MiB of HBM per device.

v0:
```python
import jax
import jax.numpy as jnp
from jax import lax
from jax.sharding import PartitionSpec as P

EPS = 1e-06


def side_by_side(arrays, axis, dim, along):
    ends, at = ([], 0)
    for a in arrays[:-1]:
        at += a.shape[along]
        ends.append(at)
    both = jnp.concatenate(arrays, axis=along)
    return tuple(jnp.split(lax.all_gather(both, axis, axis=dim, tiled=True), ends, axis=along))


def from_everyone(shard, axis):
    devices = lax.axis_size(axis)
    return lax.all_to_all(
        jnp.broadcast_to(shard[None], (devices, *shard.shape)), axis, 0, 0, tiled=True
    )


def laid_out(parts, dim):
    parts = jnp.moveaxis(parts, 0, dim)
    shape = parts.shape
    return parts.reshape(*shape[:dim], shape[dim] * shape[dim + 1], *shape[dim + 2 :])


def collect(shard, axis, dim):
    parts = from_everyone(shard, axis)
    return laid_out(parts, dim)


def total_of_pieces(shard, axis):
    return lax.all_gather(shard, axis).sum(0)


def in_blocks(shard, dim, devices):
    shape = shard.shape
    parts = shard.reshape(*shape[:dim], devices, shape[dim] // devices, *shape[dim + 1 :])
    return jnp.moveaxis(parts, dim, 0)


def sum_at_owner(shard, axis, dim):
    parts = in_blocks(shard, dim, lax.axis_size(axis))
    arrived = lax.all_to_all(parts, axis, split_axis=0, concat_axis=0, tiled=True)
    return arrived.astype(jnp.float32).sum(axis=0)


def in_one_piece(arrays, axis, dim, along):
    both = jnp.concatenate(arrays, axis=along)
    out, at, finished = (sum_at_owner(both, axis, dim), 0, [])
    for a in arrays:
        finished.append(lax.slice_in_dim(out, at, at + a.shape[along], axis=along))
        at += a.shape[along]
    return tuple(finished)


def rms_scale(values, gain):
    wide = values.astype(jnp.float32)
    return wide * lax.rsqrt(jnp.mean(wide * wide, axis=-1, keepdims=True) + EPS) * gain


def slot_numbers(flat_routes, experts_all):
    onehot = (flat_routes[:, None] == jnp.arange(experts_all, dtype=jnp.int32)[None, :]).astype(
        jnp.int32
    )
    before = jnp.cumsum(onehot, axis=0) - onehot
    return jnp.sum(before * onehot, axis=1)


def memory_step(
    query_all,
    key_all,
    value_all,
    outgate,
    gate_in,
    gate_forget,
    state_matrix,
    state_norm,
    state_max,
):
    row_count, head_count = gate_in.shape
    head_size = state_matrix.shape[-1]
    heads_q = query_all.reshape(row_count, head_count, head_size)
    heads_k = key_all.reshape(row_count, head_count, head_size) * head_size ** (-0.5)
    heads_v = value_all.reshape(row_count, head_count, head_size)
    log_keep = jax.nn.log_sigmoid(gate_forget)
    new_max = jnp.maximum(log_keep + state_max, gate_in)
    keep_factor = jnp.exp(log_keep + state_max - new_max)
    write_factor = jnp.exp(gate_in - new_max)
    new_matrix = (
        keep_factor[:, :, None, None] * state_matrix
        + write_factor[:, :, None, None] * heads_k[:, :, :, None] * heads_v[:, :, None, :]
    )
    new_norm = keep_factor[:, :, None] * state_norm + write_factor[:, :, None] * heads_k
    numer = jnp.einsum("bhk,bhkv->bhv", heads_q, new_matrix, precision=lax.Precision.HIGHEST)
    denom = jnp.sum(heads_q * new_norm, axis=-1)
    cell = numer / jnp.maximum(jnp.abs(denom), 1.0)[:, :, None]
    gated = jax.nn.sigmoid(outgate.reshape(row_count, head_count, head_size)) * cell
    mixed_heads = gated.reshape(row_count, head_count * head_size).astype(jnp.bfloat16)
    return (mixed_heads, new_matrix, new_norm, new_max)


def on_device(
    tokens,
    state_matrix,
    state_norm,
    state_max,
    mixer_gain,
    w_query,
    w_key,
    w_value,
    w_outgate,
    w_ingate,
    w_forget,
    forget_bias,
    w_proj,
    ffn_gain,
    w_branch,
    routes,
    route_weight,
    expert_gate,
    expert_up,
    expert_down,
    dense_gate,
    dense_up,
    dense_down,
):
    row_count = tokens.shape[0]
    head_count = state_matrix.shape[1]
    model_width = tokens.shape[1]
    normed = rms_scale(tokens, mixer_gain).astype(jnp.bfloat16)
    head_start = lax.axis_index("tp") * head_count
    gate_in = lax.dynamic_slice_in_dim(
        jnp.dot(normed, w_ingate, preferred_element_type=jnp.float32), head_start, head_count, 1
    )
    forget_all = jnp.dot(normed, w_forget, preferred_element_type=jnp.float32) + forget_bias
    gate_forget = lax.dynamic_slice_in_dim(forget_all, head_start, head_count, 1)
    pieces = side_by_side((w_query, w_key, w_value, w_outgate), "ep", 0, 1)
    projected = tuple(
        (jnp.dot(normed, shard_w, preferred_element_type=jnp.float32) for shard_w in pieces)
    )
    mixed_heads, new_matrix, new_norm, new_max = memory_step(
        projected[0],
        projected[1],
        projected[2],
        projected[3],
        gate_in,
        gate_forget,
        state_matrix,
        state_norm,
        state_max,
    )
    spread_out = jnp.dot(collect(mixed_heads, "ep", 0), w_proj, preferred_element_type=jnp.float32)
    mix_back = lax.all_to_all(spread_out, "ep", split_axis=0, concat_axis=1, tiled=True)
    mixer_out = total_of_pieces(mix_back, "tp")
    residual = (tokens.astype(jnp.float32) + mixer_out).astype(jnp.bfloat16)
    ffn_in = rms_scale(residual, ffn_gain).astype(jnp.bfloat16)
    branch_share = jax.nn.sigmoid(jnp.dot(ffn_in, w_branch, preferred_element_type=jnp.float32))
    dense_spread = lax.all_to_all(ffn_in, "ep", split_axis=1, concat_axis=0, tiled=True)
    dense_g, dense_u = in_one_piece(
        (
            jnp.dot(dense_spread, dense_gate, preferred_element_type=jnp.float32).astype(
                jnp.bfloat16
            ),
            jnp.dot(dense_spread, dense_up, preferred_element_type=jnp.float32).astype(
                jnp.bfloat16
            ),
        ),
        "ep",
        0,
        1,
    )
    dense_hidden = (jax.nn.silu(dense_g) * dense_u).astype(jnp.bfloat16)
    dense_spread_out = jnp.dot(
        collect(dense_hidden, "ep", 0), dense_down, preferred_element_type=jnp.float32
    )
    dense_back = lax.all_to_all(dense_spread_out, "ep", split_axis=0, concat_axis=1, tiled=True)
    ep_count = lax.axis_size("ep")
    local_experts = expert_gate.shape[0]
    experts_all = local_experts * ep_count
    top_count = routes.shape[1]
    capacity = max(2, (row_count * top_count * 4 + 3 * experts_all - 1) // (3 * experts_all))
    flat_routes = routes.reshape(-1)
    slots = slot_numbers(flat_routes, experts_all)
    outbound = (
        jnp.zeros((experts_all, capacity, model_width), jnp.bfloat16)
        .at[flat_routes, slots]
        .set(jnp.repeat(ffn_in, top_count, axis=0))
    )
    arrived = lax.all_to_all(outbound, "ep", split_axis=0, concat_axis=0, tiled=True)
    slot_count = arrived.shape[1]
    grid = arrived.reshape(ep_count, local_experts, slot_count, model_width)
    gate_part = jnp.einsum("secd,edf->secf", grid, expert_gate, preferred_element_type=jnp.float32)
    up_part = jnp.einsum("secd,edf->secf", grid, expert_up, preferred_element_type=jnp.float32)
    hidden = (jax.nn.silu(gate_part) * up_part).astype(jnp.bfloat16)
    partial_out = jnp.einsum(
        "secf,efd->secd", hidden, expert_down, preferred_element_type=jnp.float32
    )
    partial_out = sum_at_owner(partial_out.astype(jnp.bfloat16), "tp", 3)
    partial_out = partial_out.reshape(ep_count * local_experts, slot_count, partial_out.shape[3])
    returned = lax.all_to_all(
        partial_out.astype(jnp.bfloat16), "ep", split_axis=0, concat_axis=0, tiled=True
    ).astype(partial_out.dtype)
    picked = returned[flat_routes, slots].reshape(row_count, top_count, returned.shape[2])
    shares = route_weight / jnp.sum(route_weight, axis=1, keepdims=True)
    expert_rows = jnp.sum(shares[:, :, None] * picked, axis=1)
    dense_slice = sum_at_owner((branch_share[:, None] * dense_back).astype(jnp.bfloat16), "tp", 1)
    width_part = dense_slice.shape[1]
    resid_slice = lax.dynamic_slice_in_dim(
        residual, lax.axis_index("tp") * width_part, width_part, 1
    )
    out_slice = (resid_slice.astype(jnp.float32) + expert_rows + dense_slice).astype(jnp.bfloat16)
    layer_out = collect(out_slice, "tp", 1)
    return (layer_out, new_matrix, new_norm, new_max)


def solution(mesh):
    in_specs = (
        P("ep", None),
        P("ep", "tp", None, None),
        P("ep", "tp", None),
        P("ep", "tp"),
        P(),
        P("ep", "tp"),
        P("ep", "tp"),
        P("ep", "tp"),
        P("ep", "tp"),
        P(),
        P(),
        P(),
        P("tp", "ep"),
        P(),
        P(),
        P("ep", None),
        P("ep", None),
        P("ep", None, "tp"),
        P("ep", None, "tp"),
        P("ep", "tp", None),
        P("ep", "tp"),
        P("ep", "tp"),
        P("tp", "ep"),
    )
    out_specs = (P("ep", None), P("ep", "tp", None, None), P("ep", "tp", None), P("ep", "tp"))
    return jax.shard_map(
        on_device, mesh=mesh, in_specs=in_specs, out_specs=out_specs, check_vma=False
    )
```

profile of v0, /device:TPU:1, one launch (start us, length us, event | category | flops | bytes accessed | tf_op | source)
XLA Modules:
  0.0 338.2 jit_solution(3360213346436248407)
XLA Ops:
  7.3 1.8 pad_maximum_fusion.1
  14.8 56.3 %all-gather.3.cloned.1.call-done = bf16[4096,512]{1,0:T(8,128)(2,1)} async-done(((bf16[256,512]{1,0:T(8,128)(2,1)}), bf16[4096,512]{1,0:T(8,128)(2,1)}) %all-gather.3.cloned.1.call-update) | async-done | bytes 4194320 | tf_op jit(solution)/shard_map/all_gather | solution.py:15
  71.1 1.7 convolution_multiply_fusion
  72.8 2.2 fusion.61
  75.1 1.6 fusion.31
  77.4 1.9 fusion.5
  79.3 1.6 fusion.26
  80.9 11.6 %all_to_all.82 = bf16[16,32,128]{2,1,0:T(8,128)(2,1)S(1)} all-to-all(bf16[16,32,128]{2,1,0:T(8,128)(2,1)S(1)} %broadcast_in_dim.10), channel_id=1, replica_groups=mesh['ep'=16,'tp'=16] {'ep'}, dimensions={0} | all-to-all | bytes 262144 | tf_op jit(solution)/shard_map/all_to_all | solution.py:20
  92.8 12.5 %all_to_all.83 = f32[16,32,256]{2,1,0:T(8,128)S(1)} all-to-all(f32[16,32,256]{2,1,0:T(8,128)S(1)} %fusion.57), channel_id=1, replica_groups=mesh['ep'=16,'tp'=16] {'ep'}, dimensions={0} | all-to-all | bytes 1048576 | tf_op jit(solution)/shard_map/all_to_all | solution.py:158
  106.6 56.4 %all-gather.5.cloned.1.call-done = f32[16,32,4096]{2,1,0:T(8,128)} async-done(((f32[1,32,4096]{2,1,0:T(8,128)}), f32[16,32,4096]{2,1,0:T(8,128)}) %all-gather.5.cloned.1.call-update) | async-done | bytes 8388624 | tf_op jit(solution)/shard_map/all_gather | solution.py:37
  163.0 3.8 %reduce_sum.97 = f32[32,4096]{1,0:T(8,128)S(1)} reduce(f32[16,32,4096]{2,1,0:T(8,128)} %all-gather.5.cloned.1.call-done, f32[]{:T(128)} %constant.13.clone.1), dimensions={0}, to_apply=%region_2.3 | reduce | flops 1966080 | bytes 8912900 | tf_op jit(solution)/shard_map/reduce_sum | solution.py:37
  167.2 14.6 %all_to_all.84 = bf16[32,16,256]{2,0,1:T(8,128)(2,1)S(1)} all-to-all(bf16[32,16,256]{2,0,1:T(8,128)(2,1)S(1)} %bitcast.138), channel_id=1, replica_groups=mesh['ep'=16,'tp'=16] {'ep'}, dimensions={1} | all-to-all | bytes 524288 | tf_op jit(solution)/shard_map/all_to_all | solution.py:163
  183.9 4.3 %all-to-all-start.6 = ((bf16[16,32,1024]{2,1,0:T(8,128)(2,1)}), bf16[16,32,1024]{2,1,0:T(8,128)(2,1)}, u32[]{:S(2)}, u32[]{:S(2)}) async-start(bf16[16,32,1024]{2,1,0:T(8,128)(2,1)} %bitcast.38), calls=%async_computation.6 | async-start | bytes 2097152 | tf_op jit(solution)/shard_map/all_to_all | solution.py:48
  190.5 13.4 %scatter_fusion = bf16[16,6,4096]{2,0,1:T(8,128)(2,1)S(1)} fusion(bf16[16,6,4096]{2,0,1:T(8,128)(2,1)S(1)} %broadcast_in_dim.11, s32[64]{0:T(128)S(1)} %get-tuple-element.28, bf16[64,4096]{1,0:T(8,128)(2,1)} %reshape.229), kind=kCustom, calls=%fused_computation.1 | custom fusion | bytes 1573376 | tf_op jit(solution)/shard_map/scatter | solution.py:192
  203.8 1.4 copy.79
  205.3 6.5 %all-to-all-start.2 = ((bf16[16,6,4096]{2,1,0:T(8,128)(2,1)}), bf16[16,6,4096]{2,1,0:T(8,128)(2,1)S(1)}, u32[]{:S(2)}, u32[]{:S(2)}) async-start(bf16[16,6,4096]{2,1,0:T(8,128)(2,1)} %copy.79), calls=%async_computation.2 | async-start | bytes 2097152 | tf_op jit(solution)/shard_map/all_to_all | solution.py:194
  213.3 13.7 %all-to-all-done.2 = bf16[16,6,4096]{2,1,0:T(8,128)(2,1)S(1)} async-done(((bf16[16,6,4096]{2,1,0:T(8,128)(2,1)}), bf16[16,6,4096]{2,1,0:T(8,128)(2,1)S(1)}, u32[]{:S(2)}, u32[]{:S(2)}) %all-to-all-start.2) | async-done | bytes 786464 | tf_op jit(solution)/shard_map/all_to_all | solution.py:194
  227.9 4.9 %all-to-all-start.7 = ((bf16[16,32,512]{2,1,0:T(8,128)(2,1)}), bf16[16,32,512]{2,1,0:T(8,128)(2,1)}, u32[]{:S(2)}, u32[]{:S(2)}) async-start(bf16[16,32,512]{2,1,0:T(8,128)(2,1)} %broadcast_in_dim.13), calls=%async_computation.7 | async-start | bytes 1048576 | tf_op jit(solution)/shard_map/all_to_all | solution.py:20
  232.8 2.3 fusion.7
  235.1 3.8 %convolution_convert_fusion = bf16[16,6,4096]{2,0,1:T(8,128)(2,1)} fusion(bf16[1,256,4096]{2,1,0:T(8,128)(2,1)S(1)} %copy-done, bf16[1,4096,256]{2,1,0:T(8,128)(2,1)} %param.41, bf16[16,6,4096]{2,1,0:T(8,128)(2,1)S(1)} %all-to-all-done.2, f32[16,1,6,256]{3,0,2,1:T(8,128)S(1)} %fusion.7), kind=kOutput, calls=%fused_computation.2 | convolution fusion | flops 403193856 | bytes 5865472 | tf_op jit(solution)/shard_map/secf,efd->secd/dot_general | solution.py:200
  238.9 2.1 copy.102
  242.2 7.5 %all-to-all-start.3 = ((bf16[16,16,1,6,256]{4,1,3,2,0:T(8,128)(2,1)}), bf16[16,16,1,6,256]{4,1,3,2,0:T(8,128)(2,1)S(1)}, u32[]{:S(2)}, u32[]{:S(2)}) async-start(bf16[16,16,1,6,256]{4,1,3,2,0:T(8,128)(2,1)} %bitcast.130), calls=%async_computation.3 | async-start | bytes 1572864 | tf_op jit(solution)/shard_map/all_to_all | solution.py:48
  249.7 2.1 fusion.49
  251.8 20.6 %all-to-all-done.3 = bf16[16,16,1,6,256]{4,1,3,2,0:T(8,128)(2,1)S(1)} async-done(((bf16[16,16,1,6,256]{4,1,3,2,0:T(8,128)(2,1)}), bf16[16,16,1,6,256]{4,1,3,2,0:T(8,128)(2,1)S(1)}, u32[]{:S(2)}, u32[]{:S(2)}) %all-to-all-start.3) | async-done | bytes 786464 | tf_op jit(solution)/shard_map/all_to_all | solution.py:48
  272.4 5.2 %all-to-all-start.8 = ((f32[16,32,256]{2,1,0:T(8,128)}), f32[16,32,256]{2,1,0:T(8,128)}, u32[]{:S(2)}, u32[]{:S(2)}) async-start(f32[16,32,256]{2,1,0:T(8,128)} %fusion.49), calls=%async_computation.8 | async-start | bytes 1048576 | tf_op jit(solution)/shard_map/all_to_all | solution.py:181
  278.6 9.5 %all-to-all-done.8 = f32[16,32,256]{2,1,0:T(8,128)} async-done(((f32[16,32,256]{2,1,0:T(8,128)}), f32[16,32,256]{2,1,0:T(8,128)}, u32[]{:S(2)}, u32[]{:S(2)}) %all-to-all-start.8) | async-done | bytes 524320 | tf_op jit(solution)/shard_map/all_to_all | solution.py:181
  288.1 3.5 %all-to-all-start.4 = ((bf16[16,6,256]{2,1,0:T(8,128)(2,1)}), bf16[16,6,256]{2,1,0:T(8,128)(2,1)S(1)}, u32[]{:S(2)}, u32[]{:S(2)}) async-start(bf16[16,6,256]{2,1,0:T(8,128)(2,1)} %copy.83), calls=%async_computation.4 | async-start | bytes 131072 | tf_op jit(solution)/shard_map/all_to_all | solution.py:205
  291.6 1.9 multiply_convert_fusion
  293.5 5.0 %all-to-all-done.4 = bf16[16,6,256]{2,1,0:T(8,128)(2,1)S(1)} async-done(((bf16[16,6,256]{2,1,0:T(8,128)(2,1)}), bf16[16,6,256]{2,1,0:T(8,128)(2,1)S(1)}, u32[]{:S(2)}, u32[]{:S(2)}) %all-to-all-start.4) | async-done | bytes 49184 | tf_op jit(solution)/shard_map/all_to_all | solution.py:205
  298.4 5.4 %all-to-all-start.9 = ((bf16[16,32,256]{2,1,0:T(8,128)(2,1)}), bf16[16,32,256]{2,1,0:T(8,128)(2,1)S(1)}, u32[]{:S(2)}, u32[]{:S(2)}) async-start(bf16[16,32,256]{2,1,0:T(8,128)(2,1)} %multiply_convert_fusion), calls=%async_computation.9 | async-start | bytes 524288 | tf_op jit(solution)/shard_map/all_to_all | solution.py:48
  305.1 10.4 %all-to-all-done.9 = bf16[16,32,256]{2,1,0:T(8,128)(2,1)S(1)} async-done(((bf16[16,32,256]{2,1,0:T(8,128)(2,1)}), bf16[16,32,256]{2,1,0:T(8,128)(2,1)S(1)}, u32[]{:S(2)}, u32[]{:S(2)}) %all-to-all-start.9) | async-done | bytes 262176 | tf_op jit(solution)/shard_map/all_to_all | solution.py:48
  316.3 14.4 %all_to_all.85 = bf16[16,32,256]{2,1,0:T(8,128)(2,1)S(1)} all-to-all(bf16[16,32,256]{2,1,0:T(8,128)(2,1)S(1)} %broadcast_in_dim.14), channel_id=1, replica_groups=mesh['ep'=16,'tp'=16] {'tp'}, dimensions={0} | all-to-all | bytes 524288 | tf_op jit(solution)/shard_map/all_to_all | solution.py:20
  (89 shorter events, 19.7 us)
Async XLA Ops:
  7.2 227.9 %copy-start = (bf16[1,256,4096]{2,1,0:T(8,128)(2,1)S(1)}, bf16[1,256,4096]{2,1,0:T(8,128)(2,1)}, u32[]{:S(2)}) copy-start(bf16[1,256,4096]{2,1,0:T(8,128)(2,1)} %param.42) | copy-start | bytes 6291460
  7.2 63.9 %copy-start.4 = (bf16[32,4096]{1,0:T(8,128)(2,1)S(1)}, bf16[32,4096]{1,0:T(8,128)(2,1)}, u32[]{:S(2)}) copy-start(bf16[32,4096]{1,0:T(8,128)(2,1)} %param.23) | copy-start | bytes 786436
  7.2 63.9 %copy-start.16 = (f32[4096]{0:T(1024)S(1)}, f32[4096]{0:T(1024)}, u32[]{:S(2)}) copy-start(f32[4096]{0:T(1024)} %param.27) | copy-start | bytes 49156
  7.2 6.8 %copy-start.14 = (f32[32,1]{0,1:T(1,128)S(1)}, f32[32,1]{0,1:T(1,128)}, u32[]{:S(2)}) copy-start(f32[32,1]{0,1:T(1,128)} %param.26) | copy-start | bytes 388
  7.2 65.6 %copy-start.15 = (f32[32,1,128]{2,1,0:T(1,128)S(1)}, f32[32,1,128]{2,1,0:T(1,128)}, u32[]{:S(2)}) copy-start(f32[32,1,128]{2,1,0:T(1,128)} %param.25) | copy-start | bytes 49156
  7.2 63.9 %all-gather.3.cloned.1.call-start = ((), (), s32[]{:S(2)}) async-start(), calls=%async_computation.11 | async-start | bytes 4456448 | tf_op jit(solution)/shard_map/all_gather | solution.py:15
  9.1 153.8 %all-gather.5.cloned.1.call-start = ((), (), s32[]{:S(2)}) async-start(), calls=%async_computation.12 | async-start | bytes 8912896 | tf_op jit(solution)/shard_map/all_gather | solution.py:37
  14.7 61.9 %copy-start.12 = (f32[32,1]{0,1:T(1,128)}, f32[32,1]{0,1:T(1,128)S(1)}, u32[]{:S(2)}) copy-start(f32[32,1]{0,1:T(1,128)S(1)} %get-tuple-element.35) | copy-start | bytes 388
  71.1 5.5 %copy-start.2 = (f32[32,1,128,128]{3,2,1,0:T(8,128)S(1)}, f32[32,1,128,128]{3,2,1,0:T(8,128)}, u32[]{:S(2)}) copy-start(f32[32,1,128,128]{3,2,1,0:T(8,128)} %param.24) | copy-start | bytes 6291460
  77.4 15.1 %copy-start.1 = (f32[32,1,128,128]{3,2,1,0:T(8,128)}, f32[32,1,128,128]{3,2,1,0:T(8,128)S(1)}, u32[]{:S(2)}) copy-start(f32[32,1,128,128]{3,2,1,0:T(8,128)S(1)} %multiply_add_fusion) | copy-start | bytes 6291460
  77.4 15.1 %copy-start.8 = (bf16[128,256]{1,0:T(8,128)(2,1)S(1)}, bf16[128,256]{1,0:T(8,128)(2,1)}, u32[]{:S(2)}) copy-start(bf16[128,256]{1,0:T(8,128)(2,1)} %param.35) | copy-start | bytes 196612
  106.5 60.5 %copy-start.9 = (f32[4096]{0:T(1024)S(1)}, f32[4096]{0:T(1024)}, u32[]{:S(2)}) copy-start(f32[4096]{0:T(1024)} %param.36) | copy-start | bytes 49156
  166.8 15.0 %copy-start.6 = (bf16[256,512]{1,0:T(8,128)(2,1)S(1)}, bf16[256,512]{1,0:T(8,128)(2,1)}, u32[]{:S(2)}) copy-start(bf16[256,512]{1,0:T(8,128)(2,1)} %param.44) | copy-start | bytes 786436
  166.8 15.3 %copy-start.7 = (bf16[256,512]{1,0:T(8,128)(2,1)S(1)}, bf16[256,512]{1,0:T(8,128)(2,1)}, u32[]{:S(2)}) copy-start(bf16[256,512]{1,0:T(8,128)(2,1)} %param.43) | copy-start | bytes 786436
  167.0 15.1 %copy-start.3 = (bf16[32,4096]{1,0:T(8,128)(2,1)}, bf16[32,4096]{1,0:T(8,128)(2,1)S(1)}, u32[]{:S(2)}) copy-start(bf16[32,4096]{1,0:T(8,128)(2,1)S(1)} %get-tuple-element.31) | copy-start | bytes 786436
  182.5 5.7 %copy-start.13 = (s32[32,2]{0,1:T(2,128)S(1)}, s32[32,2]{0,1:T(2,128)}, u32[]{:S(2)}) copy-start(s32[32,2]{0,1:T(2,128)} %param.38) | copy-start | bytes 772
  183.9 21.4 %all-to-all-start.6 = ((bf16[16,32,1024]{2,1,0:T(8,128)(2,1)}), bf16[16,32,1024]{2,1,0:T(8,128)(2,1)}, u32[]{:S(2)}, u32[]{:S(2)}) async-start(bf16[16,32,1024]{2,1,0:T(8,128)(2,1)} %bitcast.38), calls=%async_computation.6 | async-start | bytes 2097152 | tf_op jit(solution)/shard_map/all_to_all | solution.py:48
  205.3 21.7 %all-to-all-start.2 = ((bf16[16,6,4096]{2,1,0:T(8,128)(2,1)}), bf16[16,6,4096]{2,1,0:T(8,128)(2,1)S(1)}, u32[]{:S(2)}, u32[]{:S(2)}) async-start(bf16[16,6,4096]{2,1,0:T(8,128)(2,1)} %copy.79), calls=%async_computation.2 | async-start | bytes 2097152 | tf_op jit(solution)/shard_map/all_to_all | solution.py:194
  227.9 14.3 %all-to-all-start.7 = ((bf16[16,32,512]{2,1,0:T(8,128)(2,1)}), bf16[16,32,512]{2,1,0:T(8,128)(2,1)}, u32[]{:S(2)}, u32[]{:S(2)}) async-start(bf16[16,32,512]{2,1,0:T(8,128)(2,1)} %broadcast_in_dim.13), calls=%async_computation.7 | async-start | bytes 1048576 | tf_op jit(solution)/shard_map/all_to_all | solution.py:20
  238.9 10.8 %copy-start.5 = (bf16[512,256]{1,0:T(8,128)(2,1)S(1)}, bf16[512,256]{1,0:T(8,128)(2,1)}, u32[]{:S(2)}) copy-start(bf16[512,256]{1,0:T(8,128)(2,1)} %param.45) | copy-start | bytes 786436
  241.0 36.5 %copy-start.11 = (f32[32,2]{0,1:T(2,128)S(1)}, f32[32,2]{0,1:T(2,128)}, u32[]{:S(2)}) copy-start(f32[32,2]{0,1:T(2,128)} %param.39) | copy-start | bytes 772
  241.1 36.5 %copy-start.10 = (bf16[4096]{0:T(1024)(128)(2,1)S(1)}, bf16[4096]{0:T(1024)(128)(2,1)}, u32[]{:S(2)}) copy-start(bf16[4096]{0:T(1024)(128)(2,1)} %param.37) | copy-start | bytes 24580
  242.2 30.2 %all-to-all-start.3 = ((bf16[16,16,1,6,256]{4,1,3,2,0:T(8,128)(2,1)}), bf16[16,16,1,6,256]{4,1,3,2,0:T(8,128)(2,1)S(1)}, u32[]{:S(2)}, u32[]{:S(2)}) async-start(bf16[16,16,1,6,256]{4,1,3,2,0:T(8,128)(2,1)} %bitcast.130), calls=%async_computation.3 | async-start | bytes 1572864 | tf_op jit(solution)/shard_map/all_to_all | solution.py:48
  272.4 15.7 %all-to-all-start.8 = ((f32[16,32,256]{2,1,0:T(8,128)}), f32[16,32,256]{2,1,0:T(8,128)}, u32[]{:S(2)}, u32[]{:S(2)}) async-start(f32[16,32,256]{2,1,0:T(8,128)} %fusion.49), calls=%async_computation.8 | async-start | bytes 1048576 | tf_op jit(solution)/shard_map/all_to_all | solution.py:181
  288.1 10.3 %all-to-all-start.4 = ((bf16[16,6,256]{2,1,0:T(8,128)(2,1)}), bf16[16,6,256]{2,1,0:T(8,128)(2,1)S(1)}, u32[]{:S(2)}, u32[]{:S(2)}) async-start(bf16[16,6,256]{2,1,0:T(8,128)(2,1)} %copy.83), calls=%async_computation.4 | async-start | bytes 131072 | tf_op jit(solution)/shard_map/all_to_all | solution.py:205
  298.4 17.0 %all-to-all-start.9 = ((bf16[16,32,256]{2,1,0:T(8,128)(2,1)}), bf16[16,32,256]{2,1,0:T(8,128)(2,1)S(1)}, u32[]{:S(2)}, u32[]{:S(2)}) async-start(bf16[16,32,256]{2,1,0:T(8,128)(2,1)} %multiply_convert_fusion), calls=%async_computation.9 | async-start | bytes 524288 | tf_op jit(solution)/shard_map/all_to_all | solution.py:48
Sparse Core Ops, SparseCore 0:
  11.0 60.0 all-gather.2
  106.7 56.2 all-gather.4
where the time goes:
time: 340 us; the launch traced here: 338 us
  waiting for transfers between devices  173 us (51%)
  blocking collectives  53.1 us (16%)
  starting transfers between devices  37.5 us (11%)
  local copies, waits for them, and re-layouts  26 us (8%)
  matrix products  20.7 us (6%)
  between operations  14.5 us (4%)
  other arithmetic  13.4 us (4%)
    all_gather x1, waiting for transfers between devices, total_of_pieces(): return lax.all_gather(shard, axis).sum(0)  56.4 us
    all_gather x1, waiting for transfers between devices, side_by_side(): lax.all_gather(both, axis, axis=dim, tiled=True)  56.3 us
    all_to_all x3, waiting for transfers between devices, sum_at_owner(): lax.all_to_all(parts, axis, split_axis=0, concat_axis=0, tiled=True)  31 us
    all_to_all x2, blocking collectives, from_everyone(): lax.all_to_all(jnp.broadcast_to(shard[None], (devices, *shard.shape)), ax...  26 us
    all_to_all x3, starting transfers between devices, sum_at_owner(): lax.all_to_all(parts, axis, split_axis=0, concat_axis=0, tiled=True)  17.3 us
    scatter x2, local copies, waits for them, and re-layouts, on_device(): outbound = jnp.zeros((experts_all, capacity, model_width), jnp.bfloat16)....  14.8 us
    all_to_all x1, blocking collectives, on_device(): lax.all_to_all(ffn_in, 'ep', split_axis=1, concat_axis=0, tiled=True)  14.6 us
    all_to_all x1, waiting for transfers between devices, on_device(): lax.all_to_all(outbound, 'ep', split_axis=0, concat_axis=0, tiled=True)  13.7 us
  transfers between devices with their start and end apart: 9, of which 8 were waited for; matrix products, arithmetic and copies ran while one was open for 11% of the time, Pallas kernels for 0%

commit v1 on v0

v1 whole, which is shorter than its diff:
```python
import functools

import jax
import jax.numpy as jnp
from jax import lax
from jax.experimental import pallas as pl
from jax.experimental.pallas import tpu as pltpu
from jax.sharding import PartitionSpec as P

EPS = 1e-06
MESH = pl.DeviceIdType.MESH
CAP = 6
SLOT = 8
F32 = jnp.float32
BF16 = jnp.bfloat16
HIGHEST = lax.Precision.HIGHEST
NT = (((1,), (1,)), ((), ()))


def iota(shape, dim):
    return lax.broadcasted_iota(jnp.int32, shape, dim)


def to_column(row, rows):
    diag = iota((rows, row.shape[1]), 0) == iota((rows, row.shape[1]), 1)
    return jnp.sum(jnp.where(diag, row, 0.0), axis=1, keepdims=True)


def to_row(column, lanes):
    rows = column.shape[0]
    diag = iota((rows, lanes), 0) == iota((rows, lanes), 1)
    return jnp.sum(jnp.where(diag, column, 0.0), axis=0, keepdims=True)


TOK, KEY, QKV, MIX, PRJ, RES, ROW, STA, DEN, HID, DWN, EXP, RET, OUT = range(14)
PHASES = 14


def layer_kernel(
    n,
    tok_h, sm_h, sn_h, smax_h, mgain_h, wq_h, wk_h, wv_h, wo_h, win_h, wfo_h, fbias_h,
    wproj_h, fgain_h, wbr_h, routes_h, rw_h, eg_h, eu_h, ed_h, dg_h, du_h, dd_h,
    out_h, nm_h, nn_h, nmax_h,
    tok, sm, sn, smax, mgain, wqkv, wgates, fbias, wproj, fgain, wbr, routes, rw,
    eg, eu, ed, dgu, dd,
    tok_all, key_all, qkv_part, qkv_in, mix_all, prj_part, prj_in, res_all,
    row_out, row_in, sta_out, sta_in, den_part, den_in, hid_all, dwn_part, dwn_in,
    exp_part, exp_in, ret_out, ret_in, fin_out, fin_in, out_own,
    nm, nn, nmax, pick, gu_acc, gates, wkt, qt, vrow, keep_rows, numer, ret_w,
    load_sem, send_sem, recv_sem, fin_sem, store_sem, out_sem,
):
    me_e, me_t = lax.axis_index("ep"), lax.axis_index("tp")
    rows = tok.shape[0]
    width = tok.shape[1]
    block = width // n
    head = sn.shape[1]
    hid_e = eg.shape[1]
    hid_d = dd.shape[0]
    cap_rows = CAP * n

    loads = [
        (tok_h, tok), (mgain_h, mgain), (fgain_h, fgain), (wbr_h, wbr), (routes_h, routes),
        (rw_h, rw), (win_h, wgates.at[pl.ds(0, n), :]), (wfo_h, wgates.at[pl.ds(n, n), :]),
        (fbias_h, fbias), (smax_h, smax), (sn_h, sn),
        (wq_h, wqkv.at[:, pl.ds(0, head)]), (wk_h, wqkv.at[:, pl.ds(head, head)]),
        (wv_h, wqkv.at[:, pl.ds(2 * head, head)]), (wo_h, wqkv.at[:, pl.ds(3 * head, head)]),
        (sm_h, sm), (wproj_h, wproj), (dg_h, dgu.at[:, pl.ds(0, hid_d)]),
        (du_h, dgu.at[:, pl.ds(hid_d, hid_d)]), (eg_h, eg), (eu_h, eu), (ed_h, ed), (dd_h, dd),
    ]
    loads = [pltpu.make_async_copy(a, b, load_sem.at[k]) for k, (a, b) in enumerate(loads)]
    for copy in loads:
        copy.start()

    barrier = pltpu.get_barrier_semaphore()

    def greet(d, _):
        pl.semaphore_signal(barrier, 1, device_id=(lax.rem(me_e + d, n), me_t), device_id_type=MESH)
        pl.semaphore_signal(barrier, 1, device_id=(me_e, lax.rem(me_t + d, n)), device_id_type=MESH)
        return 0

    lax.fori_loop(1, n, greet, 0)

    @pl.when(me_e != me_t)
    def _():
        pl.semaphore_signal(barrier, 1, device_id=(me_t, me_e), device_id_type=MESH)

    @pl.when(me_e != me_t)
    def _():
        pl.semaphore_wait(barrier, 2 * n - 1)

    @pl.when(me_e == me_t)
    def _():
        pl.semaphore_wait(barrier, 2 * n - 2)

    def ep_copy(phase, src, dst, peer, landing):
        return pltpu.make_async_remote_copy(
            src_ref=src, dst_ref=dst, send_sem=send_sem.at[phase],
            recv_sem=recv_sem.at[phase, landing], device_id=(peer, me_t), device_id_type=MESH)

    def tp_copy(phase, src, dst, peer, landing):
        return pltpu.make_async_remote_copy(
            src_ref=src, dst_ref=dst, send_sem=send_sem.at[phase],
            recv_sem=recv_sem.at[phase, landing], device_id=(me_e, peer), device_id_type=MESH)

    def to_peers(copy, me, phase, src_of, dst):
        def one(d, _):
            peer = lax.rem(me + d, n)
            copy(phase, src_of(peer), dst, peer, me).start()
            return 0

        lax.fori_loop(1, n, one, 0)

    def await_peers(copy, me, phase, buffer, use=None, carry=0):
        def one(d, carry):
            peer = lax.rem(me + n - d, n)
            copy(phase, buffer.at[peer], buffer.at[peer], peer, peer).wait_recv()
            return carry if use is None else use(peer, carry)

        return lax.fori_loop(1, n, one, carry)

    def sent(copy, phase, many):
        copy(phase, many, many, 0, 0).wait_send()

    loads[0].wait()
    to_peers(ep_copy, me_e, TOK,
             lambda peer: tok.at[:, pl.ds(pl.multiple_of(peer * block, block), block)],
             tok_all.at[me_e])
    tok_all[me_e] = tok[:, pl.ds(pl.multiple_of(me_e * block, block), block)]

    loads[4].wait()
    loads[5].wait()
    route_rows = [routes[pl.ds(k, 1), :] for k in range(2)]
    lanes_e = iota((128, rows), 0)
    named = sum(jnp.where(lanes_e == r, 1.0, 0.0) for r in route_rows)
    earlier = jnp.where(iota((rows, rows), 0) < iota((rows, rows), 1), 1.0, 0.0)
    before = jnp.dot(named.astype(BF16), earlier.astype(BF16), preferred_element_type=F32)
    base = (CAP * me_e).astype(F32)
    key = jnp.where(named > 0.0, before + base, -1.0)
    eye = jnp.where(iota((rows, rows), 0) == iota((rows, rows), 1), 1.0, 0.0)
    key_all[me_e] = lax.dot_general(
        eye.astype(BF16), key.astype(BF16), NT, preferred_element_type=F32).astype(BF16)
    to_peers(ep_copy, me_e, KEY, lambda peer: key_all.at[me_e], key_all.at[me_e])
    weights = [rw[pl.ds(k, 1), :] for k in range(2)]
    total = weights[0] + weights[1]
    spots = iota((n * SLOT, rows), 0)
    share_t = jnp.zeros((n * SLOT, rows), F32)
    for r, w in zip(route_rows, weights):
        slot = jnp.sum(jnp.where(lanes_e == r, before, 0.0), axis=0, keepdims=True)
        hit = (spots.astype(F32) == r.astype(F32) * SLOT + slot)
        share_t = share_t + jnp.where(hit, w / total, 0.0)
    ret_w[...] = lax.dot_general(eye, share_t, NT, precision=HIGHEST, preferred_element_type=F32)

    loads[1].wait()
    squares = jnp.zeros((rows, block), F32)
    for k in range(n):
        part = tok[:, k * block:(k + 1) * block].astype(F32)
        squares = squares + part * part
    scale = lax.rsqrt(jnp.sum(squares, axis=1, keepdims=True) / width + EPS)
    loads[6].wait()
    loads[7].wait()
    gate = jnp.zeros((rows, 2 * n), F32)
    for k in range(n):
        cols = slice(k * block, (k + 1) * block)
        gain = mgain[:, cols]
        normed = (tok[:, cols].astype(F32) * scale * gain).astype(BF16)
        gate = gate + lax.dot_general(normed, wgates[:, cols], NT, preferred_element_type=F32)
    for k in range(8, 11):
        loads[k].wait()
    lane = iota((rows, 2 * n), 1)
    gate_in = jnp.sum(jnp.where(lane == me_t, gate, 0.0), axis=1, keepdims=True)
    gate_forget = jnp.sum(jnp.where(lane == me_t + n, gate, 0.0), axis=1, keepdims=True)
    bias = jnp.sum(jnp.where(iota((1, n), 1) == me_t, fbias[...], 0.0), axis=1, keepdims=True)
    gate_forget = gate_forget + bias
    log_keep = jnp.minimum(gate_forget, 0.0) - jnp.log1p(jnp.exp(-jnp.abs(gate_forget)))
    old_max = to_column(smax[...], rows)
    new_max = jnp.maximum(log_keep + old_max, gate_in)
    keep = jnp.exp(log_keep + old_max - new_max)
    write = jnp.exp(gate_in - new_max)
    nmax[...] = to_row(new_max, rows)

    await_peers(ep_copy, me_e, TOK, tok_all)
    for k in range(11, 15):
        loads[k].wait()
    gain_m = mgain[:, pl.ds(pl.multiple_of(me_e * block, block), block)]
    group = 4
    big = group * rows

    def project(c, _):
        at = pl.multiple_of(c * group, group)
        x = tok_all[pl.ds(at, group)].reshape(big, block).astype(F32) * gain_m
        y = jnp.dot(x.astype(BF16), wqkv[...], preferred_element_type=F32)
        qkv_part[pl.ds(at, group)] = y.astype(BF16).reshape(group, rows, 4 * head)

        def one(k, _):
            peer = at + k

            @pl.when(peer != me_e)
            def _():
                ep_copy(QKV, qkv_part.at[peer], qkv_in.at[me_e], peer, me_e).start()

            return 0

        return lax.fori_loop(0, group, one, 0)

    lax.fori_loop(0, n // group, project, 0)

    loads[15].wait()
    y = await_peers(ep_copy, me_e, QKV, qkv_in,
                    lambda peer, acc: acc + qkv_in[peer].astype(F32),
                    qkv_part[me_e].astype(F32)) * scale
    query = y[:, :head]
    keys = y[:, head:2 * head] * head ** (-0.5)
    value = y[:, 2 * head:3 * head]
    outgate = y[:, 3 * head:]
    written = write * keys
    new_norm = keep * sn[...] + written
    nn[...] = new_norm
    denom = jnp.sum(query * new_norm, axis=1, keepdims=True)
    qt[...] = query.T
    wkt[...] = written.T
    vrow[...] = value
    keep_rows[...] = jnp.broadcast_to(keep, (rows, head))
    for b in range(rows):
        numer[pl.ds(b, 1), :] = jnp.sum(qt[:, b:b + 1] * sm[b], axis=0, keepdims=True)
    dots = jnp.sum(query * written, axis=1, keepdims=True)
    num = keep * numer[...] + dots * value
    cell = num / jnp.maximum(jnp.abs(denom), 1.0)
    mix_all[me_e] = (jax.nn.sigmoid(outgate) * cell).astype(BF16)
    to_peers(ep_copy, me_e, MIX, lambda peer: mix_all.at[me_e], mix_all.at[me_e])
    for b in range(rows):
        nm[b] = keep_rows[pl.ds(b, 1), :] * sm[b] + wkt[:, b:b + 1] * vrow[pl.ds(b, 1), :]
    stores = [
        pltpu.make_async_copy(a, b, store_sem.at[k])
        for k, (a, b) in enumerate([(nm, nm_h), (nn, nn_h), (nmax, nmax_h)])
    ]
    for copy in stores:
        copy.start()

    await_peers(ep_copy, me_e, KEY, key_all)
    key_t = lax.dot_general(
        jnp.where(iota((n, 128), 0) == iota((n, 128), 1), 1.0, 0.0).astype(BF16),
        key_all[...].reshape(n * rows, 128), NT, preferred_element_type=F32)
    places = iota((cap_rows, n * rows), 0).astype(F32)
    for e in range(n):
        pick[pl.ds(e * cap_rows, cap_rows), :] = jnp.where(
            places == key_t[e:e + 1, :], 1.0, 0.0).astype(BF16)

    await_peers(ep_copy, me_e, MIX, mix_all)
    loads[16].wait()
    y = jnp.dot(mix_all[...].reshape(n * rows, head), wproj[...], preferred_element_type=F32)
    prj_part[...] = y.astype(BF16).reshape(n, rows, block)
    to_peers(tp_copy, me_t, PRJ, lambda peer: prj_part.at[peer], prj_in.at[me_t])
    mixed = await_peers(tp_copy, me_t, PRJ, prj_in,
                        lambda peer, acc: acc + prj_in[peer].astype(F32),
                        prj_part[me_t].astype(F32))
    residual = (tok_all[me_t].astype(F32) + mixed).astype(BF16)
    res_all[me_t] = residual
    to_peers(tp_copy, me_t, RES, lambda peer: res_all.at[me_t], res_all.at[me_t])
    loads[2].wait()
    loads[3].wait()
    await_peers(tp_copy, me_t, RES, res_all)

    res_flat = res_all[...].reshape(n * rows, block)

    def dispatch(c, _):
        at = pl.multiple_of(c * group, group)
        y = jnp.dot(pick[pl.ds(pl.multiple_of(at * cap_rows, group * cap_rows), group * cap_rows), :],
                    res_flat, preferred_element_type=F32)
        row_out[pl.ds(at, group)] = y.astype(BF16).reshape(group, cap_rows, block)

        def one(k, _):
            peer = at + k

            @pl.when(peer != me_e)
            def _():
                ep_copy(ROW, row_out.at[peer], row_in.at[me_e], peer, me_e).start()

            return 0

        return lax.fori_loop(0, group, one, 0)

    lax.fori_loop(0, n // group, dispatch, 0)
    row_in[me_e] = row_out[me_e]

    mine = pl.multiple_of(me_e * block, block)
    gain_f = fgain[:, pl.ds(mine, block)]
    gain_b = gain_f * wbr[:, pl.ds(mine, block)].astype(F32)

    def stats(b, _):
        r = res_all[b].astype(F32)
        ss = to_row(jnp.sum(r * r, axis=1, keepdims=True), 128)
        br = to_row(jnp.sum(r * gain_b, axis=1, keepdims=True), 128)
        sta_out[b] = jnp.where(iota((8, 128), 0) == 0, ss, br)
        return 0

    lax.fori_loop(0, n, stats, 0)
    to_peers(ep_copy, me_e, STA, lambda peer: sta_out.at[peer], sta_in.at[me_e])
    loads[17].wait()
    loads[18].wait()

    def dense(c, _):
        at = pl.multiple_of(c * group, group)
        x = res_all[pl.ds(at, group)].reshape(big, block).astype(F32) * gain_f
        y = jnp.dot(x.astype(BF16), dgu[...], preferred_element_type=F32)
        den_part[pl.ds(at, group)] = y.astype(BF16).reshape(group, rows, 2 * hid_d)

        def one(k, _):
            peer = at + k

            @pl.when(peer != me_e)
            def _():
                ep_copy(DEN, den_part.at[peer], den_in.at[me_e], peer, me_e).start()

            return 0

        return lax.fori_loop(0, group, one, 0)

    lax.fori_loop(0, n // group, dense, 0)

    loads[19].wait()
    loads[20].wait()

    def expert_in(peer, ss):
        x = row_in[peer].astype(F32)
        at = pl.multiple_of(peer * block, block)
        xg = (x * fgain[:, pl.ds(at, block)]).astype(BF16)
        gu_acc[:, pl.ds(0, hid_e)] += jnp.dot(xg, eg[pl.ds(at, block), :], preferred_element_type=F32)
        gu_acc[:, pl.ds(hid_e, hid_e)] += jnp.dot(xg, eu[pl.ds(at, block), :], preferred_element_type=F32)
        return ss + jnp.sum(x * x, axis=1, keepdims=True)

    gu_acc[...] = jnp.zeros_like(gu_acc)
    ss = expert_in(me_e, jnp.zeros((cap_rows, 1), F32))
    ss = await_peers(ep_copy, me_e, ROW, row_in, expert_in, ss)
    row_scale = lax.rsqrt(ss / width + EPS)
    g = gu_acc[:, :hid_e] * row_scale
    u = gu_acc[:, hid_e:] * row_scale
    hidden = (g / (1.0 + jnp.exp(-g)) * u).astype(BF16)
    loads[21].wait()
    for k in range(n):
        exp_part[k] = jnp.dot(hidden, ed[:, k * block:(k + 1) * block],
                              preferred_element_type=F32).astype(BF16)
    to_peers(tp_copy, me_t, EXP, lambda peer: exp_part.at[peer], exp_in.at[me_t])

    sums = await_peers(ep_copy, me_e, STA, sta_in, lambda peer, acc: acc + sta_in[peer], sta_out[me_e])
    dense_scale = lax.rsqrt(to_column(sums[0:1, :], rows) / width + EPS)
    branch = jax.nn.sigmoid(to_column(sums[1:2, :], rows) * dense_scale)
    y = await_peers(ep_copy, me_e, DEN, den_in,
                    lambda peer, acc: acc + den_in[peer].astype(F32),
                    den_part[me_e].astype(F32)) * dense_scale
    g, u = y[:, :hid_d], y[:, hid_d:]
    hid_all[me_e] = (g / (1.0 + jnp.exp(-g)) * u * branch).astype(BF16)
    to_peers(ep_copy, me_e, HID, lambda peer: hid_all.at[me_e], hid_all.at[me_e])

    y = await_peers(tp_copy, me_t, EXP, exp_in,
                    lambda peer, acc: acc + exp_in[peer].astype(F32),
                    exp_part[me_t].astype(F32))
    spot, col = iota((n * SLOT, cap_rows), 0), iota((n * SLOT, cap_rows), 1)
    within = jnp.bitwise_and(spot, SLOT - 1)
    source = CAP * jnp.right_shift(spot, SLOT.bit_length() - 1) + within
    spread = jnp.where((source == col) & (within < CAP), 1.0, 0.0).astype(BF16)
    ret_out[...] = jnp.dot(spread, y.astype(BF16), preferred_element_type=F32).reshape(n, SLOT, block)
    to_peers(ep_copy, me_e, RET, lambda peer: ret_out.at[peer], ret_in.at[me_e])
    ret_in[me_e] = ret_out[me_e]

    await_peers(ep_copy, me_e, HID, hid_all)
    loads[22].wait()
    y = jnp.dot(hid_all[...].reshape(n * rows, hid_d), dd[...], preferred_element_type=F32)
    dwn_part[...] = y.astype(BF16).reshape(n, rows, block)
    to_peers(tp_copy, me_t, DWN, lambda peer: dwn_part.at[peer], dwn_in.at[me_t])

    await_peers(ep_copy, me_e, RET, ret_in)
    routed = jnp.dot(ret_w[...], ret_in[...].reshape(n * SLOT, block), precision=HIGHEST,
                     preferred_element_type=F32)

    y = await_peers(tp_copy, me_t, DWN, dwn_in,
                    lambda peer, acc: acc + dwn_in[peer].astype(F32),
                    dwn_part[me_t].astype(F32))
    fin_out[...] = res_all[me_t].astype(F32) + y

    def crossing():
        return pltpu.make_async_remote_copy(
            src_ref=fin_out, dst_ref=fin_in, send_sem=fin_sem.at[0], recv_sem=fin_sem.at[1],
            device_id=(me_t, me_e), device_id_type=MESH)

    @pl.when(me_e != me_t)
    def _():
        crossing().start()
        crossing().wait()

    @pl.when(me_e == me_t)
    def _():
        fin_in[...] = fin_out[...]

    out_own[...] = (fin_in[...] + routed).astype(BF16)
    place = out_h.at[:, pl.ds(pl.multiple_of(me_t * block, block), block)]
    to_peers(tp_copy, me_t, OUT, lambda peer: out_own, place)
    own = pltpu.make_async_copy(out_own, place, out_sem)
    own.start()

    def landed(d, _):
        peer = lax.rem(me_t + n - d, n)
        spot = out_h.at[:, pl.ds(pl.multiple_of(peer * block, block), block)]
        tp_copy(OUT, out_own, spot, peer, peer).wait_recv()
        return 0

    lax.fori_loop(1, n, landed, 0)
    own.wait()
    for copy in stores:
        copy.wait()
    rest = pl.ds(0, n - 1)
    sent(ep_copy, TOK, tok_all.at[rest])
    sent(ep_copy, KEY, key_all.at[rest])
    sent(ep_copy, QKV, qkv_part.at[rest])
    sent(ep_copy, MIX, mix_all.at[rest])
    sent(tp_copy, PRJ, prj_part.at[rest])
    sent(tp_copy, RES, res_all.at[rest])
    sent(ep_copy, ROW, row_out.at[rest])
    sent(ep_copy, STA, sta_out.at[rest])
    sent(ep_copy, DEN, den_part.at[rest])
    sent(ep_copy, HID, hid_all.at[rest])
    sent(tp_copy, DWN, dwn_part.at[rest])
    sent(tp_copy, EXP, exp_part.at[rest])
    sent(ep_copy, RET, ret_out.at[rest])
    sent(tp_copy, OUT, res_all.at[rest])


def on_device(
    n, tokens, state_matrix, state_norm, state_max, mixer_gain, w_query, w_key, w_value, w_outgate,
    w_ingate, w_forget, forget_bias, w_proj, ffn_gain, w_branch, routes, route_weight,
    expert_gate, expert_up, expert_down, dense_gate, dense_up, dense_down,
):
    rows, width = tokens.shape
    head = state_norm.shape[-1]
    block = width // n
    hid_e, hid_d = expert_gate.shape[2], dense_gate.shape[1]
    cap_rows = CAP * n
    args = (
        tokens,
        state_matrix.reshape(rows, head, head),
        state_norm.reshape(rows, head),
        state_max.T,
        mixer_gain.reshape(1, width),
        w_query, w_key, w_value, w_outgate,
        w_ingate.T, w_forget.T,
        forget_bias.reshape(1, n),
        w_proj,
        ffn_gain.reshape(1, width),
        w_branch.reshape(1, width),
        routes.T, route_weight.T,
        expert_gate.reshape(width, hid_e), expert_up.reshape(width, hid_e),
        expert_down.reshape(hid_e, width),
        dense_gate, dense_up, dense_down,
    )
    vm = pltpu.VMEM
    dma = pltpu.SemaphoreType.DMA
    scratch = [
        vm((rows, width), BF16), vm((rows, head, head), F32), vm((rows, head), F32), vm((1, rows), F32),
        vm((1, width), F32), vm((block, 4 * head), BF16), vm((2 * n, width), BF16), vm((1, n), F32),
        vm((head, block), BF16), vm((1, width), F32), vm((1, width), BF16), vm((2, rows), jnp.int32),
        vm((2, rows), F32), vm((width, hid_e), BF16), vm((width, hid_e), BF16), vm((hid_e, width), BF16),
        vm((block, 2 * hid_d), BF16), vm((hid_d, block), BF16),
        vm((n, rows, block), BF16), vm((n, rows, 128), BF16),
        vm((n, rows, 4 * head), BF16), vm((n, rows, 4 * head), BF16),
        vm((n, rows, head), BF16), vm((n, rows, block), BF16), vm((n, rows, block), BF16),
        vm((n, rows, block), BF16),
        vm((n, cap_rows, block), BF16), vm((n, cap_rows, block), BF16),
        vm((n, 8, 128), F32), vm((n, 8, 128), F32),
        vm((n, rows, 2 * hid_d), BF16), vm((n, rows, 2 * hid_d), BF16),
        vm((n, rows, hid_d), BF16), vm((n, rows, block), BF16), vm((n, rows, block), BF16),
        vm((n, cap_rows, block), BF16), vm((n, cap_rows, block), BF16),
        vm((n, SLOT, block), F32), vm((n, SLOT, block), F32),
        vm((rows, block), F32), vm((rows, block), F32), vm((rows, block), BF16),
        vm((rows, head, head), F32), vm((rows, head), F32), vm((1, rows), F32),
        vm((n * cap_rows, n * rows), BF16), vm((cap_rows, 2 * hid_e), F32), vm((rows, 2 * n), F32),
        vm((head, rows), F32), vm((head, rows), F32), vm((rows, head), F32), vm((rows, head), F32),
        vm((rows, head), F32), vm((rows, n * SLOT), F32),
        dma((len(args),)), dma((PHASES,)), dma((PHASES, n)), dma((2,)), dma((3,)), dma,
    ]
    any_space = pl.BlockSpec(memory_space=pl.ANY)
    out, new_matrix, new_norm, new_max = pl.pallas_call(
        functools.partial(layer_kernel, n),
        out_shape=(
            jax.ShapeDtypeStruct((rows, width), BF16),
            jax.ShapeDtypeStruct((rows, head, head), F32),
            jax.ShapeDtypeStruct((rows, head), F32),
            jax.ShapeDtypeStruct((1, rows), F32),
        ),
        in_specs=[any_space] * len(args),
        out_specs=[any_space] * 4,
        scratch_shapes=scratch,
        compiler_params=pltpu.CompilerParams(
            collective_id=0, has_side_effects=True, vmem_limit_bytes=56 * 1024 * 1024),
        name="layer",
    )(*args)
    return (out, new_matrix.reshape(rows, 1, head, head), new_norm.reshape(rows, 1, head), new_max.T)


def solution(mesh):
    n = mesh.shape["ep"]
    in_specs = (
        P("ep", None),
        P("ep", "tp", None, None),
        P("ep", "tp", None),
        P("ep", "tp"),
        P(),
        P("ep", "tp"),
        P("ep", "tp"),
        P("ep", "tp"),
        P("ep", "tp"),
        P(),
        P(),
        P(),
        P("tp", "ep"),
        P(),
        P(),
        P("ep", None),
        P("ep", None),
        P("ep", None, "tp"),
        P("ep", None, "tp"),
        P("ep", "tp", None),
        P("ep", "tp"),
        P("ep", "tp"),
        P("tp", "ep"),
    )
    out_specs = (P("ep", None), P("ep", "tp", None, None), P("ep", "tp", None), P("ep", "tp"))
    return jax.shard_map(
        functools.partial(on_device, n), mesh=mesh, in_specs=in_specs, out_specs=out_specs,
        check_vma=False)
```

time: 340 us -> 127 us (0.37)
  waiting for transfers between devices: 173 us -> 0 us
  Pallas kernels: 0 us -> 119 us
  blocking collectives: 53.1 us -> 0 us
  starting transfers between devices: 37.5 us -> 0 us
  matrix products: 20.7 us -> 0 us
  local copies, waits for them, and re-layouts: 26 us -> 7.26 us
  between operations: 14.5 us -> 0.64 us
  other arithmetic: 13.4 us -> 0 us
    pallas_call x0 -> x1, Pallas kernels: none -> 119 us  [on_device(): pl.pallas_call(functools.partial(layer_kernel, n), out_shape=(jax.ShapeDt...]
    all_gather x2 -> x0, waiting for transfers between devices: 113 us -> none  [the longest x1 56.4 us: total_of_pieces(): return lax.all_gather(shard, axis).sum(0)]
    all_to_all x7 -> x0, waiting for transfers between devices: 60.3 us -> none  [the longest x3 31 us: sum_at_owner(): lax.all_to_all(parts, axis, split_axis=0, concat_axis=0, tiled=True)]
    all_to_all x4 -> x0, blocking collectives: 53.1 us -> none  [the longest x2 26 us: from_everyone(): lax.all_to_all(jnp.broadcast_to(shard[None], (devices, *shard.shape)), ax...]
    all_to_all x7 -> x0, starting transfers between devices: 37.4 us -> none  [the longest x3 17.3 us: sum_at_owner(): lax.all_to_all(parts, axis, split_axis=0, concat_axis=0, tiled=True)]
    dot_general x14 -> x0, matrix products: 20.7 us -> none  [the longest x4 7.05 us: on_device(): jnp.dot(normed, shard_w, preferred_element_type=jnp.float32)]
    scatter x2 -> x0, local copies, waits for them, and re-layouts: 14.8 us -> none  [on_device(): outbound = jnp.zeros((experts_all, capacity, model_width), jnp.bfloat16)....]
    reduce_sum x9 -> x0, other arithmetic: 7.08 us -> none  [the longest x1 3.83 us: total_of_pieces(): return lax.all_gather(shard, axis).sum(0)]
  transfers between devices with their start and end apart: 9 -> 0, of which waited for: 8 -> 0; matrix products, arithmetic and copies ran while one was open for 11% -> 0% of each run, Pallas kernels for 0% -> 0%
where the time goes in v1:
time: 127 us
  Pallas kernels  119 us (94%)
  local copies, waits for them, and re-layouts  7.26 us (6%)
    pallas_call x1, Pallas kernels, on_device(): pl.pallas_call(functools.partial(layer_kernel, n), out_shape=(jax.ShapeDt...  119 us
    unnamed x8, local copies, waits for them, and re-layouts  5.94 us

profile of v1, /device:TPU:1, one launch (start us, length us, event | category | flops | bytes accessed | tf_op | source)
XLA Modules:
  0.0 126.8 jit_solution(14024352777227147519)
XLA Ops:
  0.6 1.3 %reshape.46.wbr_h = bf16[1,4096]{1,0:T(2,128)(2,1)} reshape(bf16[4096]{0:T(1024)(128)(2,1)} %param.37) | data formatting | bytes 16384 | tf_op jit(solution)/shard_map/reshape | solution.py:448
  1.9 118.9 %layer.1 = (bf16[32,4096]{1,0:T(8,128)(2,1)}, f32[32,128,128]{2,1,0:T(8,128)}, f32[32,128]{1,0:T(8,128)}, f32[1,32]{1,0:T(1,128)}) custom-call(bf16[32,4096]{1,0:T(8,128)(2,1)} %tok_h.1, f32[32,128,128]{2,1,0:T(8,128)} %bitcast.21, f32[32,128]{1,0:T(8,128)} %bitcast.27, f32[1,32]{1,0:T(1,128)} %bitcast.33, f32[1,4096]{1,0:T(1,128)} %bitcast.28, ...), custom_call_target="tpu_custom_call" | custom-call | tf_op jit(solution)/shard_map/layer/pallas_call | solution.py:480
  120.9 1.7 %copy.33 = bf16[32,4096]{1,0:T(8,128)(2,1)} copy(bf16[32,4096]{1,0:T(8,128)(2,1)} %get-tuple-element.20) | data formatting | bytes 524288
  122.6 0.0 copy-start
  122.6 0.0 copy-start.1
  122.6 3.1 %copy.34 = f32[32,1,128,128]{3,2,1,0:T(8,128)} copy(f32[32,1,128,128]{3,2,1,0:T(8,128)} %bitcast.20) | data formatting | bytes 4194304
  125.7 0.0 copy-done
  125.7 0.6 copy.35
  126.3 0.0 copy-done.1
  126.3 0.5 copy.36
Async XLA Ops:
  122.6 3.2 %copy-start = (f32[32,128]{1,0:T(8,128)S(1)}, f32[32,128]{1,0:T(8,128)}, u32[]{:S(2)}) copy-start(f32[32,128]{1,0:T(8,128)} %get-tuple-element.10) | copy-start | bytes 49156
  122.6 3.8 %copy-start.1 = (f32[1,32]{1,0:T(1,128)S(1)}, f32[1,32]{1,0:T(1,128)}, u32[]{:S(2)}) copy-start(f32[1,32]{1,0:T(1,128)} %get-tuple-element.11) | copy-start | bytes 388

commit v2 on v1

--- a/solution.py
+++ b/solution.py
@@ -32,8 +32,9 @@
     return jnp.sum(jnp.where(diag, column, 0.0), axis=0, keepdims=True)
 
 
-TOK, KEY, QKV, MIX, PRJ, RES, ROW, STA, DEN, HID, DWN, EXP, RET, OUT = range(14)
-PHASES = 14
+(TOK, KEY, QKV, MIX, PRJ_PAIR, PRJ, RES, ROW, STA, DEN, HID, DWN_PAIR, DWN, EXP_PAIR, EXP, RET,
+ OUT) = range(17)
+PHASES = 17
 
 
 def layer_kernel(
@@ -43,13 +44,17 @@
     out_h, nm_h, nn_h, nmax_h,
     tok, sm, sn, smax, mgain, wqkv, wgates, fbias, wproj, fgain, wbr, routes, rw,
     eg, eu, ed, dgu, dd,
-    tok_all, key_all, qkv_part, qkv_in, mix_all, prj_part, prj_in, res_all,
-    row_out, row_in, sta_out, sta_in, den_part, den_in, hid_all, dwn_part, dwn_in,
-    exp_part, exp_in, ret_out, ret_in, fin_out, fin_in, out_own,
-    nm, nn, nmax, pick, gu_acc, gates, wkt, qt, vrow, keep_rows, numer, ret_w,
-    load_sem, send_sem, recv_sem, fin_sem, store_sem, out_sem,
+    tok_all, key_all, qkv_part, qkv_in, mix_all, prj_part, prj_pair, prj_sum, prj_in, res_all,
+    row_out, row_in, sta_out, sta_in, den_part, den_in, hid_all, dwn_part, dwn_pair, dwn_sum, dwn_in,
+    exp_part, exp_pair, exp_sum, exp_in, ret_out, ret_in, ret_w_in, out_own, out_all,
+    wbr_wide, nm, nn, nmax, pick, gu_acc, gates, wkt, qt, vrow, keep_rows, numer, ret_w,
+    load_sem, send_sem, recv_sem, share_sem, store_sem, out_sem,
 ):
     me_e, me_t = lax.axis_index("ep"), lax.axis_index("tp")
+    chips = n // 2
+    me_z, core = lax.div(me_t, 2), lax.rem(me_t, 2)
+    partner = me_t + 1 - 2 * core
+    owned = lax.rem(me_t - me_e + n, n)
     rows = tok.shape[0]
     width = tok.shape[1]
     block = width // n
@@ -57,6 +62,7 @@
     hid_e = eg.shape[1]
     hid_d = dd.shape[0]
     cap_rows = CAP * n
+    half_rows = cap_rows // 2
 
     loads = [
         (tok_h, tok), (mgain_h, mgain), (fgain_h, fgain), (wbr_h, wbr), (routes_h, routes),
@@ -79,18 +85,7 @@
         return 0
 
     lax.fori_loop(1, n, greet, 0)
-
-    @pl.when(me_e != me_t)
-    def _():
-        pl.semaphore_signal(barrier, 1, device_id=(me_t, me_e), device_id_type=MESH)
-
-    @pl.when(me_e != me_t)
-    def _():
-        pl.semaphore_wait(barrier, 2 * n - 1)
-
-    @pl.when(me_e == me_t)
-    def _():
-        pl.semaphore_wait(barrier, 2 * n - 2)
+    pl.semaphore_wait(barrier, 2 * n - 2)
 
     def ep_copy(phase, src, dst, peer, landing):
         return pltpu.make_async_remote_copy(
@@ -101,6 +96,73 @@
         return pltpu.make_async_remote_copy(
             src_ref=src, dst_ref=dst, send_sem=send_sem.at[phase],
             recv_sem=recv_sem.at[phase, landing], device_id=(me_e, peer), device_id_type=MESH)
+
+    def over(peer_e, peer_t, phase, src, dst, landing):
+        return pltpu.make_async_remote_copy(
+            src_ref=src, dst_ref=dst, send_sem=send_sem.at[phase],
+            recv_sem=recv_sem.at[phase, landing], device_id=(peer_e, peer_t), device_id_type=MESH)
+
+    def chip(k):
+        k = chips - k
+        return lax.rem(me_z + chips + lax.div(k + 1, 2) * (2 * lax.rem(k, 2) - 1), chips)
+
+    def sum_over_tp(pair_phase, phase, part, place, pair, summed, arrived):
+        def give(k, _):
+            z = lax.rem(me_z + k, chips)
+            tp_copy(pair_phase, part.at[place(2 * z + 1 - core)], pair.at[z], partner, z).start()
+            return 0
+
+        lax.fori_loop(1, chips + 1, give, 0)
+
+        def add(z):
+            tp_copy(pair_phase, pair.at[z], pair.at[z], partner, z).wait_recv()
+            return part[place(2 * z + core)].astype(F32) + pair[z].astype(F32)
+
+        def pass_on(k, _):
+            z = chip(k)
+            summed[z] = add(z).astype(BF16)
+            tp_copy(phase, summed.at[z], arrived.at[me_z], 2 * z + core, me_z).start()
+            return 0
+
+        lax.fori_loop(1, chips, pass_on, 0)
+        return add(me_z)
+
+    def summed_over_tp(phase, arrived, acc):
+        def one(k, acc):
+            z = chip(chips - k)
+            tp_copy(phase, arrived.at[z], arrived.at[z], 2 * z + core, z).wait_recv()
+            return acc + arrived[z].astype(F32)
+
+        return lax.fori_loop(1, chips, one, acc)
+
+    def gather_over_tp(phase, blocks, place):
+        mine = blocks.at[place(me_t)]
+        tp_copy(phase, mine, mine, partner, place(me_t)).start()
+
+        def give(k, _):
+            tp_copy(phase, mine, mine, 2 * chip(k) + core, place(me_t)).start()
+            return 0
+
+        lax.fori_loop(1, chips, give, 0)
+
+        def pass_on(k, _):
+            z = chip(chips - k)
+            block = blocks.at[place(2 * z + core)]
+            tp_copy(phase, block, block, 2 * z + core, place(2 * z + core)).wait_recv()
+            tp_copy(phase, block, block, partner, place(2 * z + core)).start()
+            return 0
+
+        lax.fori_loop(1, chips, pass_on, 0)
+
+        def take(z, _):
+            at = place(2 * z + 1 - core)
+            tp_copy(phase, blocks.at[at], blocks.at[at], partner, at).wait_recv()
+            return 0
+
+        lax.fori_loop(0, chips, take, 0)
+
+    def row_place(t):
+        return lax.rem(t - me_e + n, n)
 
     def to_peers(copy, me, phase, src_of, dst):
         def one(d, _):
@@ -149,6 +211,19 @@
         hit = (spots.astype(F32) == r.astype(F32) * SLOT + slot)
         share_t = share_t + jnp.where(hit, w / total, 0.0)
     ret_w[...] = lax.dot_general(eye, share_t, NT, precision=HIGHEST, preferred_element_type=F32)
+
+    def shares():
+        return pltpu.make_async_remote_copy(
+            src_ref=ret_w, dst_ref=ret_w_in, send_sem=share_sem.at[0], recv_sem=share_sem.at[1],
+            device_id=(owned, me_t), device_id_type=MESH)
+
+    @pl.when(owned != me_e)
+    def _():
+        shares().start()
+
+    @pl.when(owned == me_e)
+    def _():
+        ret_w_in[...] = ret_w[...]
 
     loads[1].wait()
     squares = jnp.zeros((rows, block), F32)
@@ -240,51 +315,57 @@
     key_t = lax.dot_general(
         jnp.where(iota((n, 128), 0) == iota((n, 128), 1), 1.0, 0.0).astype(BF16),
         key_all[...].reshape(n * rows, 128), NT, preferred_element_type=F32)
-    places = iota((cap_rows, n * rows), 0).astype(F32)
+    places = (iota((half_rows, n * rows), 0) + core * half_rows).astype(F32)
     for e in range(n):
-        pick[pl.ds(e * cap_rows, cap_rows), :] = jnp.where(
+        pick[pl.ds(e * half_rows, half_rows), :] = jnp.where(
             places == key_t[e:e + 1, :], 1.0, 0.0).astype(BF16)
 
     await_peers(ep_copy, me_e, MIX, mix_all)
     loads[16].wait()
     y = jnp.dot(mix_all[...].reshape(n * rows, head), wproj[...], preferred_element_type=F32)
     prj_part[...] = y.astype(BF16).reshape(n, rows, block)
-    to_peers(tp_copy, me_t, PRJ, lambda peer: prj_part.at[peer], prj_in.at[me_t])
-    mixed = await_peers(tp_copy, me_t, PRJ, prj_in,
-                        lambda peer, acc: acc + prj_in[peer].astype(F32),
-                        prj_part[me_t].astype(F32))
-    residual = (tok_all[me_t].astype(F32) + mixed).astype(BF16)
-    res_all[me_t] = residual
-    to_peers(tp_copy, me_t, RES, lambda peer: res_all.at[me_t], res_all.at[me_t])
+    mixed = sum_over_tp(PRJ_PAIR, PRJ, prj_part, row_place, prj_pair, prj_sum, prj_in)
+    mixed = summed_over_tp(PRJ, prj_in, mixed)
+    residual = (tok_all[owned].astype(F32) + mixed).astype(BF16)
+    res_all[owned] = residual
+    gather_over_tp(RES, res_all, row_place)
     loads[2].wait()
     loads[3].wait()
-    await_peers(tp_copy, me_t, RES, res_all)
+
+    def pass_rows(peer):
+        spot = core * n + peer
+        tp_copy(ROW, row_in.at[spot], row_in.at[spot], partner, spot).start()
 
     res_flat = res_all[...].reshape(n * rows, block)
 
     def dispatch(c, _):
         at = pl.multiple_of(c * group, group)
-        y = jnp.dot(pick[pl.ds(pl.multiple_of(at * cap_rows, group * cap_rows), group * cap_rows), :],
+        y = jnp.dot(pick[pl.ds(pl.multiple_of(at * half_rows, group * half_rows), group * half_rows), :],
                     res_flat, preferred_element_type=F32)
-        row_out[pl.ds(at, group)] = y.astype(BF16).reshape(group, cap_rows, block)
+        row_out[pl.ds(at, group)] = y.astype(BF16).reshape(group, half_rows, block)
 
         def one(k, _):
             peer = at + k
 
             @pl.when(peer != me_e)
             def _():
-                ep_copy(ROW, row_out.at[peer], row_in.at[me_e], peer, me_e).start()
+                spot = core * n + me_e
+                ep_copy(ROW, row_out.at[peer], row_in.at[spot], peer, spot).start()
 
             return 0
 
         return lax.fori_loop(0, group, one, 0)
 
     lax.fori_loop(0, n // group, dispatch, 0)
-    row_in[me_e] = row_out[me_e]
+    row_in[core * n + me_e] = row_out[me_e]
+    pass_rows(me_e)
 
     mine = pl.multiple_of(me_e * block, block)
     gain_f = fgain[:, pl.ds(mine, block)]
-    gain_b = gain_f * wbr[:, pl.ds(mine, block)].astype(F32)
+    wbr_wide[...] = wbr[...].astype(F32)
+    lines = block // 128
+    gain_b = gain_f * jnp.concatenate(
+        [wbr_wide[pl.ds(me_e * lines + k, 1), :] for k in range(lines)], axis=1)
 
     def stats(b, _):
         r = res_all[b].astype(F32)
@@ -321,16 +402,25 @@
     loads[20].wait()
 
     def expert_in(peer, ss):
-        x = row_in[peer].astype(F32)
+        other = (1 - core) * n + peer
+        tp_copy(ROW, row_in.at[other], row_in.at[other], partner, other).wait_recv()
+        x = jnp.concatenate([row_in[peer], row_in[n + peer]], axis=0).astype(F32)
         at = pl.multiple_of(peer * block, block)
         xg = (x * fgain[:, pl.ds(at, block)]).astype(BF16)
         gu_acc[:, pl.ds(0, hid_e)] += jnp.dot(xg, eg[pl.ds(at, block), :], preferred_element_type=F32)
         gu_acc[:, pl.ds(hid_e, hid_e)] += jnp.dot(xg, eu[pl.ds(at, block), :], preferred_element_type=F32)
         return ss + jnp.sum(x * x, axis=1, keepdims=True)
 
+    def expert_next(d, ss):
+        peer = lax.rem(me_e + n - d, n)
+        spot = core * n + peer
+        ep_copy(ROW, row_in.at[spot], row_in.at[spot], peer, spot).wait_recv()
+        pass_rows(peer)
+        return expert_in(lax.rem(peer + 1, n), ss)
+
     gu_acc[...] = jnp.zeros_like(gu_acc)
-    ss = expert_in(me_e, jnp.zeros((cap_rows, 1), F32))
-    ss = await_peers(ep_copy, me_e, ROW, row_in, expert_in, ss)
+    ss = lax.fori_loop(1, n, expert_next, jnp.zeros((cap_rows, 1), F32))
+    ss = expert_in(lax.rem(me_e + 1, n), ss)
     row_scale = lax.rsqrt(ss / width + EPS)
     g = gu_acc[:, :hid_e] * row_scale
     u = gu_acc[:, hid_e:] * row_scale
@@ -339,7 +429,7 @@
     for k in range(n):
         exp_part[k] = jnp.dot(hidden, ed[:, k * block:(k + 1) * block],
                               preferred_element_type=F32).astype(BF16)
-    to_peers(tp_copy, me_t, EXP, lambda peer: exp_part.at[peer], exp_in.at[me_t])
+    routed_sum = sum_over_tp(EXP_PAIR, EXP, exp_part, row_place, exp_pair, exp_sum, exp_in)
 
     sums = await_peers(ep_copy, me_e, STA, sta_in, lambda peer, acc: acc + sta_in[peer], sta_out[me_e])
     dense_scale = lax.rsqrt(to_column(sums[0:1, :], rows) / width + EPS)
@@ -351,60 +441,103 @@
     hid_all[me_e] = (g / (1.0 + jnp.exp(-g)) * u * branch).astype(BF16)
     to_peers(ep_copy, me_e, HID, lambda peer: hid_all.at[me_e], hid_all.at[me_e])
 
-    y = await_peers(tp_copy, me_t, EXP, exp_in,
-                    lambda peer, acc: acc + exp_in[peer].astype(F32),
-                    exp_part[me_t].astype(F32))
+    y = summed_over_tp(EXP, exp_in, routed_sum)
     spot, col = iota((n * SLOT, cap_rows), 0), iota((n * SLOT, cap_rows), 1)
     within = jnp.bitwise_and(spot, SLOT - 1)
     source = CAP * jnp.right_shift(spot, SLOT.bit_length() - 1) + within
     spread = jnp.where((source == col) & (within < CAP), 1.0, 0.0).astype(BF16)
     ret_out[...] = jnp.dot(spread, y.astype(BF16), preferred_element_type=F32).reshape(n, SLOT, block)
-    to_peers(ep_copy, me_e, RET, lambda peer: ret_out.at[peer], ret_in.at[me_e])
-    ret_in[me_e] = ret_out[me_e]
+
+    def give_back(i, _):
+        place = lax.rem(i + owned, n)
+        own = (owned == me_e) & (place == me_t)
+
+        @pl.when(jnp.logical_not(own))
+        def _():
+            over(owned, place, RET, ret_out.at[i], ret_in.at[me_e], me_e).start()
+
+        @pl.when(own)
+        def _():
+            ret_in[me_e] = ret_out[i]
+
+        return 0
+
+    lax.fori_loop(0, n, give_back, 0)
 
     await_peers(ep_copy, me_e, HID, hid_all)
     loads[22].wait()
     y = jnp.dot(hid_all[...].reshape(n * rows, hid_d), dd[...], preferred_element_type=F32)
     dwn_part[...] = y.astype(BF16).reshape(n, rows, block)
-    to_peers(tp_copy, me_t, DWN, lambda peer: dwn_part.at[peer], dwn_in.at[me_t])
-
-    await_peers(ep_copy, me_e, RET, ret_in)
-    routed = jnp.dot(ret_w[...], ret_in[...].reshape(n * SLOT, block), precision=HIGHEST,
+    dense_sum = sum_over_tp(DWN_PAIR, DWN, dwn_part, row_place, dwn_pair, dwn_sum, dwn_in)
+
+    def returned(e, _):
+        source = lax.rem(e + me_e, n)
+
+        @pl.when((e != me_e) | (source != me_t))
+        def _():
+            over(e, source, RET, ret_in.at[e], ret_in.at[e], e).wait_recv()
+
+        return 0
+
+    lax.fori_loop(0, n, returned, 0)
+
+    @pl.when(owned != me_e)
+    def _():
+        shares().wait()
+
+    routed = jnp.dot(ret_w_in[...], ret_in[...].reshape(n * SLOT, block), precision=HIGHEST,
                      preferred_element_type=F32)
-
-    y = await_peers(tp_copy, me_t, DWN, dwn_in,
-                    lambda peer, acc: acc + dwn_in[peer].astype(F32),
-                    dwn_part[me_t].astype(F32))
-    fin_out[...] = res_all[me_t].astype(F32) + y
-
-    def crossing():
-        return pltpu.make_async_remote_copy(
-            src_ref=fin_out, dst_ref=fin_in, send_sem=fin_sem.at[0], recv_sem=fin_sem.at[1],
-            device_id=(me_t, me_e), device_id_type=MESH)
-
-    @pl.when(me_e != me_t)
+    known = res_all[owned].astype(F32) + routed
+
+    y = summed_over_tp(DWN, dwn_in, dense_sum)
+    out_own[...] = (known + y).astype(BF16)
+
+    def publish(k, _):
+        z = chip(k)
+        over(owned, 2 * z + core, OUT, out_own, out_all.at[me_e], me_e).start()
+        return 0
+
+    lax.fori_loop(1, chips, publish, 0)
+
+    @pl.when(owned != me_e)
     def _():
-        crossing().start()
-        crossing().wait()
-
-    @pl.when(me_e == me_t)
+        over(owned, me_t, OUT, out_own, out_all.at[me_e], me_e).start()
+
+    @pl.when(owned == me_e)
     def _():
-        fin_in[...] = fin_out[...]
-
-    out_own[...] = (fin_in[...] + routed).astype(BF16)
-    place = out_h.at[:, pl.ds(pl.multiple_of(me_t * block, block), block)]
-    to_peers(tp_copy, me_t, OUT, lambda peer: out_own, place)
-    own = pltpu.make_async_copy(out_own, place, out_sem)
-    own.start()
-
-    def landed(d, _):
-        peer = lax.rem(me_t + n - d, n)
-        spot = out_h.at[:, pl.ds(pl.multiple_of(peer * block, block), block)]
-        tp_copy(OUT, out_own, spot, peer, peer).wait_recv()
-        return 0
-
-    lax.fori_loop(1, n, landed, 0)
-    own.wait()
+        out_all[me_e] = out_own[...]
+
+    def write(j, where):
+        return pltpu.make_async_copy(
+            out_all.at[j], out_h.at[:, pl.ds(pl.multiple_of(j * block, block), block)], out_sem.at[where])
+
+    def forward(k, _):
+        j = lax.rem(2 * k + lax.rem(me_e + core, 2), n)
+        source = lax.rem(me_e + j, n)
+
+        @pl.when((j != me_e) | (source != me_t))
+        def _():
+            over(j, source, OUT, out_all.at[j], out_all.at[j], j).wait_recv()
+
+        over(me_e, partner, OUT, out_all.at[j], out_all.at[j], j).start()
+        write(j, j).start()
+        return 0
+
+    lax.fori_loop(0, chips, forward, 0)
+
+    def finish(k, _):
+        j = lax.rem(2 * k + lax.rem(me_e + core + 1, 2), n)
+        over(me_e, partner, OUT, out_all.at[j], out_all.at[j], j).wait_recv()
+        write(j, j).start()
+        return 0
+
+    lax.fori_loop(0, chips, finish, 0)
+
+    def written_out(j, _):
+        write(j, j).wait()
+        return 0
+
+    lax.fori_loop(0, n, written_out, 0)
     for copy in stores:
         copy.wait()
     rest = pl.ds(0, n - 1)
@@ -412,16 +545,28 @@
     sent(ep_copy, KEY, key_all.at[rest])
     sent(ep_copy, QKV, qkv_part.at[rest])
     sent(ep_copy, MIX, mix_all.at[rest])
-    sent(tp_copy, PRJ, prj_part.at[rest])
+    some = pl.ds(0, chips - 1)
+    sent(tp_copy, PRJ_PAIR, prj_pair)
+    sent(tp_copy, PRJ, prj_sum.at[some])
     sent(tp_copy, RES, res_all.at[rest])
-    sent(ep_copy, ROW, row_out.at[rest])
+    sent(ep_copy, ROW, row_in.at[pl.ds(0, 2 * n - 1)])
     sent(ep_copy, STA, sta_out.at[rest])
     sent(ep_copy, DEN, den_part.at[rest])
     sent(ep_copy, HID, hid_all.at[rest])
-    sent(tp_copy, DWN, dwn_part.at[rest])
-    sent(tp_copy, EXP, exp_part.at[rest])
-    sent(ep_copy, RET, ret_out.at[rest])
-    sent(tp_copy, OUT, res_all.at[rest])
+    sent(tp_copy, EXP_PAIR, exp_pair)
+    sent(tp_copy, EXP, exp_sum.at[some])
+    sent(tp_copy, DWN_PAIR, dwn_pair)
+    sent(tp_copy, DWN, dwn_sum.at[some])
+
+    @pl.when(owned != me_e)
+    def _():
+        sent(ep_copy, RET, ret_out)
+        sent(ep_copy, OUT, out_all)
+
+    @pl.when(owned == me_e)
+    def _():
+        sent(ep_copy, RET, ret_out.at[rest])
+        sent(ep_copy, OUT, out_all.at[rest])
 
 
 def on_device(
@@ -445,7 +590,7 @@
         forget_bias.reshape(1, n),
         w_proj,
         ffn_gain.reshape(1, width),
-        w_branch.reshape(1, width),
+        w_branch.reshape(width // 128, 128),
         routes.T, route_weight.T,
         expert_gate.reshape(width, hid_e), expert_up.reshape(width, hid_e),
         expert_down.reshape(hid_e, width),
@@ -453,28 +598,31 @@
     )
     vm = pltpu.VMEM
     dma = pltpu.SemaphoreType.DMA
+    half_rows = cap_rows // 2
+
+    def hier(tall):
+        return [vm((n, tall, block), BF16)] + [vm((n // 2, tall, block), BF16)] * 3
+
     scratch = [
         vm((rows, width), BF16), vm((rows, head, head), F32), vm((rows, head), F32), vm((1, rows), F32),
         vm((1, width), F32), vm((block, 4 * head), BF16), vm((2 * n, width), BF16), vm((1, n), F32),
-        vm((head, block), BF16), vm((1, width), F32), vm((1, width), BF16), vm((2, rows), jnp.int32),
+        vm((head, block), BF16), vm((1, width), F32), vm((width // 128, 128), BF16), vm((2, rows), jnp.int32),
         vm((2, rows), F32), vm((width, hid_e), BF16), vm((width, hid_e), BF16), vm((hid_e, width), BF16),
         vm((block, 2 * hid_d), BF16), vm((hid_d, block), BF16),
         vm((n, rows, block), BF16), vm((n, rows, 128), BF16),
         vm((n, rows, 4 * head), BF16), vm((n, rows, 4 * head), BF16),
-        vm((n, rows, head), BF16), vm((n, rows, block), BF16), vm((n, rows, block), BF16),
-        vm((n, rows, block), BF16),
-        vm((n, cap_rows, block), BF16), vm((n, cap_rows, block), BF16),
+        vm((n, rows, head), BF16), *hier(rows), vm((n, rows, block), BF16),
+        vm((n, half_rows, block), BF16), vm((2 * n, half_rows, block), BF16),
         vm((n, 8, 128), F32), vm((n, 8, 128), F32),
         vm((n, rows, 2 * hid_d), BF16), vm((n, rows, 2 * hid_d), BF16),
-        vm((n, rows, hid_d), BF16), vm((n, rows, block), BF16), vm((n, rows, block), BF16),
-        vm((n, cap_rows, block), BF16), vm((n, cap_rows, block), BF16),
-        vm((n, SLOT, block), F32), vm((n, SLOT, block), F32),
-        vm((rows, block), F32), vm((rows, block), F32), vm((rows, block), BF16),
-        vm((rows, head, head), F32), vm((rows, head), F32), vm((1, rows), F32),
-        vm((n * cap_rows, n * rows), BF16), vm((cap_rows, 2 * hid_e), F32), vm((rows, 2 * n), F32),
+        vm((n, rows, hid_d), BF16), *hier(rows), *hier(cap_rows),
+        vm((n, SLOT, block), F32), vm((n, SLOT, block), F32), vm((rows, n * SLOT), F32),
+        vm((rows, block), BF16), vm((n, rows, block), BF16),
+        vm((width // 128, 128), F32), vm((rows, head, head), F32), vm((rows, head), F32), vm((1, rows), F32),
+        vm((n * half_rows, n * rows), BF16), vm((cap_rows, 2 * hid_e), F32), vm((rows, 2 * n), F32),
         vm((head, rows), F32), vm((head, rows), F32), vm((rows, head), F32), vm((rows, head), F32),
         vm((rows, head), F32), vm((rows, n * SLOT), F32),
-        dma((len(args),)), dma((PHASES,)), dma((PHASES, n)), dma((2,)), dma((3,)), dma,
+        dma((len(args),)), dma((PHASES,)), dma((PHASES, 2 * n)), dma((2,)), dma((3,)), dma((n,)),
     ]
     any_space = pl.BlockSpec(memory_space=pl.ANY)
     out, new_matrix, new_norm, new_max = pl.pallas_call(

time: 127 us -> 107 us (0.84)
  Pallas kernels: 119 us -> 100 us
  local copies, waits for them, and re-layouts: 7.26 us -> 5.94 us
    pallas_call x1, Pallas kernels: 119 us -> 100 us  [on_device(): pl.pallas_call(functools.partial(layer_kernel, n), out_shape=(jax.ShapeDt...]
    reshape x1 -> x0, local copies, waits for them, and re-layouts: 1.31 us -> none  [on_device(): w_branch.reshape(1, width)]
where the time goes in v2:
time: 107 us
  Pallas kernels  100 us (93%)
  local copies, waits for them, and re-layouts  5.94 us (6%)
    pallas_call x1, Pallas kernels, on_device(): pl.pallas_call(functools.partial(layer_kernel, n), out_shape=(jax.ShapeDt...  100 us
    unnamed x8, local copies, waits for them, and re-layouts  5.94 us

profile of v2, /device:TPU:1, one launch (start us, length us, event | category | flops | bytes accessed | tf_op | source)
XLA Modules:
  0.0 106.8 jit_solution(11773231231283051282)
XLA Ops:
  0.6 100.2 %layer.1 = (bf16[32,4096]{1,0:T(8,128)(2,1)}, f32[32,128,128]{2,1,0:T(8,128)}, f32[32,128]{1,0:T(8,128)}, f32[1,32]{1,0:T(1,128)}) custom-call(bf16[32,4096]{1,0:T(8,128)(2,1)} %tok_h.1, f32[32,128,128]{2,1,0:T(8,128)} %bitcast.21, f32[32,128]{1,0:T(8,128)} %bitcast.28, f32[1,32]{1,0:T(1,128)} %bitcast.35, f32[1,4096]{1,0:T(1,128)} %bitcast.29, ...), custom_call_target="tpu_custom_call" | custom-call | tf_op jit(solution)/shard_map/layer/pallas_call | solution.py:628
  100.9 1.7 %copy.33 = bf16[32,4096]{1,0:T(8,128)(2,1)} copy(bf16[32,4096]{1,0:T(8,128)(2,1)} %get-tuple-element.20) | data formatting | bytes 524288
  102.5 0.0 copy-start
  102.5 0.0 copy-start.1
  102.5 3.1 %copy.34 = f32[32,1,128,128]{3,2,1,0:T(8,128)} copy(f32[32,1,128,128]{3,2,1,0:T(8,128)} %bitcast.25) | data formatting | bytes 4194304
  105.7 0.0 copy-done
  105.7 0.6 copy.35
  106.3 0.0 copy-done.1
  106.3 0.5 copy.36
Async XLA Ops:
  102.5 3.2 %copy-start = (f32[32,128]{1,0:T(8,128)S(1)}, f32[32,128]{1,0:T(8,128)}, u32[]{:S(2)}) copy-start(f32[32,128]{1,0:T(8,128)} %get-tuple-element.10) | copy-start | bytes 49156
  102.5 3.8 %copy-start.1 = (f32[1,32]{1,0:T(1,128)S(1)}, f32[1,32]{1,0:T(1,128)}, u32[]{:S(2)}) copy-start(f32[1,32]{1,0:T(1,128)} %get-tuple-element.11) | copy-start | bytes 388

commit v3 on v2

--- a/solution.py
+++ b/solution.py
@@ -1,4 +1,5 @@
 import functools
+import math
 
 import jax
 import jax.numpy as jnp
@@ -33,36 +34,43 @@
 
 
 (TOK, KEY, QKV, MIX, PRJ_PAIR, PRJ, RES, ROW, STA, DEN, HID, DWN_PAIR, DWN, EXP_PAIR, EXP, RET,
- OUT) = range(17)
-PHASES = 17
+ OUT, NEAR, FAR, NEAR_DOWN, FAR_DOWN) = range(21)
+PHASES = 21
+EARLY = 96
 
 
 def layer_kernel(
     n,
     tok_h, sm_h, sn_h, smax_h, mgain_h, wq_h, wk_h, wv_h, wo_h, win_h, wfo_h, fbias_h,
     wproj_h, fgain_h, wbr_h, routes_h, rw_h, eg_h, eu_h, ed_h, dg_h, du_h, dd_h,
-    out_h, nm_h, nn_h, nmax_h,
+    out, nm, nn, nmax,
     tok, sm, sn, smax, mgain, wqkv, wgates, fbias, wproj, fgain, wbr, routes, rw,
-    eg, eu, ed, dgu, dd,
-    tok_all, key_all, qkv_part, qkv_in, mix_all, prj_part, prj_pair, prj_sum, prj_in, res_all,
+    eg, eu, ed, dgu_all, dd_all,
+    tok_all, key_all, qkv_part, qkv_in, mix_all, prj_part, prj_pair, prj_sum, prj_in, res_own, res_all, res_fin,
     row_out, row_in, sta_out, sta_in, den_part, den_in, hid_all, dwn_part, dwn_pair, dwn_sum, dwn_in,
-    exp_part, exp_pair, exp_sum, exp_in, ret_out, ret_in, ret_w_in, out_own, out_all,
-    wbr_wide, nm, nn, nmax, pick, gu_acc, gates, wkt, qt, vrow, keep_rows, numer, ret_w,
-    load_sem, send_sem, recv_sem, share_sem, store_sem, out_sem,
+    exp_part, exp_pair, exp_sum, exp_in, ret_out, ret_in, ret_w_in, out_own,
+    wbr_wide, pick, x_cat, gu_acc, gates, wkt, qt, vrow, keep_rows, numer, ret_w,
+    load_sem, send_sem, recv_sem, share_sem, res_sem,
 ):
     me_e, me_t = lax.axis_index("ep"), lax.axis_index("tp")
     chips = n // 2
+    side = math.isqrt(n)
+    me_y, me_x = lax.div(me_e, side), lax.rem(me_e, side)
     me_z, core = lax.div(me_t, 2), lax.rem(me_t, 2)
     partner = me_t + 1 - 2 * core
     owned = lax.rem(me_t - me_e + n, n)
+    final_rows = side * me_y + lax.rem(owned, side)
+    final_cols = side * lax.div(owned, side) + me_x
     rows = tok.shape[0]
     width = tok.shape[1]
     block = width // n
     head = sn.shape[1]
     hid_e = eg.shape[1]
-    hid_d = dd.shape[0]
+    hid_d = dd_all.shape[1]
+    quarter = rows * side
     cap_rows = CAP * n
-    half_rows = cap_rows // 2
+    few_rows = CAP * side
+    dgu, dd = dgu_all.at[me_x], dd_all.at[me_y]
 
     loads = [
         (tok_h, tok), (mgain_h, mgain), (fgain_h, fgain), (wbr_h, wbr), (routes_h, routes),
@@ -70,8 +78,8 @@
         (fbias_h, fbias), (smax_h, smax), (sn_h, sn),
         (wq_h, wqkv.at[:, pl.ds(0, head)]), (wk_h, wqkv.at[:, pl.ds(head, head)]),
         (wv_h, wqkv.at[:, pl.ds(2 * head, head)]), (wo_h, wqkv.at[:, pl.ds(3 * head, head)]),
-        (sm_h, sm), (wproj_h, wproj), (dg_h, dgu.at[:, pl.ds(0, hid_d)]),
-        (du_h, dgu.at[:, pl.ds(hid_d, hid_d)]), (eg_h, eg), (eu_h, eu), (ed_h, ed), (dd_h, dd),
+        (sm_h, sm), (wproj_h, wproj), (dg_h, dgu_all.at[me_x, :, pl.ds(0, hid_d)]),
+        (du_h, dgu_all.at[me_x, :, pl.ds(hid_d, hid_d)]), (eg_h, eg), (eu_h, eu), (ed_h, ed), (dd_h, dd),
     ]
     loads = [pltpu.make_async_copy(a, b, load_sem.at[k]) for k, (a, b) in enumerate(loads)]
     for copy in loads:
@@ -135,31 +143,82 @@
 
         return lax.fori_loop(1, chips, one, acc)
 
-    def gather_over_tp(phase, blocks, place):
-        mine = blocks.at[place(me_t)]
-        tp_copy(phase, mine, mine, partner, place(me_t)).start()
+    def gather_quarter():
+        to_e = side * me_y + lax.rem(owned, side)
+        spot = me_x * side + lax.div(owned, side)
 
         def give(k, _):
-            tp_copy(phase, mine, mine, 2 * chip(k) + core, place(me_t)).start()
+            over(to_e, 2 * chip(k) + core, RES, res_own, res_all.at[spot], spot).start()
             return 0
 
         lax.fori_loop(1, chips, give, 0)
 
+        @pl.when(to_e != me_e)
+        def _():
+            over(to_e, me_t, RES, res_own, res_all.at[spot], spot).start()
+
+        @pl.when(to_e == me_e)
+        def _():
+            res_all[spot] = res_own[...]
+
+        def source(spot):
+            o = side * lax.rem(spot, side) + me_x
+            j = side * me_y + lax.div(spot, side)
+            return j, lax.rem(o + j, n)
+
+        def spot_of(k, parity):
+            return (2 * lax.rem(k, 2) + parity) * side + lax.div(k, 2)
+
         def pass_on(k, _):
-            z = chip(chips - k)
-            block = blocks.at[place(2 * z + core)]
-            tp_copy(phase, block, block, 2 * z + core, place(2 * z + core)).wait_recv()
-            tp_copy(phase, block, block, partner, place(2 * z + core)).start()
-            return 0
-
-        lax.fori_loop(1, chips, pass_on, 0)
-
-        def take(z, _):
-            at = place(2 * z + 1 - core)
-            tp_copy(phase, blocks.at[at], blocks.at[at], partner, at).wait_recv()
-            return 0
-
-        lax.fori_loop(0, chips, take, 0)
+            spot = spot_of(k, lax.rem(core + me_x, 2))
+            j, t = source(spot)
+
+            @pl.when((j != me_e) | (t != me_t))
+            def _():
+                over(j, t, RES, res_all.at[spot], res_all.at[spot], spot).wait_recv()
+
+            over(me_e, partner, RES, res_all.at[spot], res_all.at[spot], spot).start()
+            return 0
+
+        lax.fori_loop(0, n // 2, pass_on, 0)
+
+        def take(k, _):
+            spot = spot_of(k, lax.rem(core + me_x + 1, 2))
+            over(me_e, partner, RES, res_all.at[spot], res_all.at[spot], spot).wait_recv()
+            return 0
+
+        lax.fori_loop(0, n // 2, take, 0)
+
+    def along_x(step):
+        return side * me_y + lax.rem(me_x + step + side, side)
+
+    def along_y(step):
+        return side * lax.rem(me_y + step + side, side) + me_x
+
+    def weight_copy(phase, buffer, block_of, peer, first, many, landing):
+        part = buffer.at[block_of, pl.ds(first, many), :]
+        return over(peer, me_t, phase, part, part, landing)
+
+    def near(phase, buffer, me, along, first, many, part):
+        for way, step in enumerate((1, -1)):
+            weight_copy(phase, buffer, me, along(step), first, many, 2 * part + way).start()
+
+    def arrived_near(phase, buffer, me, along, first, many, part):
+        for way, step in enumerate((-1, 1)):
+            owner = lax.rem(me + step + side, side)
+            weight_copy(phase, buffer, owner, along(step), first, many, 2 * part + way).wait_recv()
+
+    def far(phase, buffer, me, along, first, many, part, act):
+        half = many // 2
+        for way, step in enumerate((1, -1)):
+            if act == "start":
+                owner = lax.rem(me - step + side, side)
+                weight_copy(phase, buffer, owner, along(step), first + way * half, half, 2 * part + way).start()
+            else:
+                owner = lax.rem(me + 2, side)
+                weight_copy(phase, buffer, owner, along(-step), first + way * half, half, 2 * part + way).wait_recv()
+
+    late = block - EARLY
 
     def row_place(t):
         return lax.rem(t - me_e + n, n)
@@ -180,6 +239,22 @@
 
         return lax.fori_loop(1, n, one, carry)
 
+    def to_y_peers(phase, src_of, dst):
+        def one(d, _):
+            y = lax.rem(me_y + d, side)
+            over(side * y + me_x, me_t, phase, src_of(y), dst, me_y).start()
+            return 0
+
+        lax.fori_loop(1, side, one, 0)
+
+    def await_y_peers(phase, buffer, use=None, carry=0):
+        def one(d, carry):
+            y = lax.rem(me_y + side - d, side)
+            over(side * y + me_x, me_t, phase, buffer.at[y], buffer.at[y], y).wait_recv()
+            return carry if use is None else use(y, carry)
+
+        return lax.fori_loop(1, side, one, carry)
+
     def sent(copy, phase, many):
         copy(phase, many, many, 0, 0).wait_send()
 
@@ -188,6 +263,10 @@
              lambda peer: tok.at[:, pl.ds(pl.multiple_of(peer * block, block), block)],
              tok_all.at[me_e])
     tok_all[me_e] = tok[:, pl.ds(pl.multiple_of(me_e * block, block), block)]
+
+    loads[17].wait()
+    loads[18].wait()
+    near(NEAR, dgu_all, me_x, along_x, 0, EARLY, 0)
 
     loads[4].wait()
     loads[5].wait()
@@ -196,12 +275,12 @@
     named = sum(jnp.where(lanes_e == r, 1.0, 0.0) for r in route_rows)
     earlier = jnp.where(iota((rows, rows), 0) < iota((rows, rows), 1), 1.0, 0.0)
     before = jnp.dot(named.astype(BF16), earlier.astype(BF16), preferred_element_type=F32)
-    base = (CAP * me_e).astype(F32)
+    base = (CAP * me_y).astype(F32)
     key = jnp.where(named > 0.0, before + base, -1.0)
     eye = jnp.where(iota((rows, rows), 0) == iota((rows, rows), 1), 1.0, 0.0)
-    key_all[me_e] = lax.dot_general(
+    key_all[me_y] = lax.dot_general(
         eye.astype(BF16), key.astype(BF16), NT, preferred_element_type=F32).astype(BF16)
-    to_peers(ep_copy, me_e, KEY, lambda peer: key_all.at[me_e], key_all.at[me_e])
+    to_y_peers(KEY, lambda y: key_all.at[me_y], key_all.at[me_y])
     weights = [rw[pl.ds(k, 1), :] for k in range(2)]
     total = weights[0] + weights[1]
     spots = iota((n * SLOT, rows), 0)
@@ -215,13 +294,13 @@
     def shares():
         return pltpu.make_async_remote_copy(
             src_ref=ret_w, dst_ref=ret_w_in, send_sem=share_sem.at[0], recv_sem=share_sem.at[1],
-            device_id=(owned, me_t), device_id_type=MESH)
-
-    @pl.when(owned != me_e)
+            device_id=(final_rows, me_t), device_id_type=MESH)
+
+    @pl.when(final_rows != me_e)
     def _():
         shares().start()
 
-    @pl.when(owned == me_e)
+    @pl.when(final_rows == me_e)
     def _():
         ret_w_in[...] = ret_w[...]
 
@@ -302,23 +381,22 @@
     cell = num / jnp.maximum(jnp.abs(denom), 1.0)
     mix_all[me_e] = (jax.nn.sigmoid(outgate) * cell).astype(BF16)
     to_peers(ep_copy, me_e, MIX, lambda peer: mix_all.at[me_e], mix_all.at[me_e])
+    arrived_near(NEAR, dgu_all, me_x, along_x, 0, EARLY, 0)
+    far(FAR, dgu_all, me_x, along_x, 0, EARLY, 0, "start")
+    near(NEAR, dgu_all, me_x, along_x, EARLY, late, 1)
+    loads[22].wait()
+    near(NEAR_DOWN, dd_all, me_y, along_y, 0, hid_d, 0)
     for b in range(rows):
         nm[b] = keep_rows[pl.ds(b, 1), :] * sm[b] + wkt[:, b:b + 1] * vrow[pl.ds(b, 1), :]
-    stores = [
-        pltpu.make_async_copy(a, b, store_sem.at[k])
-        for k, (a, b) in enumerate([(nm, nm_h), (nn, nn_h), (nmax, nmax_h)])
-    ]
-    for copy in stores:
-        copy.start()
-
-    await_peers(ep_copy, me_e, KEY, key_all)
+
+    await_y_peers(KEY, key_all)
     key_t = lax.dot_general(
         jnp.where(iota((n, 128), 0) == iota((n, 128), 1), 1.0, 0.0).astype(BF16),
-        key_all[...].reshape(n * rows, 128), NT, preferred_element_type=F32)
-    places = (iota((half_rows, n * rows), 0) + core * half_rows).astype(F32)
-    for e in range(n):
-        pick[pl.ds(e * half_rows, half_rows), :] = jnp.where(
-            places == key_t[e:e + 1, :], 1.0, 0.0).astype(BF16)
+        key_all[...].reshape(quarter, 128), NT, preferred_element_type=F32)
+    places = iota((few_rows, quarter), 0).astype(F32)
+    for e in range(0, n, 2):
+        both = [jnp.where(places == key_t[k:k + 1, :], 1.0, 0.0) for k in (e, e + 1)]
+        pick[pl.ds(e * few_rows, 2 * few_rows), :] = jnp.concatenate(both, axis=0).astype(BF16)
 
     await_peers(ep_copy, me_e, MIX, mix_all)
     loads[16].wait()
@@ -327,8 +405,23 @@
     mixed = sum_over_tp(PRJ_PAIR, PRJ, prj_part, row_place, prj_pair, prj_sum, prj_in)
     mixed = summed_over_tp(PRJ, prj_in, mixed)
     residual = (tok_all[owned].astype(F32) + mixed).astype(BF16)
-    res_all[owned] = residual
-    gather_over_tp(RES, res_all, row_place)
+    res_own[...] = residual
+
+    def to_final():
+        return pltpu.make_async_remote_copy(
+            src_ref=res_own, dst_ref=res_fin, send_sem=res_sem.at[0], recv_sem=res_sem.at[1],
+            device_id=(final_cols, me_t), device_id_type=MESH)
+
+    gather_quarter()
+
+    @pl.when(final_cols != me_e)
+    def _():
+        to_final().start()
+
+    @pl.when(final_cols == me_e)
+    def _():
+        res_fin[...] = res_own[...]
+
     loads[2].wait()
     loads[3].wait()
 
@@ -336,13 +429,16 @@
         spot = core * n + peer
         tp_copy(ROW, row_in.at[spot], row_in.at[spot], partner, spot).start()
 
-    res_flat = res_all[...].reshape(n * rows, block)
+    half_side = side // 2
+    res_half = jnp.concatenate(
+        [res_all[pl.ds((core * half_side + k) * side, side)].reshape(quarter, block)
+         for k in range(half_side)], axis=1)
 
     def dispatch(c, _):
         at = pl.multiple_of(c * group, group)
-        y = jnp.dot(pick[pl.ds(pl.multiple_of(at * half_rows, group * half_rows), group * half_rows), :],
-                    res_flat, preferred_element_type=F32)
-        row_out[pl.ds(at, group)] = y.astype(BF16).reshape(group, half_rows, block)
+        y = jnp.dot(pick[pl.ds(pl.multiple_of(at * few_rows, group * few_rows), group * few_rows), :],
+                    res_half, preferred_element_type=F32)
+        row_out[pl.ds(at, group)] = y.reshape(group, few_rows, half_side * block).astype(BF16)
 
         def one(k, _):
             peer = at + k
@@ -360,67 +456,74 @@
     row_in[core * n + me_e] = row_out[me_e]
     pass_rows(me_e)
 
-    mine = pl.multiple_of(me_e * block, block)
-    gain_f = fgain[:, pl.ds(mine, block)]
+    arrived_near(NEAR, dgu_all, me_x, along_x, EARLY, late, 1)
+    far(FAR, dgu_all, me_x, along_x, EARLY, late, 1, "start")
+    arrived_near(NEAR_DOWN, dd_all, me_y, along_y, 0, hid_d, 0)
+    far(FAR_DOWN, dd_all, me_y, along_y, 0, hid_d, 0, "start")
+
     wbr_wide[...] = wbr[...].astype(F32)
     lines = block // 128
-    gain_b = gain_f * jnp.concatenate(
-        [wbr_wide[pl.ds(me_e * lines + k, 1), :] for k in range(lines)], axis=1)
-
-    def stats(b, _):
-        r = res_all[b].astype(F32)
-        ss = to_row(jnp.sum(r * r, axis=1, keepdims=True), 128)
-        br = to_row(jnp.sum(r * gain_b, axis=1, keepdims=True), 128)
-        sta_out[b] = jnp.where(iota((8, 128), 0) == 0, ss, br)
-        return 0
-
-    lax.fori_loop(0, n, stats, 0)
-    to_peers(ep_copy, me_e, STA, lambda peer: sta_out.at[peer], sta_in.at[me_e])
-    loads[17].wait()
-    loads[18].wait()
-
-    def dense(c, _):
-        at = pl.multiple_of(c * group, group)
-        x = res_all[pl.ds(at, group)].reshape(big, block).astype(F32) * gain_f
-        y = jnp.dot(x.astype(BF16), dgu[...], preferred_element_type=F32)
-        den_part[pl.ds(at, group)] = y.astype(BF16).reshape(group, rows, 2 * hid_d)
+    squares = [jnp.zeros((rows, 1), F32)] * side
+    branches = [jnp.zeros((rows, 1), F32)] * side
+    for k in range(side):
+        j = side * me_y + k
+        gain_f = fgain[:, pl.ds(pl.multiple_of(j * block, block), block)]
+        gain_b = gain_f * jnp.concatenate(
+            [wbr_wide[pl.ds(j * lines + i, 1), :] for i in range(lines)], axis=1)
+        for g in range(side):
+            r = res_all[k * side + g].astype(F32)
+            squares[g] = squares[g] + jnp.sum(r * r, axis=1, keepdims=True)
+            branches[g] = branches[g] + jnp.sum(r * gain_b, axis=1, keepdims=True)
+            x_cat[pl.ds(g * rows, rows), k * block:(k + 1) * block] = (r * gain_f).astype(BF16)
+    for g in range(side):
+        sta_out[g] = jnp.where(iota((8, 128), 0) == 0, to_row(squares[g], 128), to_row(branches[g], 128))
+    to_y_peers(STA, lambda y: sta_out.at[y], sta_in.at[me_y])
+
+    loads[19].wait()
+    loads[20].wait()
+
+    deep = half_side * block
+
+    def expert_in(y, half, ss):
+        x = row_in[pl.ds(half * n + y * side, side)].astype(F32).reshape(cap_rows, deep)
+        at = pl.multiple_of(y * side * block + half * deep, deep)
+        xg = (x * fgain[:, pl.ds(at, deep)]).astype(BF16)
+        gu_acc[:, pl.ds(0, hid_e)] += jnp.dot(xg, eg[pl.ds(at, deep), :], preferred_element_type=F32)
+        gu_acc[:, pl.ds(hid_e, hid_e)] += jnp.dot(xg, eu[pl.ds(at, deep), :], preferred_element_type=F32)
+        return ss + jnp.sum(x * x, axis=1, keepdims=True)
+
+    def expert_first(d, ss):
+        y = lax.rem(me_y + side - d, side)
 
         def one(k, _):
-            peer = at + k
+            peer = side * y + lax.rem(me_x + k, side)
+            spot = core * n + peer
 
             @pl.when(peer != me_e)
             def _():
-                ep_copy(DEN, den_part.at[peer], den_in.at[me_e], peer, me_e).start()
-
-            return 0
-
-        return lax.fori_loop(0, group, one, 0)
-
-    lax.fori_loop(0, n // group, dense, 0)
-
-    loads[19].wait()
-    loads[20].wait()
-
-    def expert_in(peer, ss):
-        other = (1 - core) * n + peer
-        tp_copy(ROW, row_in.at[other], row_in.at[other], partner, other).wait_recv()
-        x = jnp.concatenate([row_in[peer], row_in[n + peer]], axis=0).astype(F32)
-        at = pl.multiple_of(peer * block, block)
-        xg = (x * fgain[:, pl.ds(at, block)]).astype(BF16)
-        gu_acc[:, pl.ds(0, hid_e)] += jnp.dot(xg, eg[pl.ds(at, block), :], preferred_element_type=F32)
-        gu_acc[:, pl.ds(hid_e, hid_e)] += jnp.dot(xg, eu[pl.ds(at, block), :], preferred_element_type=F32)
-        return ss + jnp.sum(x * x, axis=1, keepdims=True)
-
-    def expert_next(d, ss):
-        peer = lax.rem(me_e + n - d, n)
-        spot = core * n + peer
-        ep_copy(ROW, row_in.at[spot], row_in.at[spot], peer, spot).wait_recv()
-        pass_rows(peer)
-        return expert_in(lax.rem(peer + 1, n), ss)
+                ep_copy(ROW, row_in.at[spot], row_in.at[spot], peer, spot).wait_recv()
+                pass_rows(peer)
+
+            return 0
+
+        lax.fori_loop(0, side, one, 0)
+        return expert_in(y, core, ss)
+
+    def expert_second(d, ss):
+        y = lax.rem(me_y + side - d, side)
+
+        def one(k, _):
+            other = (1 - core) * n + side * y + k
+            tp_copy(ROW, row_in.at[other], row_in.at[other], partner, other).wait_recv()
+            return 0
+
+        lax.fori_loop(0, side, one, 0)
+        return expert_in(y, 1 - core, ss)
 
     gu_acc[...] = jnp.zeros_like(gu_acc)
-    ss = lax.fori_loop(1, n, expert_next, jnp.zeros((cap_rows, 1), F32))
-    ss = expert_in(lax.rem(me_e + 1, n), ss)
+    ss = expert_first(0, jnp.zeros((cap_rows, 1), F32))
+    ss = lax.fori_loop(1, side, lambda d, ss: expert_second(d - 1, expert_first(d, ss)), ss)
+    ss = expert_second(side - 1, ss)
     row_scale = lax.rsqrt(ss / width + EPS)
     g = gu_acc[:, :hid_e] * row_scale
     u = gu_acc[:, hid_e:] * row_scale
@@ -431,30 +534,60 @@
                               preferred_element_type=F32).astype(BF16)
     routed_sum = sum_over_tp(EXP_PAIR, EXP, exp_part, row_place, exp_pair, exp_sum, exp_in)
 
-    sums = await_peers(ep_copy, me_e, STA, sta_in, lambda peer, acc: acc + sta_in[peer], sta_out[me_e])
+    far(FAR, dgu_all, me_x, along_x, 0, EARLY, 0, "wait")
+    far(FAR, dgu_all, me_x, along_x, EARLY, late, 1, "wait")
+    weights = dgu_all[...].reshape(side * block, 2 * hid_d)
+    x = x_cat[...]
+    for k in range(2 * hid_d // block):
+        y = jnp.dot(x, weights[:, k * block:(k + 1) * block], preferred_element_type=F32)
+        den_part[:, :, k * block:(k + 1) * block] = y.astype(BF16).reshape(side, rows, block)
+    to_y_peers(DEN, lambda y: den_part.at[y], den_in.at[me_y])
+
+    sums = await_y_peers(STA, sta_in, lambda y, acc: acc + sta_in[y], sta_out[me_y])
     dense_scale = lax.rsqrt(to_column(sums[0:1, :], rows) / width + EPS)
     branch = jax.nn.sigmoid(to_column(sums[1:2, :], rows) * dense_scale)
-    y = await_peers(ep_copy, me_e, DEN, den_in,
-                    lambda peer, acc: acc + den_in[peer].astype(F32),
-                    den_part[me_e].astype(F32)) * dense_scale
+    y = await_y_peers(DEN, den_in, lambda y, acc: acc + den_in[y].astype(F32),
+                      den_part[me_y].astype(F32)) * dense_scale
     g, u = y[:, :hid_d], y[:, hid_d:]
-    hid_all[me_e] = (g / (1.0 + jnp.exp(-g)) * u * branch).astype(BF16)
-    to_peers(ep_copy, me_e, HID, lambda peer: hid_all.at[me_e], hid_all.at[me_e])
+    hid_all[me_x] = (g / (1.0 + jnp.exp(-g)) * u * branch).astype(BF16)
+
+    def spread_hidden(d, _):
+        over(along_x(d), me_t, HID, hid_all.at[me_x], hid_all.at[me_x], me_x).start()
+        return 0
+
+    lax.fori_loop(1, side, spread_hidden, 0)
+
+    far(FAR_DOWN, dd_all, me_y, along_y, 0, hid_d, 0, "wait")
+
+    def hidden_of(d, _):
+        x = lax.rem(me_x + side - d, side)
+        over(along_x(-d), me_t, HID, hid_all.at[x], hid_all.at[x], x).wait_recv()
+        return 0
+
+    lax.fori_loop(1, side, hidden_of, 0)
+    x = hid_all[...].reshape(quarter, hid_d)
+    for k in range(side):
+        y = jnp.dot(x, dd_all[k], preferred_element_type=F32)
+        dwn_part[pl.ds(k * side, side)] = y.astype(BF16).reshape(side, rows, block)
+    dense_sum = sum_over_tp(DWN_PAIR, DWN, dwn_part, row_place, dwn_pair, dwn_sum, dwn_in)
 
     y = summed_over_tp(EXP, exp_in, routed_sum)
     spot, col = iota((n * SLOT, cap_rows), 0), iota((n * SLOT, cap_rows), 1)
     within = jnp.bitwise_and(spot, SLOT - 1)
-    source = CAP * jnp.right_shift(spot, SLOT.bit_length() - 1) + within
+    shift = side.bit_length() - 1
+    from_e = jnp.right_shift(spot, SLOT.bit_length() - 1)
+    source = few_rows * jnp.bitwise_and(from_e, side - 1) + CAP * jnp.right_shift(from_e, shift) + within
     spread = jnp.where((source == col) & (within < CAP), 1.0, 0.0).astype(BF16)
     ret_out[...] = jnp.dot(spread, y.astype(BF16), preferred_element_type=F32).reshape(n, SLOT, block)
 
     def give_back(i, _):
         place = lax.rem(i + owned, n)
-        own = (owned == me_e) & (place == me_t)
+        column = side * lax.div(i, side) + lax.rem(owned, side)
+        own = (column == me_e) & (place == me_t)
 
         @pl.when(jnp.logical_not(own))
         def _():
-            over(owned, place, RET, ret_out.at[i], ret_in.at[me_e], me_e).start()
+            over(column, place, RET, ret_out.at[i], ret_in.at[me_e], me_e).start()
 
         @pl.when(own)
         def _():
@@ -464,14 +597,8 @@
 
     lax.fori_loop(0, n, give_back, 0)
 
-    await_peers(ep_copy, me_e, HID, hid_all)
-    loads[22].wait()
-    y = jnp.dot(hid_all[...].reshape(n * rows, hid_d), dd[...], preferred_element_type=F32)
-    dwn_part[...] = y.astype(BF16).reshape(n, rows, block)
-    dense_sum = sum_over_tp(DWN_PAIR, DWN, dwn_part, row_place, dwn_pair, dwn_sum, dwn_in)
-
     def returned(e, _):
-        source = lax.rem(e + me_e, n)
+        source = lax.rem(e + final_cols, n)
 
         @pl.when((e != me_e) | (source != me_t))
         def _():
@@ -481,92 +608,90 @@
 
     lax.fori_loop(0, n, returned, 0)
 
-    @pl.when(owned != me_e)
+    @pl.when(final_rows != me_e)
     def _():
         shares().wait()
+
+    @pl.when(final_cols != me_e)
+    def _():
+        to_final().wait()
 
     routed = jnp.dot(ret_w_in[...], ret_in[...].reshape(n * SLOT, block), precision=HIGHEST,
                      preferred_element_type=F32)
-    known = res_all[owned].astype(F32) + routed
+    known = res_fin[...].astype(F32) + routed
 
     y = summed_over_tp(DWN, dwn_in, dense_sum)
     out_own[...] = (known + y).astype(BF16)
 
+    def columns(j):
+        return out.at[:, pl.ds(pl.multiple_of(j * block, block), block)]
+
     def publish(k, _):
-        z = chip(k)
-        over(owned, 2 * z + core, OUT, out_own, out_all.at[me_e], me_e).start()
+        over(final_rows, 2 * chip(k) + core, OUT, out_own, columns(final_cols), final_cols).start()
         return 0
 
     lax.fori_loop(1, chips, publish, 0)
 
-    @pl.when(owned != me_e)
-    def _():
-        over(owned, me_t, OUT, out_own, out_all.at[me_e], me_e).start()
-
-    @pl.when(owned == me_e)
-    def _():
-        out_all[me_e] = out_own[...]
-
-    def write(j, where):
-        return pltpu.make_async_copy(
-            out_all.at[j], out_h.at[:, pl.ds(pl.multiple_of(j * block, block), block)], out_sem.at[where])
+    @pl.when(final_rows != me_e)
+    def _():
+        over(final_rows, me_t, OUT, out_own, columns(final_cols), final_cols).start()
+
+    @pl.when(final_rows == me_e)
+    def _():
+        out[:, pl.ds(pl.multiple_of(final_cols * block, block), block)] = out_own[...]
 
     def forward(k, _):
         j = lax.rem(2 * k + lax.rem(me_e + core, 2), n)
-        source = lax.rem(me_e + j, n)
-
-        @pl.when((j != me_e) | (source != me_t))
+        source_e, source_t = side * me_y + lax.rem(j, side), lax.rem(me_e + j, n)
+
+        @pl.when((source_e != me_e) | (source_t != me_t))
         def _():
-            over(j, source, OUT, out_all.at[j], out_all.at[j], j).wait_recv()
-
-        over(me_e, partner, OUT, out_all.at[j], out_all.at[j], j).start()
-        write(j, j).start()
+            over(source_e, source_t, OUT, columns(j), columns(j), j).wait_recv()
+
+        over(me_e, partner, OUT, columns(j), columns(j), j).start()
         return 0
 
     lax.fori_loop(0, chips, forward, 0)
 
     def finish(k, _):
         j = lax.rem(2 * k + lax.rem(me_e + core + 1, 2), n)
-        over(me_e, partner, OUT, out_all.at[j], out_all.at[j], j).wait_recv()
-        write(j, j).start()
+        over(me_e, partner, OUT, columns(j), columns(j), j).wait_recv()
         return 0
 
     lax.fori_loop(0, chips, finish, 0)
-
-    def written_out(j, _):
-        write(j, j).wait()
-        return 0
-
-    lax.fori_loop(0, n, written_out, 0)
-    for copy in stores:
-        copy.wait()
     rest = pl.ds(0, n - 1)
     sent(ep_copy, TOK, tok_all.at[rest])
-    sent(ep_copy, KEY, key_all.at[rest])
+    few = pl.ds(0, side - 1)
+    sent(ep_copy, KEY, key_all.at[few])
     sent(ep_copy, QKV, qkv_part.at[rest])
     sent(ep_copy, MIX, mix_all.at[rest])
     some = pl.ds(0, chips - 1)
     sent(tp_copy, PRJ_PAIR, prj_pair)
     sent(tp_copy, PRJ, prj_sum.at[some])
-    sent(tp_copy, RES, res_all.at[rest])
     sent(ep_copy, ROW, row_in.at[pl.ds(0, 2 * n - 1)])
-    sent(ep_copy, STA, sta_out.at[rest])
-    sent(ep_copy, DEN, den_part.at[rest])
-    sent(ep_copy, HID, hid_all.at[rest])
+    sent(ep_copy, STA, sta_out.at[few])
+    sent(ep_copy, DEN, den_part.at[few])
+    sent(ep_copy, HID, hid_all.at[few])
+    for phase, buffer, rows_of in (
+        (NEAR, dgu_all, block), (FAR, dgu_all, block // 2),
+        (NEAR_DOWN, dd_all, hid_d), (FAR_DOWN, dd_all, hid_d // 2)):
+        sent(ep_copy, phase, buffer.at[pl.ds(0, 2), pl.ds(0, rows_of), :])
     sent(tp_copy, EXP_PAIR, exp_pair)
     sent(tp_copy, EXP, exp_sum.at[some])
     sent(tp_copy, DWN_PAIR, dwn_pair)
     sent(tp_copy, DWN, dwn_sum.at[some])
 
-    @pl.when(owned != me_e)
+    @pl.when(final_rows != me_e)
     def _():
         sent(ep_copy, RET, ret_out)
-        sent(ep_copy, OUT, out_all)
-
-    @pl.when(owned == me_e)
+        sent(ep_copy, RES, res_all)
+        sent(ep_copy, OUT, res_all)
+
+    @pl.when(final_rows == me_e)
     def _():
         sent(ep_copy, RET, ret_out.at[rest])
-        sent(ep_copy, OUT, out_all.at[rest])
+        sent(ep_copy, RES, res_all.at[rest])
+        sent(ep_copy, OUT, res_all.at[rest])
 
 
 def on_device(
@@ -598,7 +723,7 @@
     )
     vm = pltpu.VMEM
     dma = pltpu.SemaphoreType.DMA
-    half_rows = cap_rows // 2
+    few_rows, side = CAP * math.isqrt(n), math.isqrt(n)
 
     def hier(tall):
         return [vm((n, tall, block), BF16)] + [vm((n // 2, tall, block), BF16)] * 3
@@ -608,39 +733,37 @@
         vm((1, width), F32), vm((block, 4 * head), BF16), vm((2 * n, width), BF16), vm((1, n), F32),
         vm((head, block), BF16), vm((1, width), F32), vm((width // 128, 128), BF16), vm((2, rows), jnp.int32),
         vm((2, rows), F32), vm((width, hid_e), BF16), vm((width, hid_e), BF16), vm((hid_e, width), BF16),
-        vm((block, 2 * hid_d), BF16), vm((hid_d, block), BF16),
-        vm((n, rows, block), BF16), vm((n, rows, 128), BF16),
+        vm((side, block, 2 * hid_d), BF16), vm((side, hid_d, block), BF16),
+        vm((n, rows, block), BF16), vm((side, rows, 128), BF16),
         vm((n, rows, 4 * head), BF16), vm((n, rows, 4 * head), BF16),
-        vm((n, rows, head), BF16), *hier(rows), vm((n, rows, block), BF16),
-        vm((n, half_rows, block), BF16), vm((2 * n, half_rows, block), BF16),
-        vm((n, 8, 128), F32), vm((n, 8, 128), F32),
-        vm((n, rows, 2 * hid_d), BF16), vm((n, rows, 2 * hid_d), BF16),
-        vm((n, rows, hid_d), BF16), *hier(rows), *hier(cap_rows),
+        vm((n, rows, head), BF16), *hier(rows),
+        vm((rows, block), BF16), vm((n, rows, block), BF16), vm((rows, block), BF16),
+        vm((n, few_rows, side * block // 2), BF16), vm((2 * n, few_rows, side * block // 2), BF16),
+        vm((side, 8, 128), F32), vm((side, 8, 128), F32),
+        vm((side, rows, 2 * hid_d), BF16), vm((side, rows, 2 * hid_d), BF16),
+        vm((side, rows, hid_d), BF16), *hier(rows), *hier(cap_rows),
         vm((n, SLOT, block), F32), vm((n, SLOT, block), F32), vm((rows, n * SLOT), F32),
-        vm((rows, block), BF16), vm((n, rows, block), BF16),
-        vm((width // 128, 128), F32), vm((rows, head, head), F32), vm((rows, head), F32), vm((1, rows), F32),
-        vm((n * half_rows, n * rows), BF16), vm((cap_rows, 2 * hid_e), F32), vm((rows, 2 * n), F32),
+        vm((rows, block), BF16),
+        vm((width // 128, 128), F32),
+        vm((n * few_rows, side * rows), BF16), vm((side * rows, side * block), BF16), vm((cap_rows, 2 * hid_e), F32), vm((rows, 2 * n), F32),
         vm((head, rows), F32), vm((head, rows), F32), vm((rows, head), F32), vm((rows, head), F32),
         vm((rows, head), F32), vm((rows, n * SLOT), F32),
-        dma((len(args),)), dma((PHASES,)), dma((PHASES, 2 * n)), dma((2,)), dma((3,)), dma((n,)),
+        dma((len(args),)), dma((PHASES,)), dma((PHASES, 2 * n)), dma((2,)), dma((2,)),
     ]
     any_space = pl.BlockSpec(memory_space=pl.ANY)
-    out, new_matrix, new_norm, new_max = pl.pallas_call(
+    layer_out, new_matrix, new_norm, new_max = pl.pallas_call(
         functools.partial(layer_kernel, n),
         out_shape=(
-            jax.ShapeDtypeStruct((rows, width), BF16),
-            jax.ShapeDtypeStruct((rows, head, head), F32),
-            jax.ShapeDtypeStruct((rows, head), F32),
-            jax.ShapeDtypeStruct((1, rows), F32),
+            vm((rows, width), BF16), vm((rows, head, head), F32), vm((rows, head), F32), vm((1, rows), F32),
         ),
         in_specs=[any_space] * len(args),
-        out_specs=[any_space] * 4,
+        out_specs=[pl.BlockSpec(memory_space=vm)] * 4,
         scratch_shapes=scratch,
         compiler_params=pltpu.CompilerParams(
             collective_id=0, has_side_effects=True, vmem_limit_bytes=56 * 1024 * 1024),
         name="layer",
     )(*args)
-    return (out, new_matrix.reshape(rows, 1, head, head), new_norm.reshape(rows, 1, head), new_max.T)
+    return (layer_out, new_matrix.reshape(rows, 1, head, head), new_norm.reshape(rows, 1, head), new_max.T)
 
 
 def solution(mesh):

time: 107 us -> 98.6 us (0.921)
  Pallas kernels: 100 us -> 94.7 us
  local copies, waits for them, and re-layouts: 5.94 us -> 3.14 us
    pallas_call x1, Pallas kernels: 100 us -> 94.7 us  [on_device(): pl.pallas_call(functools.partial(layer_kernel, n), out_shape=(vm((rows, w...]
    unnamed x8 -> x4, local copies, waits for them, and re-layouts: 5.94 us -> 3.14 us
where the time goes in v3:
time: 98.6 us; the launch traced here: 98.5 us
  Pallas kernels  94.7 us (96%)
  local copies, waits for them, and re-layouts  3.14 us (3%)
    pallas_call x1, Pallas kernels, on_device(): pl.pallas_call(functools.partial(layer_kernel, n), out_shape=(vm((rows, w...  94.7 us
    unnamed x4, local copies, waits for them, and re-layouts  3.14 us

profile of v3, /device:TPU:1, one launch (start us, length us, event | category | flops | bytes accessed | tf_op | source)
XLA Modules:
  0.0 98.5 jit_solution(6314283739025193214)
XLA Ops:
  0.6 94.7 %layer.1 = (bf16[32,4096]{1,0:T(8,128)(2,1)S(1)}, f32[32,128,128]{2,1,0:T(8,128)S(1)}, f32[32,128]{1,0:T(8,128)S(1)}, f32[1,32]{1,0:T(1,128)S(1)}) custom-call(bf16[32,4096]{1,0:T(8,128)(2,1)} %tok_h.1, f32[32,128,128]{2,1,0:T(8,128)} %bitcast.24, f32[32,128]{1,0:T(8,128)} %bitcast.30, f32[1,32]{1,0:T(1,128)} %bitcast.36, f32[1,4096]{1,0:T(1,128)} %bitcast.31, ...), custom_call_target="tpu_custom_call" | custom-call | tf_op jit(solution)/shard_map/layer/pallas_call | solution.py:754
  95.4 0.7 copy.33
  96.1 1.3 %copy.34 = f32[32,1,128,128]{3,2,1,0:T(8,128)} copy(f32[32,1,128,128]{3,2,1,0:T(8,128)S(1)} %bitcast.21) | data formatting | bytes 4194304
  97.4 0.5 copy.36
  97.9 0.6 copy.35

commit v4 on v3

--- a/solution.py
+++ b/solution.py
@@ -18,6 +18,20 @@
 NT = (((1,), (1,)), ((), ()))
 
 
+def landing_spots(n):
+    side = math.isqrt(n)
+    many = {ROW: 2 * n, NEAR: 6, FAR: 6, NEAR_DOWN: 2, FAR_DOWN: 2, HID: side}
+    for phase in (TOK, KEY, QKV, STA, DEN, RET, DWN, EXP):
+        many[phase] = 1
+    for phase in (DWN_PAIR, EXP_PAIR):
+        many[phase] = n // 2
+    first, at = [], 0
+    for phase in range(PHASES):
+        first.append(at)
+        at += many.get(phase, n)
+    return first, at
+
+
 def iota(shape, dim):
     return lax.broadcasted_iota(jnp.int32, shape, dim)
 
@@ -33,10 +47,10 @@
     return jnp.sum(jnp.where(diag, column, 0.0), axis=0, keepdims=True)
 
 
-(TOK, KEY, QKV, MIX, PRJ_PAIR, PRJ, RES, ROW, STA, DEN, HID, DWN_PAIR, DWN, EXP_PAIR, EXP, RET,
- OUT, NEAR, FAR, NEAR_DOWN, FAR_DOWN) = range(21)
-PHASES = 21
-EARLY = 96
+(TOK, KEY, QKV, MIX, PROJ, RES, ROW, STA, DEN, HID, DWN_PAIR, DWN, EXP_PAIR, EXP, RET,
+ OUT, NEAR, FAR, NEAR_DOWN, FAR_DOWN) = range(20)
+PHASES = 20
+PARTS = ((0, 64), (64, 64), (128, 128))
 
 
 def layer_kernel(
@@ -44,16 +58,17 @@
     tok_h, sm_h, sn_h, smax_h, mgain_h, wq_h, wk_h, wv_h, wo_h, win_h, wfo_h, fbias_h,
     wproj_h, fgain_h, wbr_h, routes_h, rw_h, eg_h, eu_h, ed_h, dg_h, du_h, dd_h,
     out, nm, nn, nmax,
-    tok, sm, sn, smax, mgain, wqkv, wgates, fbias, wproj, fgain, wbr, routes, rw,
+    tok, sm, sn, smax, mgain, wqkv, wgates, fbias, proj_all, fgain, wbr, routes, rw,
     eg, eu, ed, dgu_all, dd_all,
-    tok_all, key_all, qkv_part, qkv_in, mix_all, prj_part, prj_pair, prj_sum, prj_in, res_own, res_all, res_fin,
+    tok_all, key_all, qkv_part, qkv_in, mix_own, mix_in, res_own, res_all, res_fin,
     row_out, row_in, sta_out, sta_in, den_part, den_in, hid_all, dwn_part, dwn_pair, dwn_sum, dwn_in,
     exp_part, exp_pair, exp_sum, exp_in, ret_out, ret_in, ret_w_in, out_own,
-    wbr_wide, pick, x_cat, gu_acc, gates, wkt, qt, vrow, keep_rows, numer, ret_w,
+    wbr_wide, pick, x_cat, hidden_e, gu_acc, gates, wkt, qt, vrow, keep_rows, numer, ret_w,
     load_sem, send_sem, recv_sem, share_sem, res_sem,
 ):
     me_e, me_t = lax.axis_index("ep"), lax.axis_index("tp")
     chips = n // 2
+    first_spot, _ = landing_spots(n)
     side = math.isqrt(n)
     me_y, me_x = lax.div(me_e, side), lax.rem(me_e, side)
     me_z, core = lax.div(me_t, 2), lax.rem(me_t, 2)
@@ -78,7 +93,7 @@
         (fbias_h, fbias), (smax_h, smax), (sn_h, sn),
         (wq_h, wqkv.at[:, pl.ds(0, head)]), (wk_h, wqkv.at[:, pl.ds(head, head)]),
         (wv_h, wqkv.at[:, pl.ds(2 * head, head)]), (wo_h, wqkv.at[:, pl.ds(3 * head, head)]),
-        (sm_h, sm), (wproj_h, wproj), (dg_h, dgu_all.at[me_x, :, pl.ds(0, hid_d)]),
+        (sm_h, sm), (wproj_h, proj_all.at[me_t]), (dg_h, dgu_all.at[me_x, :, pl.ds(0, hid_d)]),
         (du_h, dgu_all.at[me_x, :, pl.ds(hid_d, hid_d)]), (eg_h, eg), (eu_h, eu), (ed_h, ed), (dd_h, dd),
     ]
     loads = [pltpu.make_async_copy(a, b, load_sem.at[k]) for k, (a, b) in enumerate(loads)]
@@ -98,96 +113,79 @@
     def ep_copy(phase, src, dst, peer, landing):
         return pltpu.make_async_remote_copy(
             src_ref=src, dst_ref=dst, send_sem=send_sem.at[phase],
-            recv_sem=recv_sem.at[phase, landing], device_id=(peer, me_t), device_id_type=MESH)
+            recv_sem=recv_sem.at[first_spot[phase] + landing], device_id=(peer, me_t), device_id_type=MESH)
 
     def tp_copy(phase, src, dst, peer, landing):
         return pltpu.make_async_remote_copy(
             src_ref=src, dst_ref=dst, send_sem=send_sem.at[phase],
-            recv_sem=recv_sem.at[phase, landing], device_id=(me_e, peer), device_id_type=MESH)
+            recv_sem=recv_sem.at[first_spot[phase] + landing], device_id=(me_e, peer), device_id_type=MESH)
 
     def over(peer_e, peer_t, phase, src, dst, landing):
         return pltpu.make_async_remote_copy(
             src_ref=src, dst_ref=dst, send_sem=send_sem.at[phase],
-            recv_sem=recv_sem.at[phase, landing], device_id=(peer_e, peer_t), device_id_type=MESH)
+            recv_sem=recv_sem.at[first_spot[phase] + landing], device_id=(peer_e, peer_t), device_id_type=MESH)
 
     def chip(k):
         k = chips - k
         return lax.rem(me_z + chips + lax.div(k + 1, 2) * (2 * lax.rem(k, 2) - 1), chips)
 
-    def sum_over_tp(pair_phase, phase, part, place, pair, summed, arrived):
+    def sum_over_tp(pair_phase, phase, part, place, pair, summed, arrived, make=None):
         def give(k, _):
             z = lax.rem(me_z + k, chips)
-            tp_copy(pair_phase, part.at[place(2 * z + 1 - core)], pair.at[z], partner, z).start()
+            at = place(2 * z + 1 - core)
+            if make is not None:
+                part[at] = make(at)
+            tp_copy(pair_phase, part.at[at], pair.at[z], partner, z).start()
             return 0
 
         lax.fori_loop(1, chips + 1, give, 0)
 
         def add(z):
+            at = place(2 * z + core)
+            mine = part[at] if make is None else make(at)
             tp_copy(pair_phase, pair.at[z], pair.at[z], partner, z).wait_recv()
-            return part[place(2 * z + core)].astype(F32) + pair[z].astype(F32)
+            return mine.astype(F32) + pair[z].astype(F32)
 
         def pass_on(k, _):
             z = chip(k)
             summed[z] = add(z).astype(BF16)
-            tp_copy(phase, summed.at[z], arrived.at[me_z], 2 * z + core, me_z).start()
+            tp_copy(phase, summed.at[z], arrived.at[me_z], 2 * z + core, 0).start()
             return 0
 
         lax.fori_loop(1, chips, pass_on, 0)
         return add(me_z)
 
     def summed_over_tp(phase, arrived, acc):
-        def one(k, acc):
-            z = chip(chips - k)
-            tp_copy(phase, arrived.at[z], arrived.at[z], 2 * z + core, z).wait_recv()
-            return acc + arrived[z].astype(F32)
-
-        return lax.fori_loop(1, chips, one, acc)
-
-    def gather_quarter():
-        to_e = side * me_y + lax.rem(owned, side)
-        spot = me_x * side + lax.div(owned, side)
+        await_blocks(phase, arrived.at[pl.ds(0, chips - 1)])
+        return others(me_z, chips, arrived, acc)
+
+    def give_projection():
+        mine = proj_all.at[me_t]
+        tp_copy(PROJ, mine, mine, partner, me_t).start()
 
         def give(k, _):
-            over(to_e, 2 * chip(k) + core, RES, res_own, res_all.at[spot], spot).start()
+            tp_copy(PROJ, mine, mine, 2 * chip(k) + core, me_t).start()
             return 0
 
         lax.fori_loop(1, chips, give, 0)
 
-        @pl.when(to_e != me_e)
-        def _():
-            over(to_e, me_t, RES, res_own, res_all.at[spot], spot).start()
-
-        @pl.when(to_e == me_e)
-        def _():
-            res_all[spot] = res_own[...]
-
-        def source(spot):
-            o = side * lax.rem(spot, side) + me_x
-            j = side * me_y + lax.div(spot, side)
-            return j, lax.rem(o + j, n)
-
-        def spot_of(k, parity):
-            return (2 * lax.rem(k, 2) + parity) * side + lax.div(k, 2)
-
+    def pass_projection():
         def pass_on(k, _):
-            spot = spot_of(k, lax.rem(core + me_x, 2))
-            j, t = source(spot)
-
-            @pl.when((j != me_e) | (t != me_t))
-            def _():
-                over(j, t, RES, res_all.at[spot], res_all.at[spot], spot).wait_recv()
-
-            over(me_e, partner, RES, res_all.at[spot], res_all.at[spot], spot).start()
-            return 0
-
-        lax.fori_loop(0, n // 2, pass_on, 0)
-
-        def take(k, _):
-            spot = spot_of(k, lax.rem(core + me_x + 1, 2))
-            over(me_e, partner, RES, res_all.at[spot], res_all.at[spot], spot).wait_recv()
-            return 0
-
-        lax.fori_loop(0, n // 2, take, 0)
+            t = 2 * chip(chips - k) + core
+            part = proj_all.at[t]
+            tp_copy(PROJ, part, part, t, t).wait_recv()
+            tp_copy(PROJ, part, part, partner, t).start()
+            return 0
+
+        lax.fori_loop(1, chips, pass_on, 0)
+
+    def take_projection():
+        def take(z, _):
+            t = 2 * z + 1 - core
+            tp_copy(PROJ, proj_all.at[t], proj_all.at[t], partner, t).wait_recv()
+            return 0
+
+        lax.fori_loop(0, chips, take, 0)
 
     def along_x(step):
         return side * me_y + lax.rem(me_x + step + side, side)
@@ -218,7 +216,62 @@
                 owner = lax.rem(me + 2, side)
                 weight_copy(phase, buffer, owner, along(-step), first + way * half, half, 2 * part + way).wait_recv()
 
-    late = block - EARLY
+    def give_weights(part):
+        near(NEAR, dgu_all, me_x, along_x, *PARTS[part], part)
+
+    def pass_weights(part):
+        arrived_near(NEAR, dgu_all, me_x, along_x, *PARTS[part], part)
+        far(FAR, dgu_all, me_x, along_x, *PARTS[part], part, "start")
+
+    def gather_quarter():
+        to_e = side * me_y + lax.rem(owned, side)
+        spot = me_x * side + lax.div(owned, side)
+
+        def give(k, _):
+            over(to_e, 2 * chip(k) + core, RES, res_own, res_all.at[spot], spot).start()
+            return 0
+
+        lax.fori_loop(1, chips, give, 0)
+
+        @pl.when(to_e != me_e)
+        def _():
+            over(to_e, me_t, RES, res_own, res_all.at[spot], spot).start()
+
+        @pl.when(to_e == me_e)
+        def _():
+            res_all[spot] = res_own[...]
+
+        pass_weights(2)
+        arrived_near(NEAR_DOWN, dd_all, me_y, along_y, 0, hid_d, 0)
+        far(FAR_DOWN, dd_all, me_y, along_y, 0, hid_d, 0, "start")
+
+        def source(spot):
+            o = side * lax.rem(spot, side) + me_x
+            j = side * me_y + lax.div(spot, side)
+            return j, lax.rem(o + j, n)
+
+        def spot_of(k, parity):
+            return (2 * lax.rem(k, 2) + parity) * side + lax.div(k, 2)
+
+        def pass_on(k, _):
+            spot = spot_of(k, lax.rem(core + me_x, 2))
+            j, t = source(spot)
+
+            @pl.when((j != me_e) | (t != me_t))
+            def _():
+                over(j, t, RES, res_all.at[spot], res_all.at[spot], spot).wait_recv()
+
+            over(me_e, partner, RES, res_all.at[spot], res_all.at[spot], spot).start()
+            return 0
+
+        lax.fori_loop(0, n // 2, pass_on, 0)
+
+        def take(k, _):
+            spot = spot_of(k, lax.rem(core + me_x + 1, 2))
+            over(me_e, partner, RES, res_all.at[spot], res_all.at[spot], spot).wait_recv()
+            return 0
+
+        lax.fori_loop(0, n // 2, take, 0)
 
     def row_place(t):
         return lax.rem(t - me_e + n, n)
@@ -242,31 +295,50 @@
     def to_y_peers(phase, src_of, dst):
         def one(d, _):
             y = lax.rem(me_y + d, side)
-            over(side * y + me_x, me_t, phase, src_of(y), dst, me_y).start()
+            over(side * y + me_x, me_t, phase, src_of(y), dst, 0).start()
             return 0
 
         lax.fori_loop(1, side, one, 0)
 
-    def await_y_peers(phase, buffer, use=None, carry=0):
-        def one(d, carry):
-            y = lax.rem(me_y + side - d, side)
-            over(side * y + me_x, me_t, phase, buffer.at[y], buffer.at[y], y).wait_recv()
-            return carry if use is None else use(y, carry)
-
-        return lax.fori_loop(1, side, one, carry)
+    def steps(far_first):
+        offsets = [(dy, dx) for dy in range(side) for dx in range(side) if dy or dx]
+        cross = lambda o: sum(min(d, side - d) for d in o)
+        return sorted(offsets, key=cross, reverse=far_first)
+
+    def ep_at(dy, dx):
+        return side * lax.rem(me_y + dy, side) + lax.rem(me_x + dx, side)
+
+    def to_ep_peers(phase, src_of, dst):
+        for dy, dx in steps(True):
+            peer = ep_at(dy, dx)
+            ep_copy(phase, src_of(peer), dst, peer, 0).start()
+
+    def await_blocks(phase, blocks):
+        over(me_e, partner, phase, blocks, blocks, 0).wait_recv()
+
+    def others(me, many, buffer, acc):
+        def one(d, acc):
+            return acc + buffer[lax.rem(me + d, many)].astype(F32)
+
+        return lax.fori_loop(1, many, one, acc)
+
+    rest, few = pl.ds(0, n - 1), pl.ds(0, side - 1)
+    far_first = (2, 1, 3, 0) if side == 4 else tuple(range(side))
 
     def sent(copy, phase, many):
         copy(phase, many, many, 0, 0).wait_send()
 
     loads[0].wait()
-    to_peers(ep_copy, me_e, TOK,
+    to_ep_peers(TOK,
              lambda peer: tok.at[:, pl.ds(pl.multiple_of(peer * block, block), block)],
              tok_all.at[me_e])
     tok_all[me_e] = tok[:, pl.ds(pl.multiple_of(me_e * block, block), block)]
 
+    loads[16].wait()
+    give_projection()
     loads[17].wait()
     loads[18].wait()
-    near(NEAR, dgu_all, me_x, along_x, 0, EARLY, 0)
+    give_weights(0)
 
     loads[4].wait()
     loads[5].wait()
@@ -332,36 +404,28 @@
     write = jnp.exp(gate_in - new_max)
     nmax[...] = to_row(new_max, rows)
 
-    await_peers(ep_copy, me_e, TOK, tok_all)
+    await_blocks(TOK, tok_all.at[rest])
     for k in range(11, 15):
         loads[k].wait()
     gain_m = mgain[:, pl.ds(pl.multiple_of(me_e * block, block), block)]
-    group = 4
-    big = group * rows
-
-    def project(c, _):
-        at = pl.multiple_of(c * group, group)
-        x = tok_all[pl.ds(at, group)].reshape(big, block).astype(F32) * gain_m
+
+    def project(dy):
+        at = pl.multiple_of(side * lax.rem(me_y + dy, side), side)
+        x = tok_all[pl.ds(at, side)].reshape(quarter, block).astype(F32) * gain_m
         y = jnp.dot(x.astype(BF16), wqkv[...], preferred_element_type=F32)
-        qkv_part[pl.ds(at, group)] = y.astype(BF16).reshape(group, rows, 4 * head)
-
-        def one(k, _):
-            peer = at + k
-
-            @pl.when(peer != me_e)
-            def _():
-                ep_copy(QKV, qkv_part.at[peer], qkv_in.at[me_e], peer, me_e).start()
-
-            return 0
-
-        return lax.fori_loop(0, group, one, 0)
-
-    lax.fori_loop(0, n // group, project, 0)
+        qkv_part[pl.ds(at, side)] = y.astype(BF16).reshape(side, rows, 4 * head)
+        for dx in far_first:
+            if dy or dx:
+                peer = ep_at(dy, dx)
+                ep_copy(QKV, qkv_part.at[peer], qkv_in.at[me_e], peer, 0).start()
+
+    for dy in far_first:
+        project(dy)
+    give_weights(1)
 
     loads[15].wait()
-    y = await_peers(ep_copy, me_e, QKV, qkv_in,
-                    lambda peer, acc: acc + qkv_in[peer].astype(F32),
-                    qkv_part[me_e].astype(F32)) * scale
+    await_blocks(QKV, qkv_in.at[rest])
+    y = others(me_e, n, qkv_in, qkv_part[me_e].astype(F32)) * scale
     query = y[:, :head]
     keys = y[:, head:2 * head] * head ** (-0.5)
     value = y[:, 2 * head:3 * head]
@@ -379,17 +443,33 @@
     dots = jnp.sum(query * written, axis=1, keepdims=True)
     num = keep * numer[...] + dots * value
     cell = num / jnp.maximum(jnp.abs(denom), 1.0)
-    mix_all[me_e] = (jax.nn.sigmoid(outgate) * cell).astype(BF16)
-    to_peers(ep_copy, me_e, MIX, lambda peer: mix_all.at[me_e], mix_all.at[me_e])
-    arrived_near(NEAR, dgu_all, me_x, along_x, 0, EARLY, 0)
-    far(FAR, dgu_all, me_x, along_x, 0, EARLY, 0, "start")
-    near(NEAR, dgu_all, me_x, along_x, EARLY, late, 1)
+    mix_own[...] = (jax.nn.sigmoid(outgate) * cell).astype(BF16)
+
+    def head_place(h):
+        return mix_in.at[:, pl.ds(pl.multiple_of(h * head, head), head)]
+
+    for dy, dx in steps(True):
+        j = ep_at(dy, dx)
+        over(j, lax.rem(me_e + j, n), MIX, mix_own, head_place(me_t), me_t).start()
+
+    @pl.when(owned != me_e)
+    def _():
+        over(me_e, lax.rem(2 * me_e, n), MIX, mix_own, head_place(me_t), me_t).start()
+
+    @pl.when(owned == me_e)
+    def _():
+        mix_in[:, pl.ds(pl.multiple_of(me_t * head, head), head)] = mix_own[...]
+
+    give_weights(2)
     loads[22].wait()
     near(NEAR_DOWN, dd_all, me_y, along_y, 0, hid_d, 0)
+    pass_projection()
+    pass_weights(0)
+    pass_weights(1)
     for b in range(rows):
         nm[b] = keep_rows[pl.ds(b, 1), :] * sm[b] + wkt[:, b:b + 1] * vrow[pl.ds(b, 1), :]
 
-    await_y_peers(KEY, key_all)
+    await_blocks(KEY, key_all.at[few])
     key_t = lax.dot_general(
         jnp.where(iota((n, 128), 0) == iota((n, 128), 1), 1.0, 0.0).astype(BF16),
         key_all[...].reshape(quarter, 128), NT, preferred_element_type=F32)
@@ -398,12 +478,17 @@
         both = [jnp.where(places == key_t[k:k + 1, :], 1.0, 0.0) for k in (e, e + 1)]
         pick[pl.ds(e * few_rows, 2 * few_rows), :] = jnp.concatenate(both, axis=0).astype(BF16)
 
-    await_peers(ep_copy, me_e, MIX, mix_all)
-    loads[16].wait()
-    y = jnp.dot(mix_all[...].reshape(n * rows, head), wproj[...], preferred_element_type=F32)
-    prj_part[...] = y.astype(BF16).reshape(n, rows, block)
-    mixed = sum_over_tp(PRJ_PAIR, PRJ, prj_part, row_place, prj_pair, prj_sum, prj_in)
-    mixed = summed_over_tp(PRJ, prj_in, mixed)
+    take_projection()
+
+    def head_in(h, _):
+        @pl.when((owned != me_e) | (h != me_t))
+        def _():
+            over(owned, h, MIX, head_place(h), head_place(h), h).wait_recv()
+
+        return 0
+
+    lax.fori_loop(0, n, head_in, 0)
+    mixed = jnp.dot(mix_in[...], proj_all[...].reshape(n * head, block), preferred_element_type=F32)
     residual = (tok_all[owned].astype(F32) + mixed).astype(BF16)
     res_own[...] = residual
 
@@ -434,32 +519,20 @@
         [res_all[pl.ds((core * half_side + k) * side, side)].reshape(quarter, block)
          for k in range(half_side)], axis=1)
 
-    def dispatch(c, _):
-        at = pl.multiple_of(c * group, group)
-        y = jnp.dot(pick[pl.ds(pl.multiple_of(at * few_rows, group * few_rows), group * few_rows), :],
+    def dispatch(dy):
+        at = pl.multiple_of(side * lax.rem(me_y + dy, side), side)
+        y = jnp.dot(pick[pl.ds(pl.multiple_of(at * few_rows, side * few_rows), side * few_rows), :],
                     res_half, preferred_element_type=F32)
-        row_out[pl.ds(at, group)] = y.reshape(group, few_rows, half_side * block).astype(BF16)
-
-        def one(k, _):
-            peer = at + k
-
-            @pl.when(peer != me_e)
-            def _():
-                spot = core * n + me_e
+        row_out[pl.ds(at, side)] = y.reshape(side, few_rows, half_side * block).astype(BF16)
+        for dx in far_first:
+            if dy or dx:
+                peer, spot = ep_at(dy, dx), core * n + me_e
                 ep_copy(ROW, row_out.at[peer], row_in.at[spot], peer, spot).start()
 
-            return 0
-
-        return lax.fori_loop(0, group, one, 0)
-
-    lax.fori_loop(0, n // group, dispatch, 0)
+    for dy in far_first:
+        dispatch(dy)
     row_in[core * n + me_e] = row_out[me_e]
     pass_rows(me_e)
-
-    arrived_near(NEAR, dgu_all, me_x, along_x, EARLY, late, 1)
-    far(FAR, dgu_all, me_x, along_x, EARLY, late, 1, "start")
-    arrived_near(NEAR_DOWN, dd_all, me_y, along_y, 0, hid_d, 0)
-    far(FAR_DOWN, dd_all, me_y, along_y, 0, hid_d, 0, "start")
 
     wbr_wide[...] = wbr[...].astype(F32)
     lines = block // 128
@@ -479,6 +552,15 @@
         sta_out[g] = jnp.where(iota((8, 128), 0) == 0, to_row(squares[g], 128), to_row(branches[g], 128))
     to_y_peers(STA, lambda y: sta_out.at[y], sta_in.at[me_y])
 
+    for part, (first, many) in enumerate(PARTS):
+        far(FAR, dgu_all, me_x, along_x, first, many, part, "wait")
+    weights = dgu_all[...].reshape(side * block, 2 * hid_d)
+    x = x_cat[...]
+    for k in range(2 * hid_d // block):
+        y = jnp.dot(x, weights[:, k * block:(k + 1) * block], preferred_element_type=F32)
+        den_part[:, :, k * block:(k + 1) * block] = y.astype(BF16).reshape(side, rows, block)
+    to_y_peers(DEN, lambda y: den_part.at[y], den_in.at[me_y])
+
     loads[19].wait()
     loads[20].wait()
 
@@ -527,27 +609,22 @@
     row_scale = lax.rsqrt(ss / width + EPS)
     g = gu_acc[:, :hid_e] * row_scale
     u = gu_acc[:, hid_e:] * row_scale
-    hidden = (g / (1.0 + jnp.exp(-g)) * u).astype(BF16)
+    hidden_e[...] = (g / (1.0 + jnp.exp(-g)) * u).astype(BF16)
     loads[21].wait()
-    for k in range(n):
-        exp_part[k] = jnp.dot(hidden, ed[:, k * block:(k + 1) * block],
-                              preferred_element_type=F32).astype(BF16)
-    routed_sum = sum_over_tp(EXP_PAIR, EXP, exp_part, row_place, exp_pair, exp_sum, exp_in)
-
-    far(FAR, dgu_all, me_x, along_x, 0, EARLY, 0, "wait")
-    far(FAR, dgu_all, me_x, along_x, EARLY, late, 1, "wait")
-    weights = dgu_all[...].reshape(side * block, 2 * hid_d)
-    x = x_cat[...]
-    for k in range(2 * hid_d // block):
-        y = jnp.dot(x, weights[:, k * block:(k + 1) * block], preferred_element_type=F32)
-        den_part[:, :, k * block:(k + 1) * block] = y.astype(BF16).reshape(side, rows, block)
-    to_y_peers(DEN, lambda y: den_part.at[y], den_in.at[me_y])
-
-    sums = await_y_peers(STA, sta_in, lambda y, acc: acc + sta_in[y], sta_out[me_y])
+
+    def expert_out(at):
+        return jnp.dot(hidden_e[...], ed[:, pl.ds(pl.multiple_of(at * block, block), block)],
+                       preferred_element_type=F32).astype(BF16)
+
+    routed_sum = sum_over_tp(
+        EXP_PAIR, EXP, exp_part, row_place, exp_pair, exp_sum, exp_in, expert_out)
+
+    await_blocks(STA, sta_in.at[few])
+    sums = others(me_y, side, sta_in, sta_out[me_y])
     dense_scale = lax.rsqrt(to_column(sums[0:1, :], rows) / width + EPS)
     branch = jax.nn.sigmoid(to_column(sums[1:2, :], rows) * dense_scale)
-    y = await_y_peers(DEN, den_in, lambda y, acc: acc + den_in[y].astype(F32),
-                      den_part[me_y].astype(F32)) * dense_scale
+    await_blocks(DEN, den_in.at[few])
+    y = others(me_y, side, den_in, den_part[me_y].astype(F32)) * dense_scale
     g, u = y[:, :hid_d], y[:, hid_d:]
     hid_all[me_x] = (g / (1.0 + jnp.exp(-g)) * u * branch).astype(BF16)
 
@@ -578,7 +655,8 @@
     from_e = jnp.right_shift(spot, SLOT.bit_length() - 1)
     source = few_rows * jnp.bitwise_and(from_e, side - 1) + CAP * jnp.right_shift(from_e, shift) + within
     spread = jnp.where((source == col) & (within < CAP), 1.0, 0.0).astype(BF16)
-    ret_out[...] = jnp.dot(spread, y.astype(BF16), preferred_element_type=F32).reshape(n, SLOT, block)
+    ret_out[...] = jnp.dot(
+        spread, y.astype(BF16), preferred_element_type=F32).reshape(n, SLOT, block).astype(BF16)
 
     def give_back(i, _):
         place = lax.rem(i + owned, n)
@@ -587,7 +665,7 @@
 
         @pl.when(jnp.logical_not(own))
         def _():
-            over(column, place, RET, ret_out.at[i], ret_in.at[me_e], me_e).start()
+            over(column, place, RET, ret_out.at[i], ret_in.at[me_e], 0).start()
 
         @pl.when(own)
         def _():
@@ -597,26 +675,23 @@
 
     lax.fori_loop(0, n, give_back, 0)
 
-    def returned(e, _):
-        source = lax.rem(e + final_cols, n)
-
-        @pl.when((e != me_e) | (source != me_t))
-        def _():
-            over(e, source, RET, ret_in.at[e], ret_in.at[e], e).wait_recv()
-
-        return 0
-
-    lax.fori_loop(0, n, returned, 0)
-
     @pl.when(final_rows != me_e)
     def _():
+        await_blocks(RET, ret_in)
+
+    @pl.when(final_rows == me_e)
+    def _():
+        await_blocks(RET, ret_in.at[rest])
+
+    @pl.when(final_rows != me_e)
+    def _():
         shares().wait()
 
     @pl.when(final_cols != me_e)
     def _():
         to_final().wait()
 
-    routed = jnp.dot(ret_w_in[...], ret_in[...].reshape(n * SLOT, block), precision=HIGHEST,
+    routed = jnp.dot(ret_w_in[...], ret_in[...].astype(F32).reshape(n * SLOT, block), precision=HIGHEST,
                      preferred_element_type=F32)
     known = res_fin[...].astype(F32) + routed
 
@@ -659,15 +734,20 @@
         return 0
 
     lax.fori_loop(0, chips, finish, 0)
-    rest = pl.ds(0, n - 1)
     sent(ep_copy, TOK, tok_all.at[rest])
-    few = pl.ds(0, side - 1)
     sent(ep_copy, KEY, key_all.at[few])
     sent(ep_copy, QKV, qkv_part.at[rest])
-    sent(ep_copy, MIX, mix_all.at[rest])
     some = pl.ds(0, chips - 1)
-    sent(tp_copy, PRJ_PAIR, prj_pair)
-    sent(tp_copy, PRJ, prj_sum.at[some])
+
+    @pl.when(owned != me_e)
+    def _():
+        sent(ep_copy, MIX, mix_in)
+
+    @pl.when(owned == me_e)
+    def _():
+        sent(ep_copy, MIX, mix_in.at[:, pl.ds(0, (n - 1) * head)])
+
+    sent(tp_copy, PROJ, proj_all.at[rest])
     sent(ep_copy, ROW, row_in.at[pl.ds(0, 2 * n - 1)])
     sent(ep_copy, STA, sta_out.at[few])
     sent(ep_copy, DEN, den_part.at[few])
@@ -731,24 +811,24 @@
     scratch = [
         vm((rows, width), BF16), vm((rows, head, head), F32), vm((rows, head), F32), vm((1, rows), F32),
         vm((1, width), F32), vm((block, 4 * head), BF16), vm((2 * n, width), BF16), vm((1, n), F32),
-        vm((head, block), BF16), vm((1, width), F32), vm((width // 128, 128), BF16), vm((2, rows), jnp.int32),
+        vm((n, head, block), BF16), vm((1, width), F32), vm((width // 128, 128), BF16), vm((2, rows), jnp.int32),
         vm((2, rows), F32), vm((width, hid_e), BF16), vm((width, hid_e), BF16), vm((hid_e, width), BF16),
         vm((side, block, 2 * hid_d), BF16), vm((side, hid_d, block), BF16),
         vm((n, rows, block), BF16), vm((side, rows, 128), BF16),
         vm((n, rows, 4 * head), BF16), vm((n, rows, 4 * head), BF16),
-        vm((n, rows, head), BF16), *hier(rows),
+        vm((rows, head), BF16), vm((rows, n * head), BF16),
         vm((rows, block), BF16), vm((n, rows, block), BF16), vm((rows, block), BF16),
         vm((n, few_rows, side * block // 2), BF16), vm((2 * n, few_rows, side * block // 2), BF16),
         vm((side, 8, 128), F32), vm((side, 8, 128), F32),
         vm((side, rows, 2 * hid_d), BF16), vm((side, rows, 2 * hid_d), BF16),
         vm((side, rows, hid_d), BF16), *hier(rows), *hier(cap_rows),
-        vm((n, SLOT, block), F32), vm((n, SLOT, block), F32), vm((rows, n * SLOT), F32),
+        vm((n, SLOT, block), BF16), vm((n, SLOT, block), BF16), vm((rows, n * SLOT), F32),
         vm((rows, block), BF16),
         vm((width // 128, 128), F32),
-        vm((n * few_rows, side * rows), BF16), vm((side * rows, side * block), BF16), vm((cap_rows, 2 * hid_e), F32), vm((rows, 2 * n), F32),
+        vm((n * few_rows, side * rows), BF16), vm((side * rows, side * block), BF16), vm((cap_rows, hid_e), BF16), vm((cap_rows, 2 * hid_e), F32), vm((rows, 2 * n), F32),
         vm((head, rows), F32), vm((head, rows), F32), vm((rows, head), F32), vm((rows, head), F32),
         vm((rows, head), F32), vm((rows, n * SLOT), F32),
-        dma((len(args),)), dma((PHASES,)), dma((PHASES, 2 * n)), dma((2,)), dma((2,)),
+        dma((len(args),)), dma((PHASES,)), dma((landing_spots(n)[1],)), dma((2,)), dma((2,)),
     ]
     any_space = pl.BlockSpec(memory_space=pl.ANY)
     layer_out, new_matrix, new_norm, new_max = pl.pallas_call(

time: 98.6 us -> 85.3 us (0.87)
  Pallas kernels: 94.7 us -> 81.5 us
    pallas_call x1, Pallas kernels: 94.7 us -> 81.5 us  [on_device(): pl.pallas_call(functools.partial(layer_kernel, n), out_shape=(vm((rows, w...]
where the time goes in v4:
time: 85.3 us
  Pallas kernels  81.5 us (96%)
  local copies, waits for them, and re-layouts  3.14 us (4%)
    pallas_call x1, Pallas kernels, on_device(): pl.pallas_call(functools.partial(layer_kernel, n), out_shape=(vm((rows, w...  81.5 us
    unnamed x4, local copies, waits for them, and re-layouts  3.14 us

profile of v4, /device:TPU:1, one launch (start us, length us, event | category | flops | bytes accessed | tf_op | source)
XLA Modules:
  0.0 85.3 jit_solution(18263902130652673022)
XLA Ops:
  0.6 81.5 %layer.1 = (bf16[32,4096]{1,0:T(8,128)(2,1)S(1)}, f32[32,128,128]{2,1,0:T(8,128)S(1)}, f32[32,128]{1,0:T(8,128)S(1)}, f32[1,32]{1,0:T(1,128)S(1)}) custom-call(bf16[32,4096]{1,0:T(8,128)(2,1)} %tok_h.1, f32[32,128,128]{2,1,0:T(8,128)} %bitcast.24, f32[32,128]{1,0:T(8,128)} %bitcast.30, f32[1,32]{1,0:T(1,128)} %bitcast.36, f32[1,4096]{1,0:T(1,128)} %bitcast.31, ...), custom_call_target="tpu_custom_call" | custom-call | tf_op jit(solution)/shard_map/layer/pallas_call | solution.py:834
  82.1 0.7 copy.33
  82.8 1.3 %copy.34 = f32[32,1,128,128]{3,2,1,0:T(8,128)} copy(f32[32,1,128,128]{3,2,1,0:T(8,128)S(1)} %bitcast.21) | data formatting | bytes 4194304
  84.1 0.5 copy.36
  84.7 0.6 copy.35

commit v5 on v4

--- a/solution.py
+++ b/solution.py
@@ -20,11 +20,11 @@
 
 def landing_spots(n):
     side = math.isqrt(n)
-    many = {ROW: 2 * n, NEAR: 6, FAR: 6, NEAR_DOWN: 2, FAR_DOWN: 2, HID: side}
-    for phase in (TOK, KEY, QKV, STA, DEN, RET, DWN, EXP):
+    many = {ROW: n + side, RES: n + 1, NEAR: 6, FAR: 6, NEAR_DOWN: 2, FAR_DOWN: 2, HID: side}
+    for phase in (TOK, KEY, QKV, STA, DEN, RET, MIX, DWN, DWN_PAIR, EXP):
         many[phase] = 1
-    for phase in (DWN_PAIR, EXP_PAIR):
-        many[phase] = n // 2
+    many[EXP_PAIR] = n // 2
+    many[PROJ] = many[OUT] = n // 2 + 1
     first, at = [], 0
     for phase in range(PHASES):
         first.append(at)
@@ -62,9 +62,9 @@
     eg, eu, ed, dgu_all, dd_all,
     tok_all, key_all, qkv_part, qkv_in, mix_own, mix_in, res_own, res_all, res_fin,
     row_out, row_in, sta_out, sta_in, den_part, den_in, hid_all, dwn_part, dwn_pair, dwn_sum, dwn_in,
-    exp_part, exp_pair, exp_sum, exp_in, ret_out, ret_in, ret_w_in, out_own,
+    exp_part, exp_pair, exp_sum, exp_in, ret_out, ret_in, out_own,
     wbr_wide, pick, x_cat, hidden_e, gu_acc, gates, wkt, qt, vrow, keep_rows, numer, ret_w,
-    load_sem, send_sem, recv_sem, share_sem, res_sem,
+    load_sem, send_sem, recv_sem, res_sem,
 ):
     me_e, me_t = lax.axis_index("ep"), lax.axis_index("tp")
     chips = n // 2
@@ -74,8 +74,6 @@
     me_z, core = lax.div(me_t, 2), lax.rem(me_t, 2)
     partner = me_t + 1 - 2 * core
     owned = lax.rem(me_t - me_e + n, n)
-    final_rows = side * me_y + lax.rem(owned, side)
-    final_cols = side * lax.div(owned, side) + me_x
     rows = tok.shape[0]
     width = tok.shape[1]
     block = width // n
@@ -129,20 +127,18 @@
         k = chips - k
         return lax.rem(me_z + chips + lax.div(k + 1, 2) * (2 * lax.rem(k, 2) - 1), chips)
 
-    def sum_over_tp(pair_phase, phase, part, place, pair, summed, arrived, make=None):
+    def sum_over_tp(pair_phase, phase, part, pair, summed, arrived, make):
         def give(k, _):
             z = lax.rem(me_z + k, chips)
-            at = place(2 * z + 1 - core)
-            if make is not None:
-                part[at] = make(at)
+            at = 2 * z + 1 - core
+            part[at] = make(at)
             tp_copy(pair_phase, part.at[at], pair.at[z], partner, z).start()
             return 0
 
         lax.fori_loop(1, chips + 1, give, 0)
 
         def add(z):
-            at = place(2 * z + core)
-            mine = part[at] if make is None else make(at)
+            mine = make(2 * z + core)
             tp_copy(pair_phase, pair.at[z], pair.at[z], partner, z).wait_recv()
             return mine.astype(F32) + pair[z].astype(F32)
 
@@ -159,33 +155,30 @@
         await_blocks(phase, arrived.at[pl.ds(0, chips - 1)])
         return others(me_z, chips, arrived, acc)
 
-    def give_projection():
-        mine = proj_all.at[me_t]
-        tp_copy(PROJ, mine, mine, partner, me_t).start()
+    def give_over_tp(phase, mine, spot):
+        tp_copy(phase, mine, spot(me_t), partner, chips).start()
 
         def give(k, _):
-            tp_copy(PROJ, mine, mine, 2 * chip(k) + core, me_t).start()
+            tp_copy(phase, mine, spot(me_t), 2 * chip(k) + core, me_z).start()
             return 0
 
         lax.fori_loop(1, chips, give, 0)
 
-    def pass_projection():
+    def pass_over_tp(phase, spot):
         def pass_on(k, _):
-            t = 2 * chip(chips - k) + core
-            part = proj_all.at[t]
-            tp_copy(PROJ, part, part, t, t).wait_recv()
-            tp_copy(PROJ, part, part, partner, t).start()
+            z = chip(chips - k)
+            part = spot(2 * z + core)
+            tp_copy(phase, part, part, 2 * z + core, z).wait_recv()
+            tp_copy(phase, part, part, partner, chips).start()
             return 0
 
         lax.fori_loop(1, chips, pass_on, 0)
 
-    def take_projection():
-        def take(z, _):
-            t = 2 * z + 1 - core
-            tp_copy(PROJ, proj_all.at[t], proj_all.at[t], partner, t).wait_recv()
-            return 0
-
-        lax.fori_loop(0, chips, take, 0)
+    def take_over_tp(phase, half):
+        tp_copy(phase, half, half, partner, chips).wait_recv()
+
+    def projection(t):
+        return proj_all.at[t]
 
     def along_x(step):
         return side * me_y + lax.rem(me_x + step + side, side)
@@ -261,36 +254,13 @@
             def _():
                 over(j, t, RES, res_all.at[spot], res_all.at[spot], spot).wait_recv()
 
-            over(me_e, partner, RES, res_all.at[spot], res_all.at[spot], spot).start()
+            over(me_e, partner, RES, res_all.at[spot], res_all.at[spot], n).start()
             return 0
 
         lax.fori_loop(0, n // 2, pass_on, 0)
 
-        def take(k, _):
-            spot = spot_of(k, lax.rem(core + me_x + 1, 2))
-            over(me_e, partner, RES, res_all.at[spot], res_all.at[spot], spot).wait_recv()
-            return 0
-
-        lax.fori_loop(0, n // 2, take, 0)
-
-    def row_place(t):
-        return lax.rem(t - me_e + n, n)
-
-    def to_peers(copy, me, phase, src_of, dst):
-        def one(d, _):
-            peer = lax.rem(me + d, n)
-            copy(phase, src_of(peer), dst, peer, me).start()
-            return 0
-
-        lax.fori_loop(1, n, one, 0)
-
-    def await_peers(copy, me, phase, buffer, use=None, carry=0):
-        def one(d, carry):
-            peer = lax.rem(me + n - d, n)
-            copy(phase, buffer.at[peer], buffer.at[peer], peer, peer).wait_recv()
-            return carry if use is None else use(peer, carry)
-
-        return lax.fori_loop(1, n, one, carry)
+        half = res_all.at[pl.ds(0, chips)]
+        over(me_e, partner, RES, half, half, n).wait_recv()
 
     def to_y_peers(phase, src_of, dst):
         def one(d, _):
@@ -335,7 +305,7 @@
     tok_all[me_e] = tok[:, pl.ds(pl.multiple_of(me_e * block, block), block)]
 
     loads[16].wait()
-    give_projection()
+    give_over_tp(PROJ, projection(me_t), projection)
     loads[17].wait()
     loads[18].wait()
     give_weights(0)
@@ -362,19 +332,6 @@
         hit = (spots.astype(F32) == r.astype(F32) * SLOT + slot)
         share_t = share_t + jnp.where(hit, w / total, 0.0)
     ret_w[...] = lax.dot_general(eye, share_t, NT, precision=HIGHEST, preferred_element_type=F32)
-
-    def shares():
-        return pltpu.make_async_remote_copy(
-            src_ref=ret_w, dst_ref=ret_w_in, send_sem=share_sem.at[0], recv_sem=share_sem.at[1],
-            device_id=(final_rows, me_t), device_id_type=MESH)
-
-    @pl.when(final_rows != me_e)
-    def _():
-        shares().start()
-
-    @pl.when(final_rows == me_e)
-    def _():
-        ret_w_in[...] = ret_w[...]
 
     loads[1].wait()
     squares = jnp.zeros((rows, block), F32)
@@ -450,11 +407,11 @@
 
     for dy, dx in steps(True):
         j = ep_at(dy, dx)
-        over(j, lax.rem(me_e + j, n), MIX, mix_own, head_place(me_t), me_t).start()
+        over(j, lax.rem(me_e + j, n), MIX, mix_own, head_place(me_t), 0).start()
 
     @pl.when(owned != me_e)
     def _():
-        over(me_e, lax.rem(2 * me_e, n), MIX, mix_own, head_place(me_t), me_t).start()
+        over(me_e, lax.rem(2 * me_e, n), MIX, mix_own, head_place(me_t), 0).start()
 
     @pl.when(owned == me_e)
     def _():
@@ -463,7 +420,7 @@
     give_weights(2)
     loads[22].wait()
     near(NEAR_DOWN, dd_all, me_y, along_y, 0, hid_d, 0)
-    pass_projection()
+    pass_over_tp(PROJ, projection)
     pass_weights(0)
     pass_weights(1)
     for b in range(rows):
@@ -478,16 +435,16 @@
         both = [jnp.where(places == key_t[k:k + 1, :], 1.0, 0.0) for k in (e, e + 1)]
         pick[pl.ds(e * few_rows, 2 * few_rows), :] = jnp.concatenate(both, axis=0).astype(BF16)
 
-    take_projection()
-
-    def head_in(h, _):
-        @pl.when((owned != me_e) | (h != me_t))
-        def _():
-            over(owned, h, MIX, head_place(h), head_place(h), h).wait_recv()
-
-        return 0
-
-    lax.fori_loop(0, n, head_in, 0)
+    take_over_tp(PROJ, proj_all.at[pl.ds(0, chips)])
+
+    @pl.when(owned != me_e)
+    def _():
+        await_blocks(MIX, mix_in)
+
+    @pl.when(owned == me_e)
+    def _():
+        await_blocks(MIX, mix_in.at[:, pl.ds(0, (n - 1) * head)])
+
     mixed = jnp.dot(mix_in[...], proj_all[...].reshape(n * head, block), preferred_element_type=F32)
     residual = (tok_all[owned].astype(F32) + mixed).astype(BF16)
     res_own[...] = residual
@@ -495,15 +452,17 @@
     def to_final():
         return pltpu.make_async_remote_copy(
             src_ref=res_own, dst_ref=res_fin, send_sem=res_sem.at[0], recv_sem=res_sem.at[1],
-            device_id=(final_cols, me_t), device_id_type=MESH)
+            device_id=(owned, me_e), device_id_type=MESH)
+
+    corner = (owned == me_e) & (me_e == me_t)
 
     gather_quarter()
 
-    @pl.when(final_cols != me_e)
+    @pl.when(jnp.logical_not(corner))
     def _():
         to_final().start()
 
-    @pl.when(final_cols == me_e)
+    @pl.when(corner)
     def _():
         res_fin[...] = res_own[...]
 
@@ -511,8 +470,8 @@
     loads[3].wait()
 
     def pass_rows(peer):
-        spot = core * n + peer
-        tp_copy(ROW, row_in.at[spot], row_in.at[spot], partner, spot).start()
+        part = row_in.at[core * n + peer]
+        tp_copy(ROW, part, part, partner, n + lax.div(peer, side)).start()
 
     half_side = side // 2
     res_half = jnp.concatenate(
@@ -527,7 +486,7 @@
         for dx in far_first:
             if dy or dx:
                 peer, spot = ep_at(dy, dx), core * n + me_e
-                ep_copy(ROW, row_out.at[peer], row_in.at[spot], peer, spot).start()
+                ep_copy(ROW, row_out.at[peer], row_in.at[spot], peer, me_e).start()
 
     for dy in far_first:
         dispatch(dy)
@@ -583,7 +542,7 @@
 
             @pl.when(peer != me_e)
             def _():
-                ep_copy(ROW, row_in.at[spot], row_in.at[spot], peer, spot).wait_recv()
+                ep_copy(ROW, row_in.at[spot], row_in.at[spot], peer, peer).wait_recv()
                 pass_rows(peer)
 
             return 0
@@ -594,12 +553,8 @@
     def expert_second(d, ss):
         y = lax.rem(me_y + side - d, side)
 
-        def one(k, _):
-            other = (1 - core) * n + side * y + k
-            tp_copy(ROW, row_in.at[other], row_in.at[other], partner, other).wait_recv()
-            return 0
-
-        lax.fori_loop(0, side, one, 0)
+        part = row_in.at[pl.ds((1 - core) * n + side * y, side)]
+        tp_copy(ROW, part, part, partner, n + y).wait_recv()
         return expert_in(y, 1 - core, ss)
 
     gu_acc[...] = jnp.zeros_like(gu_acc)
@@ -617,7 +572,7 @@
                        preferred_element_type=F32).astype(BF16)
 
     routed_sum = sum_over_tp(
-        EXP_PAIR, EXP, exp_part, row_place, exp_pair, exp_sum, exp_in, expert_out)
+        EXP_PAIR, EXP, exp_part, exp_pair, exp_sum, exp_in, expert_out)
 
     await_blocks(STA, sta_in.at[few])
     sums = others(me_y, side, sta_in, sta_out[me_y])
@@ -646,7 +601,35 @@
     for k in range(side):
         y = jnp.dot(x, dd_all[k], preferred_element_type=F32)
         dwn_part[pl.ds(k * side, side)] = y.astype(BF16).reshape(side, rows, block)
-    dense_sum = sum_over_tp(DWN_PAIR, DWN, dwn_part, row_place, dwn_pair, dwn_sum, dwn_in)
+    end_core = lax.rem(me_x, 2)
+    home = lax.rem(me_t, side) == me_x
+
+    @pl.when(core != end_core)
+    def _():
+        tp_copy(DWN_PAIR, dwn_part, dwn_pair, partner, 0).start()
+
+    @pl.when(core == end_core)
+    def _():
+        tp_copy(DWN_PAIR, dwn_pair, dwn_pair, partner, 0).wait_recv()
+        for dx in far_first:
+            def to_end(c, _):
+                x = lax.rem(me_x + dx, side)
+                k = side * c + x
+                dwn_sum[k] = (dwn_part[k].astype(F32) + dwn_pair[k].astype(F32)).astype(BF16)
+                z = 2 * c + lax.div(me_x, 2)
+                here = (x == me_x) & (z == me_z)
+
+                @pl.when(jnp.logical_not(here))
+                def _():
+                    over(side * me_y + x, 2 * z + core, DWN, dwn_sum.at[k], dwn_in.at[me_z], 0).start()
+
+                @pl.when(here)
+                def _():
+                    dwn_in[me_z] = dwn_sum[k]
+
+                return 0
+
+            lax.fori_loop(0, side, to_end, 0)
 
     y = summed_over_tp(EXP, exp_in, routed_sum)
     spot, col = iota((n * SLOT, cap_rows), 0), iota((n * SLOT, cap_rows), 1)
@@ -658,82 +641,37 @@
     ret_out[...] = jnp.dot(
         spread, y.astype(BF16), preferred_element_type=F32).reshape(n, SLOT, block).astype(BF16)
 
-    def give_back(i, _):
-        place = lax.rem(i + owned, n)
-        column = side * lax.div(i, side) + lax.rem(owned, side)
-        own = (column == me_e) & (place == me_t)
-
-        @pl.when(jnp.logical_not(own))
-        def _():
-            over(column, place, RET, ret_out.at[i], ret_in.at[me_e], 0).start()
-
-        @pl.when(own)
-        def _():
-            ret_in[me_e] = ret_out[i]
-
-        return 0
-
-    lax.fori_loop(0, n, give_back, 0)
-
-    @pl.when(final_rows != me_e)
-    def _():
-        await_blocks(RET, ret_in)
-
-    @pl.when(final_rows == me_e)
-    def _():
-        await_blocks(RET, ret_in.at[rest])
-
-    @pl.when(final_rows != me_e)
-    def _():
-        shares().wait()
-
-    @pl.when(final_cols != me_e)
+    to_ep_peers(RET, lambda peer: ret_out.at[peer], ret_in.at[me_e])
+    ret_in[me_e] = ret_out[me_e]
+
+    await_blocks(RET, ret_in.at[rest])
+
+    @pl.when(jnp.logical_not(corner))
     def _():
         to_final().wait()
 
-    routed = jnp.dot(ret_w_in[...], ret_in[...].astype(F32).reshape(n * SLOT, block), precision=HIGHEST,
+    routed = jnp.dot(ret_w[...], ret_in[...].astype(F32).reshape(n * SLOT, block), precision=HIGHEST,
                      preferred_element_type=F32)
     known = res_fin[...].astype(F32) + routed
 
-    y = summed_over_tp(DWN, dwn_in, dense_sum)
+    @pl.when(home)
+    def _():
+        await_blocks(DWN, dwn_in.at[pl.ds(0, chips - 1)])
+
+    @pl.when(jnp.logical_not(home))
+    def _():
+        await_blocks(DWN, dwn_in)
+
+    y = others(me_z, chips, dwn_in, dwn_in[me_z].astype(F32))
     out_own[...] = (known + y).astype(BF16)
 
     def columns(j):
         return out.at[:, pl.ds(pl.multiple_of(j * block, block), block)]
 
-    def publish(k, _):
-        over(final_rows, 2 * chip(k) + core, OUT, out_own, columns(final_cols), final_cols).start()
-        return 0
-
-    lax.fori_loop(1, chips, publish, 0)
-
-    @pl.when(final_rows != me_e)
-    def _():
-        over(final_rows, me_t, OUT, out_own, columns(final_cols), final_cols).start()
-
-    @pl.when(final_rows == me_e)
-    def _():
-        out[:, pl.ds(pl.multiple_of(final_cols * block, block), block)] = out_own[...]
-
-    def forward(k, _):
-        j = lax.rem(2 * k + lax.rem(me_e + core, 2), n)
-        source_e, source_t = side * me_y + lax.rem(j, side), lax.rem(me_e + j, n)
-
-        @pl.when((source_e != me_e) | (source_t != me_t))
-        def _():
-            over(source_e, source_t, OUT, columns(j), columns(j), j).wait_recv()
-
-        over(me_e, partner, OUT, columns(j), columns(j), j).start()
-        return 0
-
-    lax.fori_loop(0, chips, forward, 0)
-
-    def finish(k, _):
-        j = lax.rem(2 * k + lax.rem(me_e + core + 1, 2), n)
-        over(me_e, partner, OUT, columns(j), columns(j), j).wait_recv()
-        return 0
-
-    lax.fori_loop(0, chips, finish, 0)
+    give_over_tp(OUT, out_own, columns)
+    out[:, pl.ds(pl.multiple_of(me_t * block, block), block)] = out_own[...]
+    pass_over_tp(OUT, columns)
+    take_over_tp(OUT, out.at[:, pl.ds(0, chips * block)])
     sent(ep_copy, TOK, tok_all.at[rest])
     sent(ep_copy, KEY, key_all.at[few])
     sent(ep_copy, QKV, qkv_part.at[rest])
@@ -758,20 +696,30 @@
         sent(ep_copy, phase, buffer.at[pl.ds(0, 2), pl.ds(0, rows_of), :])
     sent(tp_copy, EXP_PAIR, exp_pair)
     sent(tp_copy, EXP, exp_sum.at[some])
-    sent(tp_copy, DWN_PAIR, dwn_pair)
-    sent(tp_copy, DWN, dwn_sum.at[some])
-
-    @pl.when(final_rows != me_e)
-    def _():
-        sent(ep_copy, RET, ret_out)
+    sent(ep_copy, RET, ret_out.at[rest])
+    sent(tp_copy, OUT, tok_all.at[rest])
+
+    @pl.when(core != end_core)
+    def _():
+        sent(tp_copy, DWN_PAIR, dwn_part)
+
+    @pl.when(home)
+    def _():
+        sent(ep_copy, DWN, dwn_sum.at[rest])
+
+    @pl.when((core == end_core) & jnp.logical_not(home))
+    def _():
+        sent(ep_copy, DWN, dwn_sum)
+
+    own_column = lax.rem(owned, side) == me_x
+
+    @pl.when(jnp.logical_not(own_column))
+    def _():
         sent(ep_copy, RES, res_all)
-        sent(ep_copy, OUT, res_all)
-
-    @pl.when(final_rows == me_e)
-    def _():
-        sent(ep_copy, RET, ret_out.at[rest])
+
+    @pl.when(own_column)
+    def _():
         sent(ep_copy, RES, res_all.at[rest])
-        sent(ep_copy, OUT, res_all.at[rest])
 
 
 def on_device(
@@ -821,14 +769,15 @@
         vm((n, few_rows, side * block // 2), BF16), vm((2 * n, few_rows, side * block // 2), BF16),
         vm((side, 8, 128), F32), vm((side, 8, 128), F32),
         vm((side, rows, 2 * hid_d), BF16), vm((side, rows, 2 * hid_d), BF16),
-        vm((side, rows, hid_d), BF16), *hier(rows), *hier(cap_rows),
-        vm((n, SLOT, block), BF16), vm((n, SLOT, block), BF16), vm((rows, n * SLOT), F32),
+        vm((side, rows, hid_d), BF16), *[vm((n, rows, block), BF16)] * 3, vm((n // 2, rows, block), BF16),
+        *hier(cap_rows),
+        vm((n, SLOT, block), BF16), vm((n, SLOT, block), BF16),
         vm((rows, block), BF16),
         vm((width // 128, 128), F32),
         vm((n * few_rows, side * rows), BF16), vm((side * rows, side * block), BF16), vm((cap_rows, hid_e), BF16), vm((cap_rows, 2 * hid_e), F32), vm((rows, 2 * n), F32),
         vm((head, rows), F32), vm((head, rows), F32), vm((rows, head), F32), vm((rows, head), F32),
         vm((rows, head), F32), vm((rows, n * SLOT), F32),
-        dma((len(args),)), dma((PHASES,)), dma((landing_spots(n)[1],)), dma((2,)), dma((2,)),
+        dma((len(args),)), dma((PHASES,)), dma((landing_spots(n)[1],)), dma((2,)),
     ]
     any_space = pl.BlockSpec(memory_space=pl.ANY)
     layer_out, new_matrix, new_norm, new_max = pl.pallas_call(

time: 85.3 us -> 81.6 us (0.957)
  Pallas kernels: 81.5 us -> 77.8 us
    pallas_call x1, Pallas kernels: 81.5 us -> 77.8 us  [on_device(): pl.pallas_call(functools.partial(layer_kernel, n), out_shape=(vm((rows, w...]
where the time goes in v5:
time: 81.6 us
  Pallas kernels  77.8 us (95%)
  local copies, waits for them, and re-layouts  3.14 us (4%)
    pallas_call x1, Pallas kernels, on_device(): pl.pallas_call(functools.partial(layer_kernel, n), out_shape=(vm((rows, w...  77.8 us
    unnamed x4, local copies, waits for them, and re-layouts  3.14 us

profile of v5, /device:TPU:1, one launch (start us, length us, event | category | flops | bytes accessed | tf_op | source)
XLA Modules:
  0.0 81.6 jit_solution(5034223143383241111)
XLA Ops:
  0.6 77.8 %layer.1 = (bf16[32,4096]{1,0:T(8,128)(2,1)S(1)}, f32[32,128,128]{2,1,0:T(8,128)S(1)}, f32[32,128]{1,0:T(8,128)S(1)}, f32[1,32]{1,0:T(1,128)S(1)}) custom-call(bf16[32,4096]{1,0:T(8,128)(2,1)} %tok_h.1, f32[32,128,128]{2,1,0:T(8,128)} %bitcast.24, f32[32,128]{1,0:T(8,128)} %bitcast.30, f32[1,32]{1,0:T(1,128)} %bitcast.36, f32[1,4096]{1,0:T(1,128)} %bitcast.31, ...), custom_call_target="tpu_custom_call" | custom-call | tf_op jit(solution)/shard_map/layer/pallas_call | solution.py:783
  78.4 0.7 copy.33
  79.1 1.3 %copy.34 = f32[32,1,128,128]{3,2,1,0:T(8,128)} copy(f32[32,1,128,128]{3,2,1,0:T(8,128)S(1)} %bitcast.21) | data formatting | bytes 4194304
  80.4 0.5 copy.36
  81.0 0.6 copy.35

commit v6 on v5

--- a/solution.py
+++ b/solution.py
@@ -50,6 +50,7 @@
 (TOK, KEY, QKV, MIX, PROJ, RES, ROW, STA, DEN, HID, DWN_PAIR, DWN, EXP_PAIR, EXP, RET,
  OUT, NEAR, FAR, NEAR_DOWN, FAR_DOWN) = range(20)
 PHASES = 20
+AHEAD = 3
 PARTS = ((0, 64), (64, 64), (128, 128))
 
 
@@ -128,27 +129,38 @@
         return lax.rem(me_z + chips + lax.div(k + 1, 2) * (2 * lax.rem(k, 2) - 1), chips)
 
     def sum_over_tp(pair_phase, phase, part, pair, summed, arrived, make):
-        def give(k, _):
-            z = lax.rem(me_z + k, chips)
+        def give(k):
+            z = chip(k)
             at = 2 * z + 1 - core
             part[at] = make(at)
             tp_copy(pair_phase, part.at[at], pair.at[z], partner, z).start()
-            return 0
-
-        lax.fori_loop(1, chips + 1, give, 0)
 
         def add(z):
             mine = make(2 * z + core)
             tp_copy(pair_phase, pair.at[z], pair.at[z], partner, z).wait_recv()
             return mine.astype(F32) + pair[z].astype(F32)
 
-        def pass_on(k, _):
+        def pass_on(k):
             z = chip(k)
             summed[z] = add(z).astype(BF16)
             tp_copy(phase, summed.at[z], arrived.at[me_z], 2 * z + core, 0).start()
+
+        def both(k, _):
+            give(k)
+            pass_on(k - AHEAD)
             return 0
 
-        lax.fori_loop(1, chips, pass_on, 0)
+        def first(k, _):
+            give(k)
+            return 0
+
+        def last(k, _):
+            pass_on(k)
+            return 0
+
+        lax.fori_loop(1, AHEAD + 1, first, 0)
+        lax.fori_loop(AHEAD + 1, chips + 1, both, 0)
+        lax.fori_loop(chips + 1 - AHEAD, chips, last, 0)
         return add(me_z)
 
     def summed_over_tp(phase, arrived, acc):
@@ -482,7 +494,9 @@
         at = pl.multiple_of(side * lax.rem(me_y + dy, side), side)
         y = jnp.dot(pick[pl.ds(pl.multiple_of(at * few_rows, side * few_rows), side * few_rows), :],
                     res_half, preferred_element_type=F32)
-        row_out[pl.ds(at, side)] = y.reshape(side, few_rows, half_side * block).astype(BF16)
+        y = y.reshape(side, few_rows, half_side * block)
+        row_out[pl.ds(at, side)] = jnp.concatenate(
+            [y[:, :, k * block:(k + 1) * block] for k in range(half_side)], axis=1).astype(BF16)
         for dx in far_first:
             if dy or dx:
                 peer, spot = ep_at(dy, dx), core * n + me_e
@@ -526,7 +540,9 @@
     deep = half_side * block
 
     def expert_in(y, half, ss):
-        x = row_in[pl.ds(half * n + y * side, side)].astype(F32).reshape(cap_rows, deep)
+        x = row_in[pl.ds(half * n + y * side, side)].astype(F32)
+        x = jnp.concatenate(
+            [x[:, k * few_rows:(k + 1) * few_rows].reshape(cap_rows, block) for k in range(half_side)], axis=1)
         at = pl.multiple_of(y * side * block + half * deep, deep)
         xg = (x * fgain[:, pl.ds(at, deep)]).astype(BF16)
         gu_acc[:, pl.ds(0, hid_e)] += jnp.dot(xg, eg[pl.ds(at, deep), :], preferred_element_type=F32)
@@ -720,6 +736,15 @@
     @pl.when(own_column)
     def _():
         sent(ep_copy, RES, res_all.at[rest])
+
+
+def put_out(*refs):
+    *arrays, sem = refs
+    copies = [pltpu.make_async_copy(arrays[k], arrays[4 + k], sem.at[k]) for k in range(4)]
+    for copy in copies:
+        copy.start()
+    for copy in copies:
+        copy.wait()
 
 
 def on_device(
@@ -766,7 +791,7 @@
         vm((n, rows, 4 * head), BF16), vm((n, rows, 4 * head), BF16),
         vm((rows, head), BF16), vm((rows, n * head), BF16),
         vm((rows, block), BF16), vm((n, rows, block), BF16), vm((rows, block), BF16),
-        vm((n, few_rows, side * block // 2), BF16), vm((2 * n, few_rows, side * block // 2), BF16),
+        vm((n, few_rows * side // 2, block), BF16), vm((2 * n, few_rows * side // 2, block), BF16),
         vm((side, 8, 128), F32), vm((side, 8, 128), F32),
         vm((side, rows, 2 * hid_d), BF16), vm((side, rows, 2 * hid_d), BF16),
         vm((side, rows, hid_d), BF16), *[vm((n, rows, block), BF16)] * 3, vm((n // 2, rows, block), BF16),
@@ -792,6 +817,16 @@
             collective_id=0, has_side_effects=True, vmem_limit_bytes=56 * 1024 * 1024),
         name="layer",
     )(*args)
+    results = (layer_out, new_matrix, new_norm, new_max)
+    results = tuple(pltpu.with_memory_space_constraint(r, vm) for r in results)
+    layer_out, new_matrix, new_norm, new_max = pl.pallas_call(
+        put_out,
+        out_shape=tuple(jax.ShapeDtypeStruct(r.shape, r.dtype) for r in results),
+        in_specs=[pl.BlockSpec(memory_space=vm)] * 4,
+        out_specs=[any_space] * 4,
+        scratch_shapes=[dma((4,))],
+        name="put_out",
+    )(*results)
     return (layer_out, new_matrix.reshape(rows, 1, head, head), new_norm.reshape(rows, 1, head), new_max.T)
 
 

time: 81.6 us -> 80.1 us (0.982)
  local copies, waits for them, and re-layouts: 3.14 us -> 0 us
  Pallas kernels: 77.8 us -> 79.4 us
    unnamed x4 -> x0, local copies, waits for them, and re-layouts: 3.14 us -> none
    pallas_call x0 -> x1, Pallas kernels: none -> 1.45 us  [on_device(): pl.pallas_call(put_out, out_shape=tuple((jax.ShapeDtypeStruct(r.shape, r....]
where the time goes in v6:
time: 80.1 us; the launch traced here: 80 us
  Pallas kernels  79.4 us (99%)
    pallas_call x1, Pallas kernels, on_device(): pl.pallas_call(functools.partial(layer_kernel, n), out_shape=(vm((rows, w...  77.9 us

profile of v6, /device:TPU:1, one launch (start us, length us, event | category | flops | bytes accessed | tf_op | source)
XLA Modules:
  0.0 80.0 jit_solution(312281792748688276)
XLA Ops:
  0.6 77.9 %layer.1 = (bf16[32,4096]{1,0:T(8,128)(2,1)S(1)}, f32[32,128,128]{2,1,0:T(8,128)S(1)}, f32[32,128]{1,0:T(8,128)S(1)}, f32[1,32]{1,0:T(1,128)S(1)}) custom-call(bf16[32,4096]{1,0:T(8,128)(2,1)} %tok_h.1, f32[32,128,128]{2,1,0:T(8,128)} %bitcast.21, f32[32,128]{1,0:T(8,128)} %bitcast.27, f32[1,32]{1,0:T(1,128)} %bitcast.33, f32[1,4096]{1,0:T(1,128)} %bitcast.28, ...), custom_call_target="tpu_custom_call" | custom-call | tf_op jit(solution)/shard_map/layer/pallas_call | solution.py:808
  78.6 1.4 %put_out.1 = (bf16[32,4096]{1,0:T(8,128)(2,1)}, f32[32,128,128]{2,1,0:T(8,128)}, f32[32,128]{1,0:T(8,128)}, f32[1,32]{1,0:T(1,128)}) custom-call(bf16[32,4096]{1,0:T(8,128)(2,1)S(1)} %get-tuple-element.12.refs_0_, f32[32,128,128]{2,1,0:T(8,128)S(1)} %get-tuple-element.13.refs_1_, f32[32,128]{1,0:T(8,128)S(1)} %get-tuple-element.14.refs_2_, ...), custom_call_target="tpu_custom_call" | custom-call | tf_op jit(solution)/shard_map/put_out/pallas_call | solution.py:822

commit v7 on v6

--- a/solution.py
+++ b/solution.py
@@ -34,6 +34,12 @@
 
 def iota(shape, dim):
     return lax.broadcasted_iota(jnp.int32, shape, dim)
+
+
+def loop(first, end, body, carry):
+    for k in range(first, end):
+        carry = body(k, carry)
+    return carry
 
 
 def to_column(row, rows):
@@ -158,9 +164,9 @@
             pass_on(k)
             return 0
 
-        lax.fori_loop(1, AHEAD + 1, first, 0)
-        lax.fori_loop(AHEAD + 1, chips + 1, both, 0)
-        lax.fori_loop(chips + 1 - AHEAD, chips, last, 0)
+        loop(1, AHEAD + 1, first, 0)
+        loop(AHEAD + 1, chips + 1, both, 0)
+        loop(chips + 1 - AHEAD, chips, last, 0)
         return add(me_z)
 
     def summed_over_tp(phase, arrived, acc):
@@ -302,7 +308,7 @@
         def one(d, acc):
             return acc + buffer[lax.rem(me + d, many)].astype(F32)
 
-        return lax.fori_loop(1, many, one, acc)
+        return loop(1, many, one, acc)
 
     rest, few = pl.ds(0, n - 1), pl.ds(0, side - 1)
     far_first = (2, 1, 3, 0) if side == 4 else tuple(range(side))
@@ -575,7 +581,7 @@
 
     gu_acc[...] = jnp.zeros_like(gu_acc)
     ss = expert_first(0, jnp.zeros((cap_rows, 1), F32))
-    ss = lax.fori_loop(1, side, lambda d, ss: expert_second(d - 1, expert_first(d, ss)), ss)
+    ss = loop(1, side, lambda d, ss: expert_second(d - 1, expert_first(d, ss)), ss)
     ss = expert_second(side - 1, ss)
     row_scale = lax.rsqrt(ss / width + EPS)
     g = gu_acc[:, :hid_e] * row_scale

time: 80.1 us -> 78.7 us (0.983)
  Pallas kernels: 79.4 us -> 77.9 us
    pallas_call x1, Pallas kernels: 77.9 us -> 76.5 us  [on_device(): pl.pallas_call(functools.partial(layer_kernel, n), out_shape=(vm((rows, w...]
where the time goes in v7:
time: 78.7 us; the launch traced here: 78.6 us
  Pallas kernels  77.9 us (99%)
    pallas_call x1, Pallas kernels, on_device(): pl.pallas_call(functools.partial(layer_kernel, n), out_shape=(vm((rows, w...  76.5 us

profile of v7, /device:TPU:1, one launch (start us, length us, event | category | flops | bytes accessed | tf_op | source)
XLA Modules:
  0.0 78.6 jit_solution(176285875346949249)
XLA Ops:
  0.6 76.5 %layer.1 = (bf16[32,4096]{1,0:T(8,128)(2,1)S(1)}, f32[32,128,128]{2,1,0:T(8,128)S(1)}, f32[32,128]{1,0:T(8,128)S(1)}, f32[1,32]{1,0:T(1,128)S(1)}) custom-call(bf16[32,4096]{1,0:T(8,128)(2,1)} %tok_h.1, f32[32,128,128]{2,1,0:T(8,128)} %bitcast.21, f32[32,128]{1,0:T(8,128)} %bitcast.27, f32[1,32]{1,0:T(1,128)} %bitcast.33, f32[1,4096]{1,0:T(1,128)} %bitcast.28, ...), custom_call_target="tpu_custom_call" | custom-call | tf_op jit(solution)/shard_map/layer/pallas_call | solution.py:814
  77.1 1.4 %put_out.1 = (bf16[32,4096]{1,0:T(8,128)(2,1)}, f32[32,128,128]{2,1,0:T(8,128)}, f32[32,128]{1,0:T(8,128)}, f32[1,32]{1,0:T(1,128)}) custom-call(bf16[32,4096]{1,0:T(8,128)(2,1)S(1)} %get-tuple-element.12.refs_0_, f32[32,128,128]{2,1,0:T(8,128)S(1)} %get-tuple-element.13.refs_1_, f32[32,128]{1,0:T(8,128)S(1)} %get-tuple-element.14.refs_2_, ...), custom_call_target="tpu_custom_call" | custom-call | tf_op jit(solution)/shard_map/put_out/pallas_call | solution.py:828

commit v8 on v7

--- a/solution.py
+++ b/solution.py
@@ -56,7 +56,7 @@
 (TOK, KEY, QKV, MIX, PROJ, RES, ROW, STA, DEN, HID, DWN_PAIR, DWN, EXP_PAIR, EXP, RET,
  OUT, NEAR, FAR, NEAR_DOWN, FAR_DOWN) = range(20)
 PHASES = 20
-AHEAD = 3
+AHEAD = 2
 PARTS = ((0, 64), (64, 64), (128, 128))
 
 

time: 78.7 us -> 78.6 us (level)
  no operation moved by 1% of the time
where the time goes in v8:
time: 78.6 us; the launch traced here: 78.5 us
  Pallas kernels  77.8 us (99%)
    pallas_call x1, Pallas kernels, on_device(): pl.pallas_call(functools.partial(layer_kernel, n), out_shape=(vm((rows, w...  76.4 us

profile of v8, /device:TPU:1, one launch (start us, length us, event | category | flops | bytes accessed | tf_op | source)
XLA Modules:
  0.0 78.5 jit_solution(9757431730656026917)
XLA Ops:
  0.6 76.4 %layer.1 = (bf16[32,4096]{1,0:T(8,128)(2,1)S(1)}, f32[32,128,128]{2,1,0:T(8,128)S(1)}, f32[32,128]{1,0:T(8,128)S(1)}, f32[1,32]{1,0:T(1,128)S(1)}) custom-call(bf16[32,4096]{1,0:T(8,128)(2,1)} %tok_h.1, f32[32,128,128]{2,1,0:T(8,128)} %bitcast.21, f32[32,128]{1,0:T(8,128)} %bitcast.27, f32[1,32]{1,0:T(1,128)} %bitcast.33, f32[1,4096]{1,0:T(1,128)} %bitcast.28, ...), custom_call_target="tpu_custom_call" | custom-call | tf_op jit(solution)/shard_map/layer/pallas_call | solution.py:814
  77.1 1.4 %put_out.1 = (bf16[32,4096]{1,0:T(8,128)(2,1)}, f32[32,128,128]{2,1,0:T(8,128)}, f32[32,128]{1,0:T(8,128)}, f32[1,32]{1,0:T(1,128)}) custom-call(bf16[32,4096]{1,0:T(8,128)(2,1)S(1)} %get-tuple-element.12.refs_0_, f32[32,128,128]{2,1,0:T(8,128)S(1)} %get-tuple-element.13.refs_1_, f32[32,128]{1,0:T(8,128)S(1)} %get-tuple-element.14.refs_2_, ...), custom_call_target="tpu_custom_call" | custom-call | tf_op jit(solution)/shard_map/put_out/pallas_call | solution.py:828
